TPU v7x, 128 devices: a whole 4x4x4 slice. The times are simulated.
128 devices in a mesh: sp: 16 (over z, y), tp: 8 (over x, core).
Axes of the slice: x: 4, y: 4, z: 4, core: 2. Of those that a mesh axis runs over, the one named last changes fastest.
Arguments:
- queries: bfloat16 [16384, 1024], P('sp', 'tp'), may hold values from -6 to 6
- keys: bfloat16 [16384, 1024], P('sp', 'tp'), may hold values from -6 to 6
- values: bfloat16 [16384, 1024], P('sp', 'tp'), may hold values from -6 to 6
- stick_bias: bfloat16 [16384, 8], P('sp', 'tp'), may hold values from -14 to 0
- residual: bfloat16 [16384, 2048], P(('sp', 'tp')), may hold values from -6 to 6
- out_weight: bfloat16 [1024, 2048], replicated, may hold values from -0.1875 to 0.1875
- norm_gain: float32 [2048], replicated, may hold values from 0.1 to 1.9
- gate_weight: bfloat16 [2048, 5632], P('sp', 'tp'), may hold values from -0.125 to 0.125
- value_weight: bfloat16 [2048, 5632], P('sp', 'tp'), may hold values from -0.125 to 0.125
- down_weight: bfloat16 [2048, 5632], P('sp', 'tp'), may hold values from -0.078125 to 0.078125
- conv_gate: float32 [3, 5632], P(None, 'tp'), may hold values from -3.5 to 3.5
- conv_value: float32 [3, 5632], P(None, 'tp'), may hold values from -3.5 to 3.5
Outputs:
- mixed: bfloat16 [16384, 2048], P(('sp', 'tp'))
All inputs are finite; a program needn't handle non-finite values.
Results may differ from a plain program's by a relative error of at most 0.023.
Values may be sent and summed in bfloat16 or wider, within the bound.
A program may use at most 128 MiB of HBM per device.

v0:
```python
import jax
import jax.numpy as jnp
from jax import lax
from jax.sharding import PartitionSpec as P

EPS = 1e-06


def in_one_piece(arrays, axis, dim, along):
    widths = [a.shape[along] for a in arrays]
    both = jnp.concatenate(arrays, axis=along)
    out = lax.all_gather(both, axis, axis=dim, tiled=True)
    return tuple(jnp.split(out, [sum(widths[:k]) for k in range(1, len(widths))], axis=along))


def from_behind(block, axis, distance):
    devices = range(lax.axis_size(axis))
    route = [(i - distance, i) for i in devices if i - distance in devices]
    return lax.ppermute(block, axis, route)


def round_keep(value):
    return lax.optimization_barrier(value.astype(jnp.bfloat16)).astype(jnp.float32)


def local(
    queries,
    keys,
    values,
    stick_bias,
    residual,
    out_weight,
    norm_gain,
    gate_weight,
    value_weight,
    down_weight,
    conv_gate,
    conv_value,
):
    rows_here = queries.shape[0]
    heads_here = stick_bias.shape[1]
    head_size = queries.shape[1] // heads_here
    width_here = queries.shape[1]
    model_width = residual.shape[1]
    units_here = gate_weight.shape[1]
    sp_count = lax.axis_size("sp")
    tp_count = lax.axis_size("tp")
    my_block = lax.axis_index("sp")
    row_share = rows_here // tp_count
    scale = head_size ** (-0.5)
    whole_gate, whole_value, whole_down = in_one_piece(
        (gate_weight, value_weight, down_weight), "sp", 0, 1
    )
    key_all, value_all, bias_all = in_one_piece((keys, values, stick_bias), "sp", 0, 1)
    query_heads = queries.reshape(rows_here, heads_here, head_size)
    query_pos = my_block * rows_here + jnp.arange(rows_here, dtype=jnp.int32)

    def visit(step, carry):
        block_index = my_block - step

        def work(state):
            acc_out, acc_log = state
            offset = block_index * rows_here
            key_block = lax.dynamic_slice_in_dim(key_all, offset, rows_here, 0).reshape(
                rows_here, heads_here, head_size
            )
            value_block = lax.dynamic_slice_in_dim(value_all, offset, rows_here, 0).reshape(
                rows_here, heads_here, head_size
            )
            bias_block = lax.dynamic_slice_in_dim(bias_all, offset, rows_here, 0).astype(
                jnp.float32
            )
            scores = (
                jnp.einsum(
                    "qhd,khd->hqk", query_heads, key_block, preferred_element_type=jnp.float32
                )
                * scale
            )
            scores = scores + bias_block.T[:, None, :]
            key_pos = offset + jnp.arange(rows_here, dtype=jnp.int32)
            before = (key_pos[None, :] < query_pos[:, None])[None]
            log_keep = jnp.where(before, jax.nn.log_sigmoid(-scores), 0.0)
            after = lax.cumsum(log_keep, axis=2, reverse=True) - log_keep
            stick = jnp.where(
                before, jnp.exp(jax.nn.log_sigmoid(scores) + after + acc_log[:, :, None]), 0.0
            )
            stick = stick.astype(jnp.bfloat16)
            acc_out = acc_out + jnp.einsum(
                "hqk,khd->qhd", stick, value_block, preferred_element_type=jnp.float32
            )
            acc_log = acc_log + jnp.sum(log_keep, axis=2)
            return (acc_out, acc_log)

        return lax.cond(block_index >= 0, work, lambda state: state, carry)

    start_state = (
        jnp.zeros((rows_here, heads_here, head_size), jnp.float32),
        jnp.zeros((heads_here, rows_here), jnp.float32),
    )
    acc_out, acc_log = lax.fori_loop(0, sp_count, visit, start_state)
    attended = acc_out.reshape(rows_here, width_here).astype(jnp.bfloat16)
    row_heads = lax.all_to_all(attended, "tp", split_axis=0, concat_axis=1, tiled=True)
    grouped = jnp.einsum(
        "rgc,gcd->grd",
        row_heads.reshape(row_share, tp_count, width_here),
        out_weight.reshape(tp_count, width_here, model_width),
        preferred_element_type=jnp.float32,
    )
    projected = jnp.sum(round_keep(grouped), axis=0)
    middle_f = (residual.astype(jnp.float32) + projected).astype(jnp.bfloat16).astype(jnp.float32)
    normed = (
        middle_f
        * lax.rsqrt(jnp.mean(middle_f * middle_f, axis=-1, keepdims=True) + EPS)
        * norm_gain
    ).astype(jnp.bfloat16)
    piece = lax.all_gather(normed, "tp", axis=0, tiled=True)
    gate_part = jnp.dot(piece, whole_gate, preferred_element_type=jnp.float32).astype(jnp.bfloat16)
    value_part = jnp.dot(piece, whole_value, preferred_element_type=jnp.float32).astype(
        jnp.bfloat16
    )
    both_up = jnp.concatenate([gate_part, value_part], axis=1)
    gate_up = both_up[:, :units_here]
    value_up = both_up[:, units_here:]
    rim_gate, rim_value = from_behind((gate_up[-2:], value_up[-2:]), "sp", 1)

    def depthwise(rim, upward, taps):
        extended = jnp.concatenate([rim, upward], axis=0).astype(jnp.float32)
        return taps[0] * extended[:-2] + taps[1] * extended[1:-1] + taps[2] * extended[2:]

    hidden = (
        jax.nn.silu(depthwise(rim_gate, gate_up, conv_gate))
        * depthwise(rim_value, value_up, conv_value)
    ).astype(jnp.bfloat16)
    down_total = lax.psum_scatter(
        round_keep(
            lax.dot_general(
                hidden, whole_down, (((1,), (1,)), ((), ())), preferred_element_type=jnp.float32
            )
        ).astype(jnp.bfloat16),
        "tp",
        scatter_dimension=0,
        tiled=True,
    ).astype(jnp.float32)
    return (middle_f + down_total).astype(jnp.bfloat16)


def solution(mesh):
    in_specs = (
        P("sp", "tp"),
        P("sp", "tp"),
        P("sp", "tp"),
        P("sp", "tp"),
        P(("sp", "tp"), None),
        P(),
        P(),
        P("sp", "tp"),
        P("sp", "tp"),
        P("sp", "tp"),
        P(None, "tp"),
        P(None, "tp"),
    )
    out_specs = P(("sp", "tp"), None)
    return jax.shard_map(local, mesh=mesh, in_specs=in_specs, out_specs=out_specs, check_vma=False)
```

profile of v0, /device:TPU:26, one launch (start us, length us, event | category | flops | bytes accessed | tf_op | source)
XLA Modules:
  0.0 703.0 jit_solution(2536579153862566432)
XLA Ops:
  12.4 72.3 %all-gather.4.cloned.1.call-done = bf16[16384,257]{0,1:T(8,128)(2,1)} async-done(((bf16[1024,257]{0,1:T(8,128)(2,1)}), bf16[16384,257]{0,1:T(8,128)(2,1)}) %all-gather.4.cloned.1.call-update) | async-done | bytes 8421392 | tf_op jit(solution)/shard_map/all_gather | solution.py:12
  84.7 5.9 fusion.47
  90.6 6.4 copy.24
  97.0 6.5 copy.25
  104.5 119.5 %while.16 = (s32[]{:T(128)}, f32[1024,1,128]{0,2,1:T(8,128)S(1)}, f32[1,1024]{1,0:T(1,128)S(1)}, s32[]{:T(128)}, bf16[16384,128]{1,0:T(8,128)(2,1)}, /*index=5*/...) while((s32[]{:T(128)}, f32[1024,1,128]{0,2,1:T(8,128)S(1)}, ...), condition=%wide.region_6.7_spmd.clone, body=%wide.region_0.6_spmd.clone.sunk | while | flops 700647424 | bytes 60856664 | solution.py:100
  104.6 29.8 %conditional.3 = ((f32[1024,1,128]{0,2,1:T(8,128)S(1)}, f32[1,1024]{1,0:T(1,128)S(1)})) conditional(s32[]{:T(128)} %convert_element_type.109, (f32[1024,1,128]{0,2,1:T(8,128)S(1)}, f32[1,1024]{1,0:T(1,128)S(1)}) %tuple.56, (s32[]{:T(128)}, bf16[16384,128]{1,0:T(8,128)(2,1)}, s32[]{:T(128)}, bf16[16384,128]{1,0:T(8,128)(2,1)}, ...), branch_computations={%region_1.0_spmd, %region_2.5_spmd} | conditional | flops 700647424 | bytes 60852344 | solution.py:94
  104.6 6.1 fusion.46
  110.7 10.1 %fusion.13 = f32[1,1024,8,128]{1,2,3,0:T(8,128)S(1)} fusion(f32[1,1024,8,128]{1,3,2,0:T(8,128)S(1)} %bitcast.57), kind=kOutput, calls=%fused_computation.20 | output fusion | flops 133169152 | bytes 8388608 | tf_op jit(solution)/shard_map/reduce-window
  120.8 4.4 copy.21
  125.3 7.6 %fusion.2 = bf16[1024,1024]{0,1:T(8,128)(2,1)S(1)} fusion(f32[1024,1024]{0,1:T(8,128)} %copy-done, f32[1,1024,8,128]{1,3,2,0:T(8,128)} %copy.21, f32[1024,1024]{1,0:T(8,128)} %get-tuple-element.266, f32[1024]{0:T(1024)S(1)} %bitcast.60, f32[1024,8]{0,1:T(8,128)S(1)} %slice_bitcast_fusion, f32[1024]{0:T(1024)S(1)} %bitcast.62, ...), kind=kLoop, calls=%fused_computation.5 | loop fusion | flops 17825792 | bytes 14729216 | tf_op jit(solution)/shard_map/while/body/eval_jaxpr/cond/branch_1_fun/convert_element_type | solution.py:87
  134.4 29.7 %conditional.3 = ((f32[1024,1,128]{0,2,1:T(8,128)S(1)}, f32[1,1024]{1,0:T(1,128)S(1)})) conditional(s32[]{:T(128)} %convert_element_type.109, (f32[1024,1,128]{0,2,1:T(8,128)S(1)}, f32[1,1024]{1,0:T(1,128)S(1)}) %tuple.56, (s32[]{:T(128)}, bf16[16384,128]{1,0:T(8,128)(2,1)}, s32[]{:T(128)}, bf16[16384,128]{1,0:T(8,128)(2,1)}, ...), branch_computations={%region_1.0_spmd, %region_2.5_spmd} | conditional | flops 700647424 | bytes 60852344 | solution.py:94
  134.5 6.1 fusion.46
  140.5 10.1 %fusion.13 = f32[1,1024,8,128]{1,2,3,0:T(8,128)S(1)} fusion(f32[1,1024,8,128]{1,3,2,0:T(8,128)S(1)} %bitcast.57), kind=kOutput, calls=%fused_computation.20 | output fusion | flops 133169152 | bytes 8388608 | tf_op jit(solution)/shard_map/reduce-window
  150.6 4.4 copy.21
  155.1 7.5 %fusion.2 = bf16[1024,1024]{0,1:T(8,128)(2,1)S(1)} fusion(f32[1024,1024]{0,1:T(8,128)} %copy-done, f32[1,1024,8,128]{1,3,2,0:T(8,128)} %copy.21, f32[1024,1024]{1,0:T(8,128)} %get-tuple-element.266, f32[1024]{0:T(1024)S(1)} %bitcast.60, f32[1024,8]{0,1:T(8,128)S(1)} %slice_bitcast_fusion, f32[1024]{0:T(1024)S(1)} %bitcast.62, ...), kind=kLoop, calls=%fused_computation.5 | loop fusion | flops 17825792 | bytes 14729216 | tf_op jit(solution)/shard_map/while/body/eval_jaxpr/cond/branch_1_fun/convert_element_type | solution.py:87
  164.2 29.6 %conditional.3 = ((f32[1024,1,128]{0,2,1:T(8,128)S(1)}, f32[1,1024]{1,0:T(1,128)S(1)})) conditional(s32[]{:T(128)} %convert_element_type.109, (f32[1024,1,128]{0,2,1:T(8,128)S(1)}, f32[1,1024]{1,0:T(1,128)S(1)}) %tuple.56, (s32[]{:T(128)}, bf16[16384,128]{1,0:T(8,128)(2,1)}, s32[]{:T(128)}, bf16[16384,128]{1,0:T(8,128)(2,1)}, ...), branch_computations={%region_1.0_spmd, %region_2.5_spmd} | conditional | flops 700647424 | bytes 60852344 | solution.py:94
  164.2 6.1 fusion.46
  170.3 10.1 %fusion.13 = f32[1,1024,8,128]{1,2,3,0:T(8,128)S(1)} fusion(f32[1,1024,8,128]{1,3,2,0:T(8,128)S(1)} %bitcast.57), kind=kOutput, calls=%fused_computation.20 | output fusion | flops 133169152 | bytes 8388608 | tf_op jit(solution)/shard_map/reduce-window
  180.4 4.4 copy.21
  184.9 7.4 %fusion.2 = bf16[1024,1024]{0,1:T(8,128)(2,1)S(1)} fusion(f32[1024,1024]{0,1:T(8,128)} %copy-done, f32[1,1024,8,128]{1,3,2,0:T(8,128)} %copy.21, f32[1024,1024]{1,0:T(8,128)} %get-tuple-element.266, f32[1024]{0:T(1024)S(1)} %bitcast.60, f32[1024,8]{0,1:T(8,128)S(1)} %slice_bitcast_fusion, f32[1024]{0:T(1024)S(1)} %bitcast.62, ...), kind=kLoop, calls=%fused_computation.5 | loop fusion | flops 17825792 | bytes 14729216 | tf_op jit(solution)/shard_map/while/body/eval_jaxpr/cond/branch_1_fun/convert_element_type | solution.py:87
  193.8 29.6 %conditional.3 = ((f32[1024,1,128]{0,2,1:T(8,128)S(1)}, f32[1,1024]{1,0:T(1,128)S(1)})) conditional(s32[]{:T(128)} %convert_element_type.109, (f32[1024,1,128]{0,2,1:T(8,128)S(1)}, f32[1,1024]{1,0:T(1,128)S(1)}) %tuple.56, (s32[]{:T(128)}, bf16[16384,128]{1,0:T(8,128)(2,1)}, s32[]{:T(128)}, bf16[16384,128]{1,0:T(8,128)(2,1)}, ...), branch_computations={%region_1.0_spmd, %region_2.5_spmd} | conditional | flops 700647424 | bytes 60852344 | solution.py:94
  193.9 6.1 fusion.46
  199.9 10.1 %fusion.13 = f32[1,1024,8,128]{1,2,3,0:T(8,128)S(1)} fusion(f32[1,1024,8,128]{1,3,2,0:T(8,128)S(1)} %bitcast.57), kind=kOutput, calls=%fused_computation.20 | output fusion | flops 133169152 | bytes 8388608 | tf_op jit(solution)/shard_map/reduce-window
  210.0 4.4 copy.21
  214.5 7.4 %fusion.2 = bf16[1024,1024]{0,1:T(8,128)(2,1)S(1)} fusion(f32[1024,1024]{0,1:T(8,128)} %copy-done, f32[1,1024,8,128]{1,3,2,0:T(8,128)} %copy.21, f32[1024,1024]{1,0:T(8,128)} %get-tuple-element.266, f32[1024]{0:T(1024)S(1)} %bitcast.60, f32[1024,8]{0,1:T(8,128)S(1)} %slice_bitcast_fusion, f32[1024]{0:T(1024)S(1)} %bitcast.62, ...), kind=kLoop, calls=%fused_computation.5 | loop fusion | flops 17825792 | bytes 14729216 | tf_op jit(solution)/shard_map/while/body/eval_jaxpr/cond/branch_1_fun/convert_element_type | solution.py:87
  224.3 10.6 %all_to_all.13 = bf16[8,128,128]{2,1,0:T(8,128)(2,1)S(1)} all-to-all(bf16[8,128,128]{2,1,0:T(8,128)(2,1)S(1)} %bitcast.59), channel_id=1, replica_groups=mesh['sp'=16,'tp'=8] {'tp'}, dimensions={0} | all-to-all | bytes 524288 | tf_op jit(solution)/shard_map/all_to_all | solution.py:102
  240.8 383.7 %all-gather.6.cloned.1.call-done = bf16[1024,2048]{1,0:T(8,128)(2,1)} async-done(((bf16[128,2048]{1,0:T(8,128)(2,1)}), bf16[1024,2048]{1,0:T(8,128)(2,1)}) %all-gather.6.cloned.1.call-update) | async-done | bytes 4194320 | tf_op jit(solution)/shard_map/all_gather | solution.py:116
  624.5 6.4 fusion.33
  634.5 5.0 fusion.36
  644.0 3.9 collective-permute-done.1
  648.7 10.6 %convolution_convert_fusion = bf16[1024,2048]{1,0:T(8,128)(2,1)} fusion(bf16[2048,2112]{0,1:T(8,128)(2,1)} %all-gather.8.cloned.1.call-done, f32[1026,704]{0,1:T(8,128)S(1)} %maximum_convert_fusion.1, f32[1026,704]{0,1:T(8,128)S(1)} %maximum_convert_fusion, f32[704]{0:T(1024)S(1)} %get-tuple-element.242, f32[704]{0:T(1024)S(1)} %get-tuple-element.243, ...), kind=kOutput, calls=%fused_computation.37 | convolution fusion | flops 2966421504 | bytes 24403968 | tf_op jit(solution)/shard_map/dot_general | solution.py:136
  659.3 35.2 %reduce-scatter.2.cloned.1.call-done = bf16[128,2048]{1,0:T(8,128)(2,1)} async-done(((bf16[1024,2048]{1,0:T(8,128)(2,1)}), bf16[128,2048]{1,0:T(8,128)(2,1)}) %reduce-scatter.2.cloned.1.call-update) | async-done | bytes 524304 | tf_op jit(solution)/shard_map/reduce_scatter | solution.py:134
  (108 shorter events, 30.0 us)
Async XLA Ops:
  6.5 78.2 %all-gather.4.cloned.1.call-start = ((), (), s32[]{:S(2)}) async-start(), calls=%async_computation.2 | async-start | bytes 9191424 | tf_op jit(solution)/shard_map/all_gather | solution.py:12
  10.3 230.5 %all-gather.8.cloned.1.call-start = ((), (), s32[]{:S(2)}) async-start(), calls=%async_computation.4 | async-start | bytes 9191424 | tf_op jit(solution)/shard_map/all_gather | solution.py:12
  12.3 612.2 %all-gather.6.cloned.1.call-start = ((), (), s32[]{:S(2)}) async-start(), calls=%async_computation.3 | async-start | bytes 4718592 | tf_op jit(solution)/shard_map/all_gather | solution.py:116
  97.0 7.5 %copy-start.6 = (bf16[1024,128]{1,0:T(8,128)(2,1)S(1)}, bf16[1024,128]{1,0:T(8,128)(2,1)}, u32[]{:S(2)}) copy-start(bf16[1024,128]{1,0:T(8,128)(2,1)} %param.16) | copy-start | bytes 786436
  110.7 10.1 %copy-start = (f32[1024,1024]{0,1:T(8,128)}, f32[1024,1024]{0,1:T(8,128)S(1)}, u32[]{:S(2)}) copy-start(f32[1024,1024]{0,1:T(8,128)S(1)} %get-tuple-element.263) | copy-start | bytes 12582916 | tf_op jit(solution)/shard_map/while/body/eval_jaxpr/cond
  140.5 10.1 %copy-start = (f32[1024,1024]{0,1:T(8,128)}, f32[1024,1024]{0,1:T(8,128)S(1)}, u32[]{:S(2)}) copy-start(f32[1024,1024]{0,1:T(8,128)S(1)} %get-tuple-element.263) | copy-start | bytes 12582916 | tf_op jit(solution)/shard_map/while/body/eval_jaxpr/cond
  170.3 10.1 %copy-start = (f32[1024,1024]{0,1:T(8,128)}, f32[1024,1024]{0,1:T(8,128)S(1)}, u32[]{:S(2)}) copy-start(f32[1024,1024]{0,1:T(8,128)S(1)} %get-tuple-element.263) | copy-start | bytes 12582916 | tf_op jit(solution)/shard_map/while/body/eval_jaxpr/cond
  199.9 10.1 %copy-start = (f32[1024,1024]{0,1:T(8,128)}, f32[1024,1024]{0,1:T(8,128)S(1)}, u32[]{:S(2)}) copy-start(f32[1024,1024]{0,1:T(8,128)S(1)} %get-tuple-element.263) | copy-start | bytes 12582916 | tf_op jit(solution)/shard_map/while/body/eval_jaxpr/cond
  238.3 1.0 copy-start.1
  238.4 1.3 copy-start.2
  238.4 2.3 copy-start.3
  238.4 2.3 copy-start.4
  240.6 453.9 %reduce-scatter.2.cloned.1.call-start = ((), (), s32[]{:S(2)}) async-start(), calls=%async_computation.5 | async-start | bytes 4718592 | tf_op jit(solution)/shard_map/reduce_scatter | solution.py:134
  624.5 9.9 %copy-start.5 = (bf16[1024,2048]{1,0:T(8,128)(2,1)S(1)}, bf16[1024,2048]{1,0:T(8,128)(2,1)}, u32[]{:S(2)}) copy-start(bf16[1024,2048]{1,0:T(8,128)(2,1)} %all-gather.6.cloned.1.call-done) | copy-start | bytes 12582916
  631.0 12.2 %collective-permute-start = (bf16[2,704]{0,1:T(8,128)(2,1)S(1)}, bf16[2,704]{0,1:T(8,128)(2,1)S(1)}, u32[]{:S(2)}, u32[]{:S(2)}) collective-permute-start(bf16[2,704]{0,1:T(8,128)(2,1)S(1)} %slice.64), channel_id=1, source_target_pairs={{0,8},{8,16},{16,24},{24,32},{32,40},{40,48},{48,56},{56,64},{64,7... | collective-permute-start | bytes 8456 | tf_op jit(solution)/shard_map/ppermute | solution.py:19
  639.6 8.3 %collective-permute-start.1 = (bf16[2,704]{0,1:T(8,128)(2,1)S(1)}, bf16[2,704]{0,1:T(8,128)(2,1)S(1)}, u32[]{:S(2)}, u32[]{:S(2)}) collective-permute-start(bf16[2,704]{0,1:T(8,128)(2,1)S(1)} %slice.68), channel_id=1, source_target_pairs={{0,8},{8,16},{16,24},{24,32},{32,40},{40,48},{48,56},{56,64},{64,7... | collective-permute-start | bytes 8456 | tf_op jit(solution)/shard_map/ppermute | solution.py:19
Sparse Core Ops, SparseCore 0:
  10.4 74.2 all-gather.3
  86.8 77.9 all-gather.7
  240.8 383.6 all-gather.5
  659.4 35.0 reduce-scatter.1
where the time goes:
time: 709 us; the launch traced here: 703 us
  waiting for transfers between devices  495 us (70%)
  other arithmetic  79.6 us (11%)
  matrix products  55.4 us (8%)
  local copies, waits for them, and re-layouts  40.5 us (6%)
  between operations  13.3 us (2%)
  blocking collectives  10.6 us (1%)
  starting transfers between devices  7.13 us (1%)
    all_gather x1, waiting for transfers between devices, local(): piece = lax.all_gather(normed, 'tp', axis=0, tiled=True)  384 us
    all_gather x2, waiting for transfers between devices, in_one_piece(): out = lax.all_gather(both, axis, axis=dim, tiled=True)  72.3 us
    another operation x8, other arithmetic  40.5 us
    reduce_scatter x1, waiting for transfers between devices, local(): lax.psum_scatter(round_keep(lax.dot_general(hidden, whole_down, (((1,), (...  35.2 us
    convert_element_type x4, other arithmetic, work(): stick = stick.astype(jnp.bfloat16)  30 us
    dot_general x4, matrix products, work(): jnp.einsum('qhd,khd->hqk', query_heads, key_block, preferred_element_type...  24.3 us
    another operation x12, local copies, waits for them, and re-layouts  17.7 us
    unnamed x16, local copies, waits for them, and re-layouts  15.4 us
  transfers between devices with their start and end apart: 6, of which 4 were waited for; matrix products, arithmetic and copies ran while one was open for 22% of the time, Pallas kernels for 0%

commit v1 on v0

v1 whole, which is shorter than its diff:
```python
import jax
import jax.numpy as jnp
from jax import lax
from jax.experimental import pallas as pl
from jax.experimental.pallas import tpu as pltpu
from jax.sharding import PartitionSpec as P

EPS = 1e-06
LOG2E = 1.4426950408889634
NT = (((1,), (1,)), ((), ()))
CHUNK = 256
PAD = 16


def from_behind(block, axis, distance):
    devices = range(lax.axis_size(axis))
    route = [(i - distance, i) for i in devices if i - distance in devices]
    return lax.ppermute(block, axis, route)


def tri_matrix():
    rows = lax.broadcasted_iota(jnp.int32, (CHUNK, CHUNK), 0)
    cols = lax.broadcasted_iota(jnp.int32, (CHUNK, CHUNK), 1)
    return (rows > cols).astype(jnp.bfloat16), rows > cols


def visit_chunk(q, k, v, bias, tri, gone, acc, mask=None):
    scale = 128 ** (-0.5) * LOG2E
    s = lax.dot_general(q, k, NT, preferred_element_type=jnp.float32) * scale + bias
    if mask is not None:
        s = jnp.where(mask, s, -1e30)
    soft = jnp.maximum(jnp.log(1.0 + jnp.exp2(jnp.minimum(s, 126.0))) * LOG2E, s)
    behind = jnp.dot(soft.astype(jnp.bfloat16), tri, preferred_element_type=jnp.float32)
    stick = jnp.exp2((s - soft) - (behind + gone)).astype(jnp.bfloat16)
    acc = acc + jnp.dot(stick, v, preferred_element_type=jnp.float32)
    gone = gone + (behind[:, 0:1] + soft[:, 0:1])
    return gone, acc


def attention_kernel(q_ref, kv_ref, o_ref, acc_ref, gone_ref):
    rows, head = q_ref.shape
    stride = rows + PAD
    chunks = rows // CHUNK
    me = lax.axis_index("sp")
    tri, lower = tri_matrix()

    def load(block, c):
        at = pl.ds(pl.multiple_of(block * stride + c * CHUNK, 16), CHUNK)
        return kv_ref[at, :head], kv_ref[at, head:]

    def biases(block):
        at = pl.ds(pl.multiple_of(block * stride + rows, 16), PAD)
        return kv_ref[at, :].astype(jnp.float32) * LOG2E

    bias = biases(me)
    for t in range(chunks):
        here = slice(t * CHUNK, (t + 1) * CHUNK)
        q = q_ref[here, :]
        gone = jnp.zeros((CHUNK, 1), jnp.float32)
        acc = jnp.zeros((CHUNK, head), jnp.float32)
        for c in range(t, -1, -1):
            k, v = load(me, c)
            gone, acc = visit_chunk(
                q, k, v, bias[c : c + 1, :], tri, gone, acc, lower if c == t else None
            )
        acc_ref[here, :] = acc
        gone_ref[here, :] = jnp.broadcast_to(gone, (CHUNK, head))

    def block_step(step, carry):
        block = me - 1 - step
        gone, acc = carry
        bias = biases(block)
        for c in range(chunks - 1, -1, -1):
            k, v = load(block, c)
            gone, acc = visit_chunk(q_ref[...], k, v, bias[c : c + 1, :], tri, gone, acc)
        return gone, acc

    gone, acc = lax.fori_loop(0, me, block_step, (gone_ref[:, 0:1], acc_ref[...]))
    o_ref[...] = acc.astype(o_ref.dtype)


def attention(queries, kv_all):
    rows, head = queries.shape
    vmem = pl.BlockSpec(memory_space=pltpu.VMEM)
    return pl.pallas_call(
        attention_kernel,
        out_shape=jax.ShapeDtypeStruct((rows, head), jnp.bfloat16),
        in_specs=[vmem, vmem],
        out_specs=vmem,
        scratch_shapes=[
            pltpu.VMEM((rows, head), jnp.float32),
            pltpu.VMEM((rows, head), jnp.float32),
        ],
        compiler_params=pltpu.CompilerParams(vmem_limit_bytes=48 * 2**20),
        cost_estimate=pl.CostEstimate(
            flops=16 * 6 * rows * rows * head, bytes_accessed=9 * 2**20, transcendentals=0
        ),
        name="attention",
    )(queries, kv_all)


def local(
    queries,
    keys,
    values,
    stick_bias,
    residual,
    out_weight,
    norm_gain,
    gate_weight,
    value_weight,
    down_weight,
    conv_gate,
    conv_value,
):
    rows_here = queries.shape[0]
    model_width = residual.shape[1]
    bias_rows = stick_bias.reshape(rows_here // CHUNK, CHUNK)
    kv = jnp.concatenate(
        [
            jnp.concatenate([keys, values], axis=1),
            jnp.pad(bias_rows, ((0, PAD - bias_rows.shape[0]), (0, 0))),
        ],
        axis=0,
    )
    kv_all = lax.all_gather(kv, "sp", axis=0, tiled=True)
    whole_gate = lax.all_gather(gate_weight, "sp", axis=0, tiled=True)
    whole_value = lax.all_gather(value_weight, "sp", axis=0, tiled=True)
    whole_down = lax.all_gather(down_weight, "sp", axis=0, tiled=True)
    attended = attention(queries, kv_all)
    row_heads = lax.all_to_all(attended, "tp", split_axis=0, concat_axis=1, tiled=True)
    projected = jnp.dot(row_heads, out_weight, preferred_element_type=jnp.float32)
    middle_f = (residual.astype(jnp.float32) + projected).astype(jnp.bfloat16).astype(jnp.float32)
    normed = (
        middle_f
        * lax.rsqrt(jnp.mean(middle_f * middle_f, axis=-1, keepdims=True) + EPS)
        * norm_gain
    ).astype(jnp.bfloat16)
    piece = lax.all_gather(normed, "tp", axis=0, tiled=True)
    gate_up = jnp.dot(piece, whole_gate, preferred_element_type=jnp.float32).astype(jnp.bfloat16)
    value_up = jnp.dot(piece, whole_value, preferred_element_type=jnp.float32).astype(jnp.bfloat16)
    rim_gate, rim_value = from_behind((gate_up[-2:], value_up[-2:]), "sp", 1)

    def depthwise(rim, upward, taps):
        extended = jnp.concatenate([rim, upward], axis=0).astype(jnp.float32)
        return taps[0] * extended[:-2] + taps[1] * extended[1:-1] + taps[2] * extended[2:]

    hidden = (
        jax.nn.silu(depthwise(rim_gate, gate_up, conv_gate))
        * depthwise(rim_value, value_up, conv_value)
    ).astype(jnp.bfloat16)
    down = lax.dot_general(hidden, whole_down, NT, preferred_element_type=jnp.float32)
    down_total = lax.psum_scatter(
        down.astype(jnp.bfloat16), "tp", scatter_dimension=0, tiled=True
    ).astype(jnp.float32)
    return (middle_f + down_total).astype(jnp.bfloat16)


def solution(mesh):
    in_specs = (
        P("sp", "tp"),
        P("sp", "tp"),
        P("sp", "tp"),
        P("sp", "tp"),
        P(("sp", "tp"), None),
        P(),
        P(),
        P("sp", "tp"),
        P("sp", "tp"),
        P("sp", "tp"),
        P(None, "tp"),
        P(None, "tp"),
    )
    out_specs = P(("sp", "tp"), None)
    return jax.shard_map(local, mesh=mesh, in_specs=in_specs, out_specs=out_specs, check_vma=False)
```

time: 709 us -> 345 us (0.49)
  waiting for transfers between devices: 495 us -> 252 us
  other arithmetic: 79.6 us -> 10.5 us
  local copies, waits for them, and re-layouts: 40.5 us -> 1.47 us
  matrix products: 55.4 us -> 31.2 us
  Pallas kernels: 0 us -> 14.7 us
    all_gather x1, waiting for transfers between devices: 384 us -> 41.6 us  [local(): piece = lax.all_gather(normed, 'tp', axis=0, tiled=True)]
    all_gather x2 -> x4, waiting for transfers between devices: 72.3 us -> 172 us  [the longest x1 73.2 us: local(): kv_all = lax.all_gather(kv, 'sp', axis=0, tiled=True)]
    another operation x8 -> x0, other arithmetic: 40.5 us -> none
    convert_element_type x5 -> x0, other arithmetic: 30 us -> none  [the longest x4 30 us: work(): stick = stick.astype(jnp.bfloat16)]
    dot_general x10 -> x2, matrix products: 44 us -> 18.7 us  [the longest x1 15.7 us: local(): lax.dot_general(hidden, whole_down, NT, preferred_element_type=jnp.float32)]
    another operation x12 -> x0, local copies, waits for them, and re-layouts: 17.7 us -> none
    pallas_call x0 -> x1, Pallas kernels: none -> 14.7 us  [attention(): pl.pallas_call(attention_kernel, out_shape=jax.ShapeDtypeStruct((rows, he...]
    unnamed x16 -> x10, local copies, waits for them, and re-layouts: 15.4 us -> 0.96 us
  transfers between devices with their start and end apart: 6 -> 8, of which waited for: 4 -> 7; matrix products, arithmetic and copies ran while one was open for 22% -> 6% of each run, Pallas kernels for 0% -> 4%
where the time goes in v1:
time: 345 us; the launch traced here: 341 us
  waiting for transfers between devices  252 us (73%)
  matrix products  31.2 us (9%)
  Pallas kernels  14.7 us (4%)
  between operations  13.6 us (4%)
  blocking collectives  10.7 us (3%)
  other arithmetic  10.5 us (3%)
  starting transfers between devices  7.14 us (2%)
    all_gather x1, waiting for transfers between devices, local(): kv_all = lax.all_gather(kv, 'sp', axis=0, tiled=True)  73.2 us
    all_gather x1, waiting for transfers between devices, local(): whole_value = lax.all_gather(value_weight, 'sp', axis=0, tiled=True)  43.4 us
    all_gather x1, waiting for transfers between devices, local(): piece = lax.all_gather(normed, 'tp', axis=0, tiled=True)  41.6 us
    all_gather x1, waiting for transfers between devices, local(): whole_down = lax.all_gather(down_weight, 'sp', axis=0, tiled=True)  35.1 us
    reduce_scatter x1, waiting for transfers between devices, local(): lax.psum_scatter(down.astype(jnp.bfloat16), 'tp', scatter_dimension=0, ti...  34.1 us
    all_gather x1, waiting for transfers between devices, local(): whole_gate = lax.all_gather(gate_weight, 'sp', axis=0, tiled=True)  20.3 us
    dot_general x1, matrix products, local(): lax.dot_general(hidden, whole_down, NT, preferred_element_type=jnp.float32)  15.7 us
    pallas_call x1, Pallas kernels, attention(): pl.pallas_call(attention_kernel, out_shape=jax.ShapeDtypeStruct((rows, he...  14.7 us
  transfers between devices with their start and end apart: 8, of which 7 were waited for; matrix products, arithmetic and copies ran while one was open for 6% of the time, Pallas kernels for 4%

profile of v1, /device:TPU:26, one launch (start us, length us, event | category | flops | bytes accessed | tf_op | source)
XLA Modules:
  0.0 340.8 jit_solution(3400992977155542295)
XLA Ops:
  6.5 0.7 reduce
  7.3 1.9 fusion.10
  9.2 0.0 all-gather.10.cloned.1.call-start
  9.2 0.7 all-gather.10.cloned.1.call-update
  9.9 0.0 all-gather.8.cloned.1.call-start
  10.0 73.2 %all-gather.6.cloned.1.call-done.kv_ref = bf16[16640,256]{1,0:T(8,128)(2,1)} async-done(((bf16[1040,256]{1,0:T(8,128)(2,1)}), bf16[16640,256]{1,0:T(8,128)(2,1)}) %all-gather.6.cloned.1.call-update) | async-done | bytes 8519696 | tf_op jit(solution)/shard_map/all_gather | solution.py:126
  83.2 0.9 copy-done
  84.1 14.7 %attention.1 = bf16[1024,128]{1,0:T(8,128)(2,1)S(1)} custom-call(bf16[1024,128]{1,0:T(8,128)(2,1)S(1)} %copy-done, bf16[16640,256]{1,0:T(8,128)(2,1)} %all-gather.6.cloned.1.call-done.kv_ref), custom_call_target="tpu_custom_call" | custom-call | flops 12884901888 | bytes 9437184 | tf_op jit(solution)/shard_map/attention/pallas_call | solution.py:85
  98.8 0.2 copy.13
  99.0 10.7 %all_to_all.19 = bf16[8,128,128]{1,2,0:T(8,128)(2,1)S(1)} all-to-all(bf16[8,128,128]{1,2,0:T(8,128)(2,1)S(1)} %copy.13), channel_id=1, replica_groups=mesh['sp'=16,'tp'=8] {'tp'}, dimensions={0} | all-to-all | bytes 524288 | tf_op jit(solution)/shard_map/all_to_all | solution.py:131
  109.7 3.0 multiply_reduce_fusion
  112.7 1.0 multiply_convert_fusion
  113.7 0.0 all-gather.12.cloned.1.call-start
  113.7 0.5 all-gather.12.cloned.1.call-update
  114.3 0.5 all-gather.14.cloned.1.call-update
  114.9 0.1 slice_reduce_fusion.2
  115.0 20.3 %all-gather.10.cloned.1.call-done = bf16[2048,704]{0,1:T(8,128)(2,1)} async-done(((bf16[128,704]{0,1:T(8,128)(2,1)}), bf16[2048,704]{0,1:T(8,128)(2,1)}) %all-gather.10.cloned.1.call-update) | async-done | bytes 2883600 | tf_op jit(solution)/shard_map/all_gather | solution.py:127
  135.3 41.6 %all-gather.8.cloned.1.call-done = bf16[1024,2048]{1,0:T(8,128)(2,1)} async-done(((bf16[128,2048]{1,0:T(8,128)(2,1)}), bf16[1024,2048]{1,0:T(8,128)(2,1)}) %all-gather.8.cloned.1.call-update) | async-done | bytes 4194320 | tf_op jit(solution)/shard_map/all_gather | solution.py:139
  176.9 6.3 %convolution_convert_fusion.2 = bf16[1024,704]{0,1:T(8,128)(2,1)S(1)} fusion(bf16[1024,2048]{1,0:T(8,128)(2,1)} %all-gather.8.cloned.1.call-done, bf16[2048,704]{0,1:T(8,128)(2,1)} %all-gather.10.cloned.1.call-done), kind=kOutput, calls=%fused_computation.17 | convolution fusion | flops 2953510912 | bytes 8519680 | tf_op jit(solution)/shard_map/dot_general | solution.py:140
  183.2 0.1 slice.56
  183.3 3.6 %collective-permute-start = (bf16[2,704]{0,1:T(8,128)(2,1)S(1)}, bf16[2,704]{0,1:T(8,128)(2,1)S(1)}, u32[]{:S(2)}, u32[]{:S(2)}) collective-permute-start(bf16[2,704]{0,1:T(8,128)(2,1)S(1)} %slice.56), channel_id=1, source_target_pairs={{0,8},{8,16},{16,24},{24,32},{32,40},{40,48},{48,56},{56,64},{64,7... | collective-permute-start | bytes 8456 | tf_op jit(solution)/shard_map/ppermute | solution.py:18
  186.9 43.4 %all-gather.12.cloned.1.call-done = bf16[2048,704]{0,1:T(8,128)(2,1)} async-done(((bf16[128,704]{0,1:T(8,128)(2,1)}), bf16[2048,704]{0,1:T(8,128)(2,1)}) %all-gather.12.cloned.1.call-update) | async-done | bytes 2883600 | tf_op jit(solution)/shard_map/all_gather | solution.py:128
  230.3 6.3 %convolution_convert_fusion.1 = bf16[1024,704]{0,1:T(8,128)(2,1)S(1)} fusion(bf16[1024,2048]{1,0:T(8,128)(2,1)} %all-gather.8.cloned.1.call-done, bf16[2048,704]{0,1:T(8,128)(2,1)} %all-gather.12.cloned.1.call-done), kind=kOutput, calls=%fused_computation.16 | convolution fusion | flops 2953510912 | bytes 8519680 | tf_op jit(solution)/shard_map/dot_general | solution.py:141
  236.5 0.1 slice.60
  236.7 3.4 collective-permute-start.1
  240.1 2.5 maximum_convert_fusion
  242.6 2.1 collective-permute-done.1
  244.7 2.5 maximum_convert_fusion.1
  247.2 35.1 %all-gather.14.cloned.1.call-done = bf16[2048,704]{0,1:T(8,128)(2,1)} async-done(((bf16[128,704]{0,1:T(8,128)(2,1)}), bf16[2048,704]{0,1:T(8,128)(2,1)}) %all-gather.14.cloned.1.call-update) | async-done | bytes 2883600 | tf_op jit(solution)/shard_map/all_gather | solution.py:129
  282.3 15.7 %convolution_convert_fusion = bf16[1024,2048]{1,0:T(8,128)(2,1)} fusion(bf16[2048,704]{0,1:T(8,128)(2,1)} %all-gather.14.cloned.1.call-done, f32[1026,704]{0,1:T(8,128)} %maximum_convert_fusion.1, f32[1026,704]{0,1:T(8,128)} %maximum_convert_fusion, f32[704]{0:T(1024)S(1)} %get-tuple-element.9, f32[704]{0:T(1024)S(1)} %get-tuple-element.10, ...), kind=kOutput, calls=%fused_computation | convolution fusion | flops 2966421504 | bytes 24396288 | tf_op jit(solution)/shard_map/dot_general | solution.py:152
  297.9 34.1 %reduce-scatter.2.cloned.1.call-done = bf16[128,2048]{1,0:T(8,128)(2,1)} async-done(((bf16[1024,2048]{1,0:T(8,128)(2,1)}), bf16[128,2048]{1,0:T(8,128)(2,1)}) %reduce-scatter.2.cloned.1.call-update) | async-done | bytes 524304 | tf_op jit(solution)/shard_map/reduce_scatter | solution.py:153
  332.0 1.9 add_convert_fusion
  (18 shorter events, 0.2 us)
Async XLA Ops:
  6.5 76.7 %all-gather.6.cloned.1.call-start = ((), (), s32[]{:S(2)}) async-start(), calls=%async_computation.2 | async-start | bytes 9052160 | tf_op jit(solution)/shard_map/all_gather | solution.py:126
  9.2 126.2 %all-gather.10.cloned.1.call-start = ((), (), s32[]{:S(2)}) async-start(), calls=%async_computation.4 | async-start | bytes 3063808 | tf_op jit(solution)/shard_map/all_gather | solution.py:127
  9.9 167.0 %all-gather.8.cloned.1.call-start = ((), (), s32[]{:S(2)}) async-start(), calls=%async_computation.3 | async-start | bytes 4718592 | tf_op jit(solution)/shard_map/all_gather | solution.py:139
  83.2 0.9 copy-start
  84.1 25.5 %copy-start.1 = (bf16[128,2048]{1,0:T(8,128)(2,1)S(1)}, bf16[128,2048]{1,0:T(8,128)(2,1)}, u32[]{:S(2)}) copy-start(bf16[128,2048]{1,0:T(8,128)(2,1)} %param.16) | copy-start | bytes 1572868
  109.6 3.1 copy-start.2
  109.6 5.3 %copy-start.3 = (f32[3,704]{1,0:T(4,128)S(1)}, f32[3,704]{1,0:T(4,128)}, u32[]{:S(2)}) copy-start(f32[3,704]{1,0:T(4,128)} %param.23) | copy-start | bytes 25348
  109.6 5.3 %copy-start.4 = (f32[3,704]{1,0:T(4,128)S(1)}, f32[3,704]{1,0:T(4,128)}, u32[]{:S(2)}) copy-start(f32[3,704]{1,0:T(4,128)} %param.22) | copy-start | bytes 25348
  113.7 116.6 %all-gather.12.cloned.1.call-start = ((), (), s32[]{:S(2)}) async-start(), calls=%async_computation.5 | async-start | bytes 3063808 | tf_op jit(solution)/shard_map/all_gather | solution.py:128
  114.3 168.0 %all-gather.14.cloned.1.call-start = ((), (), s32[]{:S(2)}) async-start(), calls=%async_computation.6 | async-start | bytes 3063808 | tf_op jit(solution)/shard_map/all_gather | solution.py:129
  114.9 217.2 %reduce-scatter.2.cloned.1.call-start = ((), (), s32[]{:S(2)}) async-start(), calls=%async_computation.7 | async-start | bytes 4718592 | tf_op jit(solution)/shard_map/reduce_scatter | solution.py:153
  183.3 56.8 %collective-permute-start = (bf16[2,704]{0,1:T(8,128)(2,1)S(1)}, bf16[2,704]{0,1:T(8,128)(2,1)S(1)}, u32[]{:S(2)}, u32[]{:S(2)}) collective-permute-start(bf16[2,704]{0,1:T(8,128)(2,1)S(1)} %slice.56), channel_id=1, source_target_pairs={{0,8},{8,16},{16,24},{24,32},{32,40},{40,48},{48,56},{56,64},{64,7... | collective-permute-start | bytes 8456 | tf_op jit(solution)/shard_map/ppermute | solution.py:18
  236.7 8.0 %collective-permute-start.1 = (bf16[2,704]{0,1:T(8,128)(2,1)S(1)}, bf16[2,704]{0,1:T(8,128)(2,1)S(1)}, u32[]{:S(2)}, u32[]{:S(2)}) collective-permute-start(bf16[2,704]{0,1:T(8,128)(2,1)S(1)} %slice.60), channel_id=1, source_target_pairs={{0,8},{8,16},{16,24},{24,32},{32,40},{40,48},{48,56},{56,64},{64,7... | collective-permute-start | bytes 8456 | tf_op jit(solution)/shard_map/ppermute | solution.py:18
Sparse Core Ops, SparseCore 0:
  9.5 73.6 all-gather.5
  85.3 49.9 all-gather.9
  137.0 39.8 all-gather.7
  178.9 51.3 all-gather.11
  232.2 49.9 all-gather.13
  298.1 33.9 reduce-scatter.1

commit v2 on v1

--- a/solution.py
+++ b/solution.py
@@ -10,6 +10,7 @@
 NT = (((1,), (1,)), ((), ()))
 CHUNK = 256
 PAD = 16
+SIDE = 4
 
 
 def from_behind(block, axis, distance):
@@ -37,66 +38,323 @@
     return gone, acc
 
 
-def attention_kernel(q_ref, kv_ref, o_ref, acc_ref, gone_ref):
+def position():
+    me = lax.axis_index("sp")
+    return me, me // SIDE, me % SIDE
+
+
+def exchange_kernel(q_ref, k_ref, v_ref, b_ref, qs_ref, ks_ref, vs_ref, bs_ref, send_sem, recv_sem, q_send, q_recv):
+    me, z, y = position()
+    quarter = q_ref.shape[0] // SIDE
+
+    def copy_row(d, part):
+        src, dst = ((k_ref, ks_ref), (v_ref, vs_ref), (b_ref, bs_ref))[part]
+        return pltpu.make_async_remote_copy(
+            src_ref=src,
+            dst_ref=dst.at[y],
+            send_sem=send_sem.at[part, d],
+            recv_sem=recv_sem.at[part, y],
+            device_id={"sp": z * SIDE + (y + d) % SIDE},
+            device_id_type=pl.DeviceIdType.MESH,
+        )
+
+    def copy_query(dz, dy):
+        to_y = (y + dy) % SIDE
+        return pltpu.make_async_remote_copy(
+            src_ref=q_ref.at[pl.ds(pl.multiple_of(to_y * quarter, quarter), quarter)],
+            dst_ref=qs_ref.at[me],
+            send_sem=q_send.at[dz, dy],
+            recv_sem=q_recv.at[me],
+            device_id={"sp": (z - dz) * SIDE + to_y},
+            device_id_type=pl.DeviceIdType.MESH,
+        )
+
+    def for_queries(act):
+        for dz in range(SIDE):
+            for dy in range(SIDE):
+                if dz or dy:
+
+                    @pl.when(z >= dz)
+                    def _():
+                        act(copy_query(dz, dy))
+
+    for d in (2, 1, 3):
+        for part in range(3):
+            copy_row(d, part).start()
+    for_queries(lambda copy: copy.start())
+    for d in (1, 3, 2):
+        slot = (y + d) % SIDE
+        for part in range(3):
+            dst = (ks_ref, vs_ref, bs_ref)[part].at[slot]
+            pltpu.make_async_copy(dst, dst, recv_sem.at[part, slot]).wait()
+    for slot in range(SIDE * SIDE):
+
+        @pl.when((slot // SIDE >= z) & (slot != me))
+        def _():
+            dst = qs_ref.at[slot]
+            pltpu.make_async_copy(dst, dst, q_recv.at[slot]).wait()
+
+    for d in (1, 2, 3):
+        for part in range(3):
+            copy_row(d, part).wait_send()
+    for_queries(lambda copy: copy.wait_send())
+
+
+def exchange(queries, keys, values, bias_rows):
+    rows, head = queries.shape
+    anywhere = pl.BlockSpec(memory_space=pl.ANY)
+    count = SIDE * SIDE
+    return pl.pallas_call(
+        exchange_kernel,
+        out_shape=(
+            jax.ShapeDtypeStruct((count, rows // SIDE, head), jnp.bfloat16),
+            jax.ShapeDtypeStruct((SIDE, rows, head), jnp.bfloat16),
+            jax.ShapeDtypeStruct((SIDE, rows, head), jnp.bfloat16),
+            jax.ShapeDtypeStruct((SIDE,) + bias_rows.shape, jnp.bfloat16),
+        ),
+        in_specs=[anywhere] * 4,
+        out_specs=[anywhere] * 4,
+        scratch_shapes=[
+            pltpu.SemaphoreType.DMA((3, SIDE)),
+            pltpu.SemaphoreType.DMA((3, SIDE)),
+            pltpu.SemaphoreType.DMA((SIDE, SIDE)),
+            pltpu.SemaphoreType.DMA((count,)),
+        ],
+        compiler_params=pltpu.CompilerParams(has_side_effects=True),
+        cost_estimate=pl.CostEstimate(flops=10**10, bytes_accessed=4 * 2**20, transcendentals=0),
+        name="exchange",
+    )(queries, keys, values, bias_rows)
+
+
+def attention_kernel(
+    q_ref, k_ref, v_ref, b_ref, qs_ref, ks_ref, vs_ref, bs_ref,
+    o_ref, g_ref, q_all, k_all, v_all, b_all, acc_ref, gone_ref, kv_sem, q_sem,
+):
     rows, head = q_ref.shape
-    stride = rows + PAD
+    quarter = rows // SIDE
     chunks = rows // CHUNK
-    me = lax.axis_index("sp")
-    tri, lower = tri_matrix()
-
-    def load(block, c):
-        at = pl.ds(pl.multiple_of(block * stride + c * CHUNK, 16), CHUNK)
-        return kv_ref[at, :head], kv_ref[at, head:]
-
-    def biases(block):
-        at = pl.ds(pl.multiple_of(block * stride + rows, 16), PAD)
-        return kv_ref[at, :].astype(jnp.float32) * LOG2E
-
-    bias = biases(me)
-    for t in range(chunks):
-        here = slice(t * CHUNK, (t + 1) * CHUNK)
-        q = q_ref[here, :]
-        gone = jnp.zeros((CHUNK, 1), jnp.float32)
-        acc = jnp.zeros((CHUNK, head), jnp.float32)
-        for c in range(t, -1, -1):
-            k, v = load(me, c)
+    me, z, y = position()
+    tri, _ = tri_matrix()
+    own = (k_ref, v_ref, b_ref)
+    others = (ks_ref, vs_ref, bs_ref)
+    wholes = (k_all, v_all, b_all)
+
+    for slot in range(SIDE - 1, -1, -1):
+        for part in range(3):
+
+            @pl.when(slot == y)
+            def _():
+                pltpu.make_async_copy(own[part], wholes[part].at[slot], kv_sem.at[part, slot]).start()
+
+            @pl.when(slot != y)
+            def _():
+                pltpu.make_async_copy(
+                    others[part].at[slot], wholes[part].at[slot], kv_sem.at[part, slot]
+                ).start()
+
+    for slot in range(SIDE * SIDE):
+        dst = q_all.at[pl.ds(slot * quarter, quarter)]
+
+        @pl.when(slot == me)
+        def _():
+            src = q_ref.at[pl.ds(pl.multiple_of(y * quarter, quarter), quarter)]
+            pltpu.make_async_copy(src, dst, q_sem.at[slot]).start()
+
+        @pl.when((slot // SIDE >= z) & (slot != me))
+        def _():
+            pltpu.make_async_copy(qs_ref.at[slot], dst, q_sem.at[slot]).start()
+
+    for slot in range(SIDE * SIDE):
+
+        @pl.when(slot // SIDE >= z)
+        def _():
+            dst = q_all.at[pl.ds(slot * quarter, quarter)]
+            pltpu.make_async_copy(qs_ref.at[slot], dst, q_sem.at[slot]).wait()
+
+    for slot in range(SIDE):
+        for part in range(3):
+            pltpu.make_async_copy(
+                others[part].at[slot], wholes[part].at[slot], kv_sem.at[part, slot]
+            ).wait()
+
+    def finish(group, gone, acc):
+        for m in range(SIDE):
+            here = slice(m * quarter, (m + 1) * quarter)
+            o_ref[group * SIDE + m] = acc[here].astype(o_ref.dtype)
+            turned = jnp.broadcast_to(gone[here], (quarter, 128)).T
+            for half in range(2):
+                g_ref[group * SIDE + m, half] = turned[0:8, half * 128 : (half + 1) * 128]
+
+    acc_ref[...] = jnp.zeros_like(acc_ref)
+    gone_ref[...] = jnp.zeros_like(gone_ref)
+    for j in range(SIDE - 1, -1, -1):
+        low = j * quarter
+        size = rows - low
+        q = q_all[pl.ds(pl.multiple_of(z * rows + low, quarter), size), :]
+        bias = b_all[j].astype(jnp.float32) * LOG2E
+        acc = acc_ref[low:, :]
+        gone = gone_ref[low:, 0:1]
+        row = lax.broadcasted_iota(jnp.int32, (size, CHUNK), 0)
+        col = lax.broadcasted_iota(jnp.int32, (size, CHUNK), 1)
+        for c in range(chunks - 1, -1, -1):
+            at = slice(c * CHUNK, (c + 1) * CHUNK)
+            mask = (row >= quarter) | (col - row < y * quarter - c * CHUNK)
             gone, acc = visit_chunk(
-                q, k, v, bias[c : c + 1, :], tri, gone, acc, lower if c == t else None
+                q, k_all[j, at, :], v_all[j, at, :], bias[c : c + 1, :], tri, gone, acc, mask
             )
-        acc_ref[here, :] = acc
-        gone_ref[here, :] = jnp.broadcast_to(gone, (CHUNK, head))
-
-    def block_step(step, carry):
-        block = me - 1 - step
-        gone, acc = carry
-        bias = biases(block)
-        for c in range(chunks - 1, -1, -1):
-            k, v = load(block, c)
-            gone, acc = visit_chunk(q_ref[...], k, v, bias[c : c + 1, :], tri, gone, acc)
-        return gone, acc
-
-    gone, acc = lax.fori_loop(0, me, block_step, (gone_ref[:, 0:1], acc_ref[...]))
-    o_ref[...] = acc.astype(o_ref.dtype)
-
-
-def attention(queries, kv_all):
+        acc_ref[low:, :] = acc
+        gone_ref[low:, :] = jnp.broadcast_to(gone, (size, 128))
+    finish(z, gone_ref[:, 0:1], acc_ref[...])
+
+    def group_step(group, carry):
+        q = q_all[pl.ds(pl.multiple_of(group * rows, rows), rows), :]
+
+        def block_step(step, state):
+            gone, acc = state
+            j = SIDE - 1 - step
+            bias = b_all[j].astype(jnp.float32) * LOG2E
+            for c in range(chunks - 1, -1, -1):
+                at = slice(c * CHUNK, (c + 1) * CHUNK)
+                gone, acc = visit_chunk(
+                    q, k_all[j, at, :], v_all[j, at, :], bias[c : c + 1, :], tri, gone, acc
+                )
+            return gone, acc
+
+        start = (jnp.zeros((rows, 1), jnp.float32), jnp.zeros((rows, head), jnp.float32))
+        gone, acc = lax.fori_loop(0, SIDE, block_step, start)
+        finish(group, gone, acc)
+        return carry
+
+    lax.fori_loop(z + 1, SIDE, group_step, 0)
+
+
+def attention(queries, keys, values, bias_rows, q_parts, k_parts, v_parts, b_parts):
     rows, head = queries.shape
+    anywhere = pl.BlockSpec(memory_space=pl.ANY)
     vmem = pl.BlockSpec(memory_space=pltpu.VMEM)
+    count = SIDE * SIDE
     return pl.pallas_call(
         attention_kernel,
-        out_shape=jax.ShapeDtypeStruct((rows, head), jnp.bfloat16),
-        in_specs=[vmem, vmem],
-        out_specs=vmem,
+        out_shape=(
+            jax.ShapeDtypeStruct((count, rows // SIDE, head), jnp.bfloat16),
+            jax.ShapeDtypeStruct((count, 2, 8, 128), jnp.float32),
+        ),
+        in_specs=[anywhere] * 8,
+        out_specs=[vmem, vmem],
         scratch_shapes=[
+            pltpu.VMEM((SIDE * rows, head), jnp.bfloat16),
+            pltpu.VMEM((SIDE, rows, head), jnp.bfloat16),
+            pltpu.VMEM((SIDE, rows, head), jnp.bfloat16),
+            pltpu.VMEM((SIDE,) + bias_rows.shape, jnp.bfloat16),
             pltpu.VMEM((rows, head), jnp.float32),
-            pltpu.VMEM((rows, head), jnp.float32),
+            pltpu.VMEM((rows, 128), jnp.float32),
+            pltpu.SemaphoreType.DMA((3, SIDE)),
+            pltpu.SemaphoreType.DMA((count,)),
         ],
         compiler_params=pltpu.CompilerParams(vmem_limit_bytes=48 * 2**20),
         cost_estimate=pl.CostEstimate(
-            flops=16 * 6 * rows * rows * head, bytes_accessed=9 * 2**20, transcendentals=0
+            flops=14 * 6 * rows * rows * head, bytes_accessed=4 * 2**20, transcendentals=0
         ),
         name="attention",
-    )(queries, kv_all)
+    )(queries, keys, values, bias_rows, q_parts, k_parts, v_parts, b_parts)
+
+
+def deliver_kernel(o_ref, g_ref, os_ref, gs_ref, send_sem, recv_sem):
+    me, z, y = position()
+    head = lax.axis_index("tp")
+    owner_rows = os_ref.shape[2]
+
+    def pieces(block, half):
+        src = o_ref.at[block, pl.ds(half * owner_rows, owner_rows)]
+        return ((src, os_ref), (g_ref.at[block, half], gs_ref))
+
+    def remote(block, half, part):
+        src, dst = pieces(block, half)[part]
+        return pltpu.make_async_remote_copy(
+            src_ref=src,
+            dst_ref=dst.at[head, z],
+            send_sem=send_sem.at[part, block, half],
+            recv_sem=recv_sem.at[part, head, z],
+            device_id={"sp": block, "tp": 2 * y + half},
+            device_id_type=pl.DeviceIdType.MESH,
+        )
+
+    def local_copy(block, half, part):
+        src, dst = pieces(block, half)[part]
+        return pltpu.make_async_copy(src, dst.at[head, z], recv_sem.at[part, head, z])
+
+    def is_me(block, half):
+        return (block == me) & (2 * y + half == head)
+
+    def send(block, carry):
+        for half in range(2):
+
+            @pl.when(is_me(block, half))
+            def _():
+                for part in range(2):
+                    local_copy(block, half, part).start()
+
+            @pl.when(jnp.logical_not(is_me(block, half)))
+            def _():
+                for part in range(2):
+                    remote(block, half, part).start()
+
+        return carry
+
+    lax.fori_loop(z * SIDE, SIDE * SIDE, send, 0)
+
+    def take(group, carry):
+        for h in range(os_ref.shape[0]):
+            for part in range(2):
+                dst = (os_ref, gs_ref)[part].at[h, group]
+                pltpu.make_async_copy(dst, dst, recv_sem.at[part, h, group]).wait()
+        return carry
+
+    lax.fori_loop(0, z + 1, take, 0)
+
+    def sent(block, carry):
+        for half in range(2):
+
+            @pl.when(jnp.logical_not(is_me(block, half)))
+            def _():
+                for part in range(2):
+                    remote(block, half, part).wait_send()
+
+        return carry
+
+    lax.fori_loop(z * SIDE, SIDE * SIDE, sent, 0)
+
+
+def deliver(outs, logs, heads):
+    count, quarter, head = outs.shape
+    vmem = pl.BlockSpec(memory_space=pltpu.VMEM)
+    return pl.pallas_call(
+        deliver_kernel,
+        out_shape=(
+            jax.ShapeDtypeStruct((heads, SIDE, quarter // 2, head), jnp.bfloat16),
+            jax.ShapeDtypeStruct((heads, SIDE, 8, 128), jnp.float32),
+        ),
+        in_specs=[vmem, vmem],
+        out_specs=[vmem, vmem],
+        scratch_shapes=[
+            pltpu.SemaphoreType.DMA((2, count, 2)),
+            pltpu.SemaphoreType.DMA((2, heads, SIDE)),
+        ],
+        compiler_params=pltpu.CompilerParams(has_side_effects=True),
+        cost_estimate=pl.CostEstimate(flops=5 * 10**9, bytes_accessed=4 * 2**20, transcendentals=0),
+        name="deliver",
+    )(outs, logs)
+
+
+def combine(parts, logs):
+    group = lax.axis_index("sp") // SIDE
+    valid = jnp.arange(SIDE) <= group
+    left = jnp.where(valid[None, :, None], logs[:, :, 0, :], 0.0)
+    later = jnp.flip(jnp.cumsum(jnp.flip(left, 1), axis=1), 1) - left
+    weight = jnp.where(valid[None, :, None], jnp.exp2(-later), 0.0)
+    terms = jnp.where(valid[None, :, None, None], parts.astype(jnp.float32), 0.0)
+    total = jnp.sum(terms * weight[..., None], axis=1)
+    return total.transpose(1, 0, 2).reshape(total.shape[1], -1).astype(jnp.bfloat16)
 
 
 def local(
@@ -116,19 +374,15 @@
     rows_here = queries.shape[0]
     model_width = residual.shape[1]
     bias_rows = stick_bias.reshape(rows_here // CHUNK, CHUNK)
-    kv = jnp.concatenate(
-        [
-            jnp.concatenate([keys, values], axis=1),
-            jnp.pad(bias_rows, ((0, PAD - bias_rows.shape[0]), (0, 0))),
-        ],
-        axis=0,
-    )
-    kv_all = lax.all_gather(kv, "sp", axis=0, tiled=True)
-    whole_gate = lax.all_gather(gate_weight, "sp", axis=0, tiled=True)
-    whole_value = lax.all_gather(value_weight, "sp", axis=0, tiled=True)
-    whole_down = lax.all_gather(down_weight, "sp", axis=0, tiled=True)
-    attended = attention(queries, kv_all)
-    row_heads = lax.all_to_all(attended, "tp", split_axis=0, concat_axis=1, tiled=True)
+    bias_rows = jnp.pad(bias_rows, ((0, PAD - bias_rows.shape[0]), (0, 0)))
+    units = gate_weight.shape[1]
+    shared = exchange(queries, keys, values, bias_rows)
+    weights = jnp.concatenate([gate_weight, value_weight, down_weight], axis=1)
+    weights, shared = lax.optimization_barrier((weights, shared))
+    whole = lax.all_gather(weights, "sp", axis=0, tiled=True)
+    whole_gate, whole_value, whole_down = (whole[:, k * units : (k + 1) * units] for k in range(3))
+    outs, logs = attention(queries, keys, values, bias_rows, *shared)
+    row_heads = combine(*deliver(outs, logs, lax.axis_size("tp")))
     projected = jnp.dot(row_heads, out_weight, preferred_element_type=jnp.float32)
     middle_f = (residual.astype(jnp.float32) + projected).astype(jnp.bfloat16).astype(jnp.float32)
     normed = (

time: 345 us -> 376 us (1.090)
  Pallas kernels: 14.7 us -> 140 us
  waiting for transfers between devices: 252 us -> 170 us
  blocking collectives: 10.7 us -> 0 us
  local copies, waits for them, and re-layouts: 1.47 us -> 8.19 us
  matrix products: 31.2 us -> 25 us
    pallas_call x1 -> x3, Pallas kernels: 14.7 us -> 140 us  [the longest x1 51.1 us: exchange(): pl.pallas_call(exchange_kernel, out_shape=(jax.ShapeDtypeStruct((count, r...]
    all_gather x4 -> x1, waiting for transfers between devices: 172 us -> 81.5 us  [local(): whole = lax.all_gather(weights, 'sp', axis=0, tiled=True)]
    all_to_all x1 -> x0, blocking collectives: 10.7 us -> none  [local(): lax.all_to_all(attended, 'tp', split_axis=0, concat_axis=1, tiled=True)]
    all_gather x1, waiting for transfers between devices: 41.6 us -> 48.3 us  [local(): piece = lax.all_gather(normed, 'tp', axis=0, tiled=True)]
    unnamed x10 -> x30, local copies, waits for them, and re-layouts: 0.96 us -> 6.1 us
    dot_general x1, matrix products: 15.7 us -> 10.6 us  [local(): lax.dot_general(hidden, whole_down, NT, preferred_element_type=jnp.float32)]
  transfers between devices with their start and end apart: 8 -> 5, of which waited for: 7 -> 4; matrix products, arithmetic and copies ran while one was open for 6% -> 2% of each run, Pallas kernels for 4% -> 0%
where the time goes in v2:
time: 376 us; the launch traced here: 372 us
  waiting for transfers between devices  170 us (45%)
  Pallas kernels  140 us (37%)
  matrix products  25 us (7%)
  between operations  13.3 us (4%)
  other arithmetic  9.21 us (2%)
  local copies, waits for them, and re-layouts  8.19 us (2%)
  starting transfers between devices  5.81 us (2%)
    all_gather x1, waiting for transfers between devices, local(): whole = lax.all_gather(weights, 'sp', axis=0, tiled=True)  81.5 us
    pallas_call x1, Pallas kernels, exchange(): pl.pallas_call(exchange_kernel, out_shape=(jax.ShapeDtypeStruct((count, r...  51.1 us
    all_gather x1, waiting for transfers between devices, local(): piece = lax.all_gather(normed, 'tp', axis=0, tiled=True)  48.3 us
    pallas_call x1, Pallas kernels, deliver(): pl.pallas_call(deliver_kernel, out_shape=(jax.ShapeDtypeStruct((heads, SI...  44.9 us
    pallas_call x1, Pallas kernels, attention(): pl.pallas_call(attention_kernel, out_shape=(jax.ShapeDtypeStruct((count,...  44.4 us
    reduce_scatter x1, waiting for transfers between devices, local(): lax.psum_scatter(down.astype(jnp.bfloat16), 'tp', scatter_dimension=0, ti...  35.1 us
    dot_general x1, matrix products, local(): lax.dot_general(hidden, whole_down, NT, preferred_element_type=jnp.float32)  10.6 us
  transfers between devices with their start and end apart: 5, of which 4 were waited for; matrix products, arithmetic and copies ran while one was open for 2% of the time, Pallas kernels for 0%

profile of v2, /device:TPU:26, one launch (start us, length us, event | category | flops | bytes accessed | tf_op | source)
XLA Modules:
  0.0 371.7 jit_solution(1789530845712237865)
XLA Ops:
  6.5 0.7 reduce
  7.3 0.6 pad.4.b_ref
  7.9 2.0 pad_maximum_fusion
  9.9 51.1 %exchange.1 = (bf16[16,256,128]{2,1,0:T(8,128)(2,1)}, bf16[4,1024,128]{2,1,0:T(8,128)(2,1)}, bf16[4,1024,128]{2,1,0:T(8,128)(2,1)}, bf16[4,16,256]{2,1,0:T(8,128)(2,1)}) custom-call(bf16[1024,128]{1,0:T(8,128)(2,1)} %q_ref.3, bf16[1024,128]{1,0:T(8,128)(2,1)} %k_ref.3, bf16[1024,128]{1,0:T(8,128)(2,1)} %v_ref.3, bf16[16,256]{1,0:T(8,128)(2,1)} %pad.4.b_ref), custom_call_target="tpu_custom_call" | custom-call | flops 10000000000 | bytes 4194304 | tf_op jit(solution)/shard_map/exchange/pallas_call | solution.py:107
  61.0 1.2 copy-done.5
  62.2 1.2 copy-done.6
  63.5 1.2 copy-done.7
  64.7 0.8 copy-done.9
  65.4 44.4 %attention.1 = (bf16[16,256,128]{2,1,0:T(8,128)(2,1)S(1)}, f32[16,2,8,128]{3,2,1,0:T(8,128)S(1)}) custom-call(bf16[1024,128]{1,0:T(8,128)(2,1)S(1)} %copy-done.1, bf16[1024,128]{1,0:T(8,128)(2,1)S(1)} %copy-done.2, bf16[1024,128]{1,0:T(8,128)(2,1)S(1)} %copy-done.3, bf16[16,256]{1,0:T(8,128)(2,1)S(1)} %copy-done, bf16[16,256,128]{2,1,0:T(8,128)(2,1)S(1)} %copy-done.5, ...), custom_call_target="tpu_custom_call" | custom-call | flops 11274289152 | bytes 4194304 | tf_op jit(solution)/shard_map/attention/pallas_call | solution.py:236
  109.8 1.0 copy-done.4
  110.8 0.7 copy-done.8
  111.5 44.9 %deliver.1 = (bf16[8,4,128,128]{3,2,1,0:T(8,128)(2,1)}, f32[8,4,8,128]{3,2,1,0:T(8,128)}) custom-call(bf16[16,256,128]{2,1,0:T(8,128)(2,1)} %copy-done.4, f32[16,2,8,128]{3,2,1,0:T(8,128)} %copy-done.8), custom_call_target="tpu_custom_call" | custom-call | flops 5000000000 | bytes 4194304 | tf_op jit(solution)/shard_map/deliver/pallas_call | solution.py:331
  156.4 0.9 slice.54
  157.6 1.8 multiply_reduce_fusion
  159.4 0.2 copy.13
  159.6 3.0 multiply_reduce_fusion.1
  162.7 1.0 multiply_convert_fusion
  163.7 0.7 all-gather.5.cloned.1.call-update
  164.5 48.3 %all-gather.3.cloned.1.call-done = bf16[1024,2048]{1,0:T(8,128)(2,1)} async-done(((bf16[128,2048]{1,0:T(8,128)(2,1)}), bf16[1024,2048]{1,0:T(8,128)(2,1)}) %all-gather.3.cloned.1.call-update) | async-done | bytes 4194320 | tf_op jit(solution)/shard_map/all_gather | solution.py:393
  212.8 81.5 %all-gather.5.cloned.1.call-done = bf16[2048,2112]{0,1:T(8,128)(2,1)} async-done(((bf16[128,2112]{0,1:T(8,128)(2,1)}), bf16[2048,2112]{0,1:T(8,128)(2,1)}) %all-gather.5.cloned.1.call-update) | async-done | bytes 8650768 | tf_op jit(solution)/shard_map/all_gather | solution.py:382
  294.3 6.4 %fusion.13 = bf16[1024,704]{0,1:T(8,128)(2,1)S(1)} fusion(bf16[1024,2048]{1,0:T(8,128)(2,1)} %all-gather.3.cloned.1.call-done, bf16[2048,2112]{0,1:T(8,128)(2,1)} %all-gather.5.cloned.1.call-done), kind=kOutput, calls=%fused_computation.22 | convolution fusion | flops 2953510912 | bytes 8519680 | tf_op jit(solution)/shard_map/dot_general | solution.py:394
  300.7 0.1 slice.73
  300.8 3.4 collective-permute-start
  304.2 5.0 %fusion.16 = bf16[1024,704]{0,1:T(8,128)(2,1)S(1)} fusion(bf16[1024,2048]{1,0:T(8,128)(2,1)S(1)} %copy-done.14, bf16[2048,2112]{0,1:T(8,128)(2,1)} %all-gather.5.cloned.1.call-done), kind=kOutput, calls=%fused_computation.23 | convolution fusion | flops 2953510912 | bytes 8519680 | tf_op jit(solution)/shard_map/dot_general | solution.py:395
  309.2 0.1 slice.78
  309.4 2.4 collective-permute-start.1
  311.7 0.8 maximum_convert_fusion
  312.5 4.2 %collective-permute-done.1 = bf16[2,704]{0,1:T(8,128)(2,1)S(1)} collective-permute-done((bf16[2,704]{0,1:T(8,128)(2,1)S(1)}, bf16[2,704]{0,1:T(8,128)(2,1)S(1)}, u32[]{:S(2)}, u32[]{:S(2)}) %collective-permute-start.1) | collective-permute-done | bytes 2848 | tf_op jit(solution)/shard_map/ppermute | solution.py:19
  316.7 0.8 maximum_convert_fusion.1
  317.5 10.6 %convolution_convert_fusion = bf16[1024,2048]{1,0:T(8,128)(2,1)} fusion(bf16[2048,2112]{0,1:T(8,128)(2,1)} %all-gather.5.cloned.1.call-done, f32[1026,704]{0,1:T(8,128)S(1)} %maximum_convert_fusion.1, f32[1026,704]{0,1:T(8,128)S(1)} %maximum_convert_fusion, f32[704]{0:T(1024)S(1)} %get-tuple-element.35, f32[704]{0:T(1024)S(1)} %get-tuple-element.36, ...), kind=kOutput, calls=%fused_computation | convolution fusion | flops 2966421504 | bytes 24403968 | tf_op jit(solution)/shard_map/dot_general | solution.py:406
  328.1 35.1 %reduce-scatter.2.cloned.1.call-done = bf16[128,2048]{1,0:T(8,128)(2,1)} async-done(((bf16[1024,2048]{1,0:T(8,128)(2,1)}), bf16[128,2048]{1,0:T(8,128)(2,1)}) %reduce-scatter.2.cloned.1.call-update) | async-done | bytes 524304 | tf_op jit(solution)/shard_map/reduce_scatter | solution.py:407
  363.2 1.9 add_convert_fusion
  (39 shorter events, 0.5 us)
Async XLA Ops:
  6.5 206.3 %all-gather.3.cloned.1.call-start = ((), (), s32[]{:S(2)}) async-start(), calls=%async_computation.1 | async-start | bytes 4718592 | tf_op jit(solution)/shard_map/all_gather | solution.py:393
  9.8 51.1 %copy-start = (bf16[16,256]{1,0:T(8,128)(2,1)S(1)}, bf16[16,256]{1,0:T(8,128)(2,1)}, u32[]{:S(2)}) copy-start(bf16[16,256]{1,0:T(8,128)(2,1)} %pad.4.b_ref) | copy-start | bytes 24580
  9.9 51.1 %copy-start.1 = (bf16[1024,128]{1,0:T(8,128)(2,1)S(1)}, bf16[1024,128]{1,0:T(8,128)(2,1)}, u32[]{:S(2)}) copy-start(bf16[1024,128]{1,0:T(8,128)(2,1)} %q_ref.3) | copy-start | bytes 786436
  9.9 51.1 %copy-start.2 = (bf16[1024,128]{1,0:T(8,128)(2,1)S(1)}, bf16[1024,128]{1,0:T(8,128)(2,1)}, u32[]{:S(2)}) copy-start(bf16[1024,128]{1,0:T(8,128)(2,1)} %k_ref.3) | copy-start | bytes 786436
  9.9 51.1 %copy-start.3 = (bf16[1024,128]{1,0:T(8,128)(2,1)S(1)}, bf16[1024,128]{1,0:T(8,128)(2,1)}, u32[]{:S(2)}) copy-start(bf16[1024,128]{1,0:T(8,128)(2,1)} %v_ref.3) | copy-start | bytes 786436
  61.0 1.2 copy-start.5
  62.2 1.2 copy-start.6
  63.5 1.2 copy-start.7
  64.7 0.8 copy-start.9
  109.8 1.0 copy-start.4
  110.8 0.7 copy-start.8
  111.5 48.1 %copy-start.10 = (bf16[128,2048]{1,0:T(8,128)(2,1)S(1)}, bf16[128,2048]{1,0:T(8,128)(2,1)}, u32[]{:S(2)}) copy-start(bf16[128,2048]{1,0:T(8,128)(2,1)} %param.16) | copy-start | bytes 1572868
  159.6 3.1 copy-start.11
  159.6 4.8 %copy-start.12 = (f32[3,704]{1,0:T(4,128)S(1)}, f32[3,704]{1,0:T(4,128)}, u32[]{:S(2)}) copy-start(f32[3,704]{1,0:T(4,128)} %param.23) | copy-start | bytes 25348
  159.6 4.8 %copy-start.13 = (f32[3,704]{1,0:T(4,128)S(1)}, f32[3,704]{1,0:T(4,128)}, u32[]{:S(2)}) copy-start(f32[3,704]{1,0:T(4,128)} %param.22) | copy-start | bytes 25348
  163.6 130.7 %all-gather.5.cloned.1.call-start = ((), (), s32[]{:S(2)}) async-start(), calls=%async_computation.2 | async-start | bytes 9191424 | tf_op jit(solution)/shard_map/all_gather | solution.py:382
  164.4 198.8 %reduce-scatter.2.cloned.1.call-start = ((), (), s32[]{:S(2)}) async-start(), calls=%async_computation.3 | async-start | bytes 4718592 | tf_op jit(solution)/shard_map/reduce_scatter | solution.py:407
  294.3 9.9 %copy-start.14 = (bf16[1024,2048]{1,0:T(8,128)(2,1)S(1)}, bf16[1024,2048]{1,0:T(8,128)(2,1)}, u32[]{:S(2)}) copy-start(bf16[1024,2048]{1,0:T(8,128)(2,1)} %all-gather.3.cloned.1.call-done) | copy-start | bytes 12582916
  300.8 10.9 %collective-permute-start = (bf16[2,704]{0,1:T(8,128)(2,1)S(1)}, bf16[2,704]{0,1:T(8,128)(2,1)S(1)}, u32[]{:S(2)}, u32[]{:S(2)}) collective-permute-start(bf16[2,704]{0,1:T(8,128)(2,1)S(1)} %slice.73), channel_id=1, source_target_pairs={{0,8},{8,16},{16,24},{24,32},{32,40},{40,48},{48,56},{56,64},{64,7... | collective-permute-start | bytes 8456 | tf_op jit(solution)/shard_map/ppermute | solution.py:19
  309.4 7.4 %collective-permute-start.1 = (bf16[2,704]{0,1:T(8,128)(2,1)S(1)}, bf16[2,704]{0,1:T(8,128)(2,1)S(1)}, u32[]{:S(2)}, u32[]{:S(2)}) collective-permute-start(bf16[2,704]{0,1:T(8,128)(2,1)S(1)} %slice.78), channel_id=1, source_target_pairs={{0,8},{8,16},{16,24},{24,32},{32,40},{40,48},{48,56},{56,64},{64,7... | collective-permute-start | bytes 8456 | tf_op jit(solution)/shard_map/ppermute | solution.py:19
Sparse Core Ops, SparseCore 0:
  163.8 49.0 all-gather.2
  215.0 79.2 all-gather.4
  328.3 34.9 reduce-scatter.1

commit v3 on v2

--- a/solution.py
+++ b/solution.py
@@ -11,12 +11,7 @@
 CHUNK = 256
 PAD = 16
 SIDE = 4
-
-
-def from_behind(block, axis, distance):
-    devices = range(lax.axis_size(axis))
-    route = [(i - distance, i) for i in devices if i - distance in devices]
-    return lax.ppermute(block, axis, route)
+RIM = 16
 
 
 def tri_matrix():
@@ -43,67 +38,128 @@
     return me, me // SIDE, me % SIDE
 
 
-def exchange_kernel(q_ref, k_ref, v_ref, b_ref, qs_ref, ks_ref, vs_ref, bs_ref, send_sem, recv_sem, q_send, q_recv):
+def owners_of(y):
+    core = lax.axis_index("tp") % 2
+    return 2 * ((y + core) % SIDE), 2 * ((y + core + 2) % SIDE) + 1
+
+
+def remote_copy(src, dst, send_sem, recv_sem, **where):
+    return pltpu.make_async_remote_copy(
+        src_ref=src,
+        dst_ref=dst,
+        send_sem=send_sem,
+        recv_sem=recv_sem,
+        device_id=where,
+        device_id_type=pl.DeviceIdType.MESH,
+    )
+
+
+def arrived(dst, sem):
+    pltpu.make_async_copy(dst, dst, sem).wait()
+
+
+def exchange_kernel(
+    q_ref, k_ref, v_ref, b_ref, qs_ref, ks_ref, vs_ref, bs_ref,
+    send_sem, recv_sem, bias_send, bias_recv, q_send, q_recv, own_sem, z_send, z_recv,
+):
     me, z, y = position()
-    quarter = q_ref.shape[0] // SIDE
-
-    def copy_row(d, part):
-        src, dst = ((k_ref, ks_ref), (v_ref, vs_ref), (b_ref, bs_ref))[part]
-        return pltpu.make_async_remote_copy(
-            src_ref=src,
-            dst_ref=dst.at[y],
-            send_sem=send_sem.at[part, d],
-            recv_sem=recv_sem.at[part, y],
-            device_id={"sp": z * SIDE + (y + d) % SIDE},
-            device_id_type=pl.DeviceIdType.MESH,
-        )
-
-    def copy_query(dz, dy):
-        to_y = (y + dy) % SIDE
-        return pltpu.make_async_remote_copy(
-            src_ref=q_ref.at[pl.ds(pl.multiple_of(to_y * quarter, quarter), quarter)],
-            dst_ref=qs_ref.at[me],
-            send_sem=q_send.at[dz, dy],
-            recv_sem=q_recv.at[me],
-            device_id={"sp": (z - dz) * SIDE + to_y},
-            device_id_type=pl.DeviceIdType.MESH,
-        )
-
-    def for_queries(act):
-        for dz in range(SIDE):
-            for dy in range(SIDE):
-                if dz or dy:
-
-                    @pl.when(z >= dz)
-                    def _():
-                        act(copy_query(dz, dy))
-
+    share = q_ref.shape[0] // (2 * SIDE)
+    right = (y + 1) % SIDE
+    left = (y + 3) % SIDE
+    across = (y + 2) % SIDE
+    row = z * SIDE
+
+    def hop(part, src_slot, to, lane):
+        src = (k_ref, v_ref)[part] if src_slot is None else (ks_ref, vs_ref)[part].at[src_slot]
+        slot = y if src_slot is None else src_slot
+        return remote_copy(
+            src,
+            (ks_ref, vs_ref)[part].at[slot],
+            send_sem.at[part, lane],
+            recv_sem.at[part, slot],
+            sp=row + to,
+        )
+
+    def bias_hop(d):
+        return remote_copy(
+            b_ref, bs_ref.at[y], bias_send.at[d], bias_recv.at[y], sp=row + (y + d) % SIDE
+        )
+
+    def q_piece(of, half, act_remote, d):
+        src = q_ref.at[pl.ds(pl.multiple_of(owners_of(of)[half] * share, share), share)]
+        dst = qs_ref.at[me, pl.ds(half * share, share)]
+        if act_remote:
+            return remote_copy(
+                src, dst, q_send.at[d, half], q_recv.at[me % SIDE, half], sp=row + of
+            )
+        return pltpu.make_async_copy(src, dst, own_sem.at[half])
+
+    for half in range(2):
+        q_piece(y, half, False, 0).start()
     for d in (2, 1, 3):
-        for part in range(3):
-            copy_row(d, part).start()
-    for_queries(lambda copy: copy.start())
-    for d in (1, 3, 2):
+        for half in range(2):
+            q_piece((y + d) % SIDE, half, True, d).start()
+        bias_hop(d).start()
+    hop(0, None, right, 0).start()
+    hop(1, None, left, 0).start()
+    hop(1, None, right, 1).start()
+    hop(0, None, left, 1).start()
+
+    for half in range(2):
+        q_piece(y, half, False, 0).wait()
+        for d in (1, 2, 3):
+            slot = (y + d) % SIDE
+            arrived(qs_ref.at[row + slot, pl.ds(half * share, share)], q_recv.at[slot, half])
+
+    def down_row(dz):
+        ours = qs_ref.at[pl.ds(pl.multiple_of(row, SIDE), SIDE)]
+        return remote_copy(ours, ours, z_send.at[dz], z_recv.at[z], sp=row - dz * SIDE + y)
+
+    for dz in (2, 3, 1):
+
+        @pl.when(z >= dz)
+        def _():
+            down_row(dz).start()
+
+    arrived(ks_ref.at[left], recv_sem.at[0, left])
+    hop(0, left, right, 2).start()
+    arrived(vs_ref.at[right], recv_sem.at[1, right])
+    hop(1, right, left, 2).start()
+    arrived(vs_ref.at[left], recv_sem.at[1, left])
+    arrived(ks_ref.at[right], recv_sem.at[0, right])
+    arrived(ks_ref.at[across], recv_sem.at[0, across])
+    arrived(vs_ref.at[across], recv_sem.at[1, across])
+    for d in (1, 2, 3):
         slot = (y + d) % SIDE
-        for part in range(3):
-            dst = (ks_ref, vs_ref, bs_ref)[part].at[slot]
-            pltpu.make_async_copy(dst, dst, recv_sem.at[part, slot]).wait()
-    for slot in range(SIDE * SIDE):
-
-        @pl.when((slot // SIDE >= z) & (slot != me))
+        arrived(bs_ref.at[slot], bias_recv.at[slot])
+    for other in range(1, SIDE):
+
+        @pl.when(z < other)
         def _():
-            dst = qs_ref.at[slot]
-            pltpu.make_async_copy(dst, dst, q_recv.at[slot]).wait()
-
+            arrived(qs_ref.at[pl.ds(other * SIDE, SIDE)], z_recv.at[other])
+
+    hop(0, None, right, 0).wait_send()
+    hop(1, None, left, 0).wait_send()
+    hop(1, None, right, 1).wait_send()
+    hop(0, None, left, 1).wait_send()
+    hop(0, left, right, 2).wait_send()
+    hop(1, right, left, 2).wait_send()
     for d in (1, 2, 3):
-        for part in range(3):
-            copy_row(d, part).wait_send()
-    for_queries(lambda copy: copy.wait_send())
+        bias_hop(d).wait_send()
+        for half in range(2):
+            q_piece((y + d) % SIDE, half, True, d).wait_send()
+    for dz in (1, 2, 3):
+
+        @pl.when(z >= dz)
+        def _():
+            down_row(dz).wait_send()
 
 
 def exchange(queries, keys, values, bias_rows):
     rows, head = queries.shape
     anywhere = pl.BlockSpec(memory_space=pl.ANY)
     count = SIDE * SIDE
+    dma = pltpu.SemaphoreType.DMA
     return pl.pallas_call(
         exchange_kernel,
         out_shape=(
@@ -115,10 +171,8 @@
         in_specs=[anywhere] * 4,
         out_specs=[anywhere] * 4,
         scratch_shapes=[
-            pltpu.SemaphoreType.DMA((3, SIDE)),
-            pltpu.SemaphoreType.DMA((3, SIDE)),
-            pltpu.SemaphoreType.DMA((SIDE, SIDE)),
-            pltpu.SemaphoreType.DMA((count,)),
+            dma((2, 3)), dma((2, SIDE)), dma((SIDE,)), dma((SIDE,)), dma((SIDE, 2)),
+            dma((SIDE, 2)), dma((2,)), dma((SIDE,)), dma((SIDE,)),
         ],
         compiler_params=pltpu.CompilerParams(has_side_effects=True),
         cost_estimate=pl.CostEstimate(flops=10**10, bytes_accessed=4 * 2**20, transcendentals=0),
@@ -127,13 +181,14 @@
 
 
 def attention_kernel(
-    q_ref, k_ref, v_ref, b_ref, qs_ref, ks_ref, vs_ref, bs_ref,
+    k_ref, v_ref, b_ref, qs_ref, ks_ref, vs_ref, bs_ref,
     o_ref, g_ref, q_all, k_all, v_all, b_all, acc_ref, gone_ref, kv_sem, q_sem,
 ):
-    rows, head = q_ref.shape
+    rows, head = k_ref.shape
     quarter = rows // SIDE
     chunks = rows // CHUNK
-    me, z, y = position()
+    _, z, y = position()
+    first, second = (owner * (quarter // 2) for owner in owners_of(y))
     tri, _ = tri_matrix()
     own = (k_ref, v_ref, b_ref)
     others = (ks_ref, vs_ref, bs_ref)
@@ -155,12 +210,7 @@
     for slot in range(SIDE * SIDE):
         dst = q_all.at[pl.ds(slot * quarter, quarter)]
 
-        @pl.when(slot == me)
-        def _():
-            src = q_ref.at[pl.ds(pl.multiple_of(y * quarter, quarter), quarter)]
-            pltpu.make_async_copy(src, dst, q_sem.at[slot]).start()
-
-        @pl.when((slot // SIDE >= z) & (slot != me))
+        @pl.when(slot // SIDE >= z)
         def _():
             pltpu.make_async_copy(qs_ref.at[slot], dst, q_sem.at[slot]).start()
 
@@ -196,9 +246,10 @@
         gone = gone_ref[low:, 0:1]
         row = lax.broadcasted_iota(jnp.int32, (size, CHUNK), 0)
         col = lax.broadcasted_iota(jnp.int32, (size, CHUNK), 1)
+        place = row + jnp.where(row < quarter // 2, first, second - quarter // 2)
         for c in range(chunks - 1, -1, -1):
             at = slice(c * CHUNK, (c + 1) * CHUNK)
-            mask = (row >= quarter) | (col - row < y * quarter - c * CHUNK)
+            mask = (row >= quarter) | (col + c * CHUNK < place)
             gone, acc = visit_chunk(
                 q, k_all[j, at, :], v_all[j, at, :], bias[c : c + 1, :], tri, gone, acc, mask
             )
@@ -228,8 +279,8 @@
     lax.fori_loop(z + 1, SIDE, group_step, 0)
 
 
-def attention(queries, keys, values, bias_rows, q_parts, k_parts, v_parts, b_parts):
-    rows, head = queries.shape
+def attention(keys, values, bias_rows, q_parts, k_parts, v_parts, b_parts):
+    rows, head = keys.shape
     anywhere = pl.BlockSpec(memory_space=pl.ANY)
     vmem = pl.BlockSpec(memory_space=pltpu.VMEM)
     count = SIDE * SIDE
@@ -239,7 +290,7 @@
             jax.ShapeDtypeStruct((count, rows // SIDE, head), jnp.bfloat16),
             jax.ShapeDtypeStruct((count, 2, 8, 128), jnp.float32),
         ),
-        in_specs=[anywhere] * 8,
+        in_specs=[anywhere] * 7,
         out_specs=[vmem, vmem],
         scratch_shapes=[
             pltpu.VMEM((SIDE * rows, head), jnp.bfloat16),
@@ -256,13 +307,14 @@
             flops=14 * 6 * rows * rows * head, bytes_accessed=4 * 2**20, transcendentals=0
         ),
         name="attention",
-    )(queries, keys, values, bias_rows, q_parts, k_parts, v_parts, b_parts)
+    )(keys, values, bias_rows, q_parts, k_parts, v_parts, b_parts)
 
 
 def deliver_kernel(o_ref, g_ref, os_ref, gs_ref, send_sem, recv_sem):
     me, z, y = position()
     head = lax.axis_index("tp")
     owner_rows = os_ref.shape[2]
+    owners = owners_of(y)
 
     def pieces(block, half):
         src = o_ref.at[block, pl.ds(half * owner_rows, owner_rows)]
@@ -275,7 +327,7 @@
             dst_ref=dst.at[head, z],
             send_sem=send_sem.at[part, block, half],
             recv_sem=recv_sem.at[part, head, z],
-            device_id={"sp": block, "tp": 2 * y + half},
+            device_id={"sp": block, "tp": owners[half]},
             device_id_type=pl.DeviceIdType.MESH,
         )
 
@@ -284,7 +336,7 @@
         return pltpu.make_async_copy(src, dst.at[head, z], recv_sem.at[part, head, z])
 
     def is_me(block, half):
-        return (block == me) & (2 * y + half == head)
+        return (block == me) & (owners[half] == head)
 
     def send(block, carry):
         for half in range(2):
@@ -357,6 +409,292 @@
     return total.transpose(1, 0, 2).reshape(total.shape[1], -1).astype(jnp.bfloat16)
 
 
+def place_of():
+    me = lax.axis_index("tp")
+    return me // 2, me % 2
+
+
+def gather_kernel(n_ref, all_ref, rim_ref, ring_send, ring_recv, twin_send, twin_recv, rim_send, rim_recv, own_sem):
+    x, core = place_of()
+    block = lax.axis_index("sp")
+    rows = n_ref.shape[0]
+    part = rows // 2
+    right = (x + 1) % SIDE
+    left = (x + 3) % SIDE
+    across = (x + 2) % SIDE
+
+    def spot(chip, half, of_core=None):
+        of_core = core if of_core is None else of_core
+        return all_ref.at[2 * chip + of_core, pl.ds(half * part, part)]
+
+    def ring(chip, half, to, lane):
+        src = n_ref.at[pl.ds(half * part, part)] if chip is None else spot(chip, half)
+        chip = x if chip is None else chip
+        return remote_copy(
+            src, spot(chip, half), ring_send.at[lane, half], ring_recv.at[chip, half], tp=2 * to + core
+        )
+
+    def twin(chip, half):
+        src = n_ref.at[pl.ds(half * part, part)] if chip is None else spot(chip, half)
+        chip = x if chip is None else chip
+        return remote_copy(
+            src, spot(chip, half), twin_send.at[chip, half], twin_recv.at[chip, half], tp=2 * x + 1 - core
+        )
+
+    def rim(to):
+        return remote_copy(
+            n_ref.at[pl.ds(rows - RIM, RIM)], rim_ref, rim_send.at[to], rim_recv, sp=block + 1, tp=to
+        )
+
+    last = (x == SIDE - 1) & (core == 1) & (block < SIDE * SIDE - 1)
+    own = pltpu.make_async_copy(n_ref, all_ref.at[2 * x + core], own_sem)
+    ring(None, 0, right, 0).start()
+    ring(None, 1, left, 1).start()
+    ring(None, 1, right, 0).start()
+    ring(None, 0, left, 1).start()
+    own.start()
+    for half in range(2):
+        twin(None, half).start()
+
+    @pl.when(last)
+    def _():
+        for to in range(2 * SIDE):
+            rim(to).start()
+
+    arrived(spot(left, 0), ring_recv.at[left, 0])
+    ring(left, 0, right, 2).start()
+    twin(left, 0).start()
+    arrived(spot(right, 1), ring_recv.at[right, 1])
+    ring(right, 1, left, 2).start()
+    twin(right, 1).start()
+    for chip, half in ((left, 1), (right, 0), (across, 0), (across, 1)):
+        arrived(spot(chip, half), ring_recv.at[chip, half])
+        twin(chip, half).start()
+    own.wait()
+    for chip in range(SIDE):
+        for half in range(2):
+            arrived(spot(chip, half, 1 - core), twin_recv.at[chip, half])
+
+    @pl.when(block > 0)
+    def _():
+        arrived(rim_ref, rim_recv)
+
+    for half in range(2):
+        ring(None, half, right, 0).wait_send()
+        ring(None, half, left, 1).wait_send()
+        twin(None, half).wait_send()
+        for chip in (left, right, across):
+            twin(chip, half).wait_send()
+    ring(left, 0, right, 2).wait_send()
+    ring(right, 1, left, 2).wait_send()
+
+    @pl.when(last)
+    def _():
+        for to in range(2 * SIDE):
+            rim(to).wait_send()
+
+
+def gather_rows(normed):
+    rows, width = normed.shape
+    vmem = pl.BlockSpec(memory_space=pltpu.VMEM)
+    dma = pltpu.SemaphoreType.DMA
+    return pl.pallas_call(
+        gather_kernel,
+        out_shape=(
+            jax.ShapeDtypeStruct((2 * SIDE, rows, width), jnp.bfloat16),
+            jax.ShapeDtypeStruct((RIM, width), jnp.bfloat16),
+        ),
+        in_specs=[vmem],
+        out_specs=[vmem, vmem],
+        scratch_shapes=[
+            dma((3, 2)), dma((SIDE, 2)), dma((SIDE, 2)), dma((SIDE, 2)), dma((2 * SIDE,)), dma(()), dma(()),
+        ],
+        compiler_params=pltpu.CompilerParams(has_side_effects=True, vmem_limit_bytes=24 * 2**20),
+        cost_estimate=pl.CostEstimate(flops=5 * 10**9, bytes_accessed=4 * 2**20, transcendentals=0),
+        name="gather_rows",
+    )(normed)
+
+
+def feed_forward_kernel(
+    x_ref, rim_ref, w_ref, cg_ref, cv_ref, out_ref, up_ref, down_ref, gate_ref, value_ref, w_sem
+):
+    blocks, rows, depth = x_ref.shape
+    units = down_ref.shape[0]
+    shards = w_ref.shape[0]
+    deep = depth // shards
+    tile = 2 * rows
+    first = lax.axis_index("sp") == 0
+
+    def weight_copies(k):
+        at = slice(k * deep, (k + 1) * deep)
+        return (
+            pltpu.make_async_copy(
+                w_ref.at[k, pl.ds(0, 2 * units)], up_ref.at[:, at], w_sem.at[0, k]
+            ),
+            pltpu.make_async_copy(
+                w_ref.at[k, pl.ds(2 * units, units)], down_ref.at[:, at], w_sem.at[1, k]
+            ),
+        )
+
+    for k in range(shards):
+        for copy in weight_copies(k):
+            copy.start()
+    for k in range(shards):
+        weight_copies(k)[0].wait()
+
+    def up(x, which):
+        w = up_ref[which * units : (which + 1) * units, :]
+        return lax.dot_general(x, w, NT, preferred_element_type=jnp.float32)
+
+    for which, ref in enumerate((gate_ref, value_ref)):
+        rim = up(rim_ref[...], which)
+        ref[0:RIM, :] = jnp.where(first, 0.0, rim)
+
+    def conv(ref, taps, start):
+        at = pl.multiple_of(start, tile)
+        window = ref[pl.ds(at, tile + RIM), :]
+        return (
+            taps[0:1, :] * window[RIM - 2 : RIM - 2 + tile]
+            + taps[1:2, :] * window[RIM - 1 : RIM - 1 + tile]
+            + taps[2:3, :] * window[RIM : RIM + tile]
+        )
+
+    for k in range(shards):
+        weight_copies(k)[1].wait()
+
+    @pl.loop(0, blocks // 2)
+    def _(t):
+        x = x_ref[pl.ds(t * 2, 2)].reshape(tile, depth)
+        start = t * tile
+        for which, ref in enumerate((gate_ref, value_ref)):
+            ref[pl.ds(pl.multiple_of(start + RIM, RIM), tile), :] = up(x, which)
+        gate = conv(gate_ref, cg_ref, start)
+        value = conv(value_ref, cv_ref, start)
+        hidden = (gate / (1.0 + jnp.exp(-gate)) * value).astype(jnp.bfloat16)
+        down = jnp.dot(hidden, down_ref[...], preferred_element_type=jnp.float32)
+        out_ref[pl.ds(t * 2, 2)] = down.astype(out_ref.dtype).reshape(2, rows, depth)
+
+
+def feed_forward(pieces, rim, whole, conv_gate, conv_value):
+    blocks, rows, depth = pieces.shape
+    units = conv_gate.shape[1]
+    vmem = pl.BlockSpec(memory_space=pltpu.VMEM)
+    return pl.pallas_call(
+        feed_forward_kernel,
+        out_shape=jax.ShapeDtypeStruct((blocks, rows, depth), jnp.bfloat16),
+        in_specs=[vmem, vmem, pl.BlockSpec(memory_space=pl.ANY), vmem, vmem],
+        out_specs=vmem,
+        scratch_shapes=[
+            pltpu.VMEM((2 * units, depth), jnp.bfloat16),
+            pltpu.VMEM((units, depth), jnp.bfloat16),
+            pltpu.VMEM((RIM + blocks * rows, units), jnp.float32),
+            pltpu.VMEM((RIM + blocks * rows, units), jnp.float32),
+            pltpu.SemaphoreType.DMA((2, whole.shape[0])),
+        ],
+        compiler_params=pltpu.CompilerParams(vmem_limit_bytes=56 * 2**20),
+        cost_estimate=pl.CostEstimate(flops=9 * 10**9, bytes_accessed=18 * 2**20, transcendentals=0),
+        name="feed_forward",
+    )(pieces, rim, whole, conv_gate, conv_value)
+
+
+def reduce_kernel(p_ref, m_ref, out_ref, twin_buf, sum_buf, relay_buf, ring_buf, twin_send, twin_recv, relay_send, relay_recv, ring_send, ring_recv):
+    x, core = place_of()
+    rows = p_ref.shape[1]
+    part = rows // 2
+    right = (x + 1) % SIDE
+    left = (x + 3) % SIDE
+    across = (x + 2) % SIDE
+    halves = (slice(0, part), slice(part, rows))
+
+    def twin(chip):
+        return remote_copy(
+            p_ref.at[2 * chip + 1 - core],
+            twin_buf.at[chip],
+            twin_send.at[chip],
+            twin_recv.at[chip],
+            tp=2 * x + 1 - core,
+        )
+
+    for chip in (across, right, left, x):
+        twin(chip).start()
+
+    def pair_sum(chip, half):
+        mine = p_ref[2 * chip + core, halves[half], :].astype(jnp.float32)
+        return mine + twin_buf[chip, halves[half], :].astype(jnp.float32)
+
+    def relay(side):
+        to = (right, left)[side]
+        return remote_copy(
+            sum_buf.at[0, halves[side]],
+            relay_buf.at[side],
+            relay_send.at[side],
+            relay_recv.at[side],
+            tp=2 * to + core,
+        )
+
+    def ring(side, half):
+        to = (right, left)[side]
+        return remote_copy(
+            sum_buf.at[1 + side, halves[half]],
+            ring_buf.at[side, halves[half]],
+            ring_send.at[side, half],
+            ring_recv.at[side, half],
+            tp=2 * to + core,
+        )
+
+    arrived(twin_buf.at[across], twin_recv.at[across])
+    for side in range(2):
+        sum_buf[0, halves[side], :] = pair_sum(across, side).astype(jnp.bfloat16)
+        relay(side).start()
+    for side in range(2):
+        to = (right, left)[side]
+        arrived(twin_buf.at[to], twin_recv.at[to])
+        half = 1 - side
+        sum_buf[1 + side, halves[half], :] = pair_sum(to, half).astype(jnp.bfloat16)
+        ring(side, half).start()
+    arrived(twin_buf.at[x], twin_recv.at[x])
+    for side in range(2):
+        to = (right, left)[side]
+        arrived(relay_buf.at[side], relay_recv.at[side])
+        total = pair_sum(to, side) + relay_buf[side].astype(jnp.float32)
+        sum_buf[1 + side, halves[side], :] = total.astype(jnp.bfloat16)
+        ring(side, side).start()
+    for half in range(2):
+        total = m_ref[halves[half], :].astype(jnp.float32) + pair_sum(x, half)
+        for side in (1 - half, half):
+            arrived(ring_buf.at[side, halves[half]], ring_recv.at[side, half])
+            total = total + ring_buf[side, halves[half], :].astype(jnp.float32)
+        out_ref[halves[half], :] = total.astype(out_ref.dtype)
+    for chip in range(SIDE):
+        twin(chip).wait_send()
+    for side in range(2):
+        relay(side).wait_send()
+        for half in range(2):
+            ring(side, half).wait_send()
+
+
+def reduce_rows(parts, middle):
+    _, rows, depth = parts.shape
+    vmem = pl.BlockSpec(memory_space=pltpu.VMEM)
+    dma = pltpu.SemaphoreType.DMA
+    return pl.pallas_call(
+        reduce_kernel,
+        out_shape=jax.ShapeDtypeStruct((rows, depth), jnp.bfloat16),
+        in_specs=[vmem, vmem],
+        out_specs=vmem,
+        scratch_shapes=[
+            pltpu.VMEM((SIDE, rows, depth), jnp.bfloat16),
+            pltpu.VMEM((3, rows, depth), jnp.bfloat16),
+            pltpu.VMEM((2, rows // 2, depth), jnp.bfloat16),
+            pltpu.VMEM((2, rows, depth), jnp.bfloat16),
+            dma((SIDE,)), dma((SIDE,)), dma((2,)), dma((2,)), dma((2, 2)), dma((2, 2)),
+        ],
+        compiler_params=pltpu.CompilerParams(has_side_effects=True, vmem_limit_bytes=32 * 2**20),
+        cost_estimate=pl.CostEstimate(flops=5 * 10**9, bytes_accessed=6 * 2**20, transcendentals=0),
+        name="reduce_rows",
+    )(parts, middle)
+
+
 def local(
     queries,
     keys,
@@ -372,42 +710,25 @@
     conv_value,
 ):
     rows_here = queries.shape[0]
-    model_width = residual.shape[1]
     bias_rows = stick_bias.reshape(rows_here // CHUNK, CHUNK)
     bias_rows = jnp.pad(bias_rows, ((0, PAD - bias_rows.shape[0]), (0, 0)))
-    units = gate_weight.shape[1]
     shared = exchange(queries, keys, values, bias_rows)
-    weights = jnp.concatenate([gate_weight, value_weight, down_weight], axis=1)
+    weights = jnp.concatenate([gate_weight.T, value_weight.T, down_weight.T], axis=0)
     weights, shared = lax.optimization_barrier((weights, shared))
-    whole = lax.all_gather(weights, "sp", axis=0, tiled=True)
-    whole_gate, whole_value, whole_down = (whole[:, k * units : (k + 1) * units] for k in range(3))
-    outs, logs = attention(queries, keys, values, bias_rows, *shared)
+    whole = lax.all_gather(weights, "sp", axis=0, tiled=False)
+    outs, logs = attention(keys, values, bias_rows, *shared)
     row_heads = combine(*deliver(outs, logs, lax.axis_size("tp")))
     projected = jnp.dot(row_heads, out_weight, preferred_element_type=jnp.float32)
-    middle_f = (residual.astype(jnp.float32) + projected).astype(jnp.bfloat16).astype(jnp.float32)
+    middle = (residual.astype(jnp.float32) + projected).astype(jnp.bfloat16)
+    middle_f = middle.astype(jnp.float32)
     normed = (
         middle_f
         * lax.rsqrt(jnp.mean(middle_f * middle_f, axis=-1, keepdims=True) + EPS)
         * norm_gain
     ).astype(jnp.bfloat16)
-    piece = lax.all_gather(normed, "tp", axis=0, tiled=True)
-    gate_up = jnp.dot(piece, whole_gate, preferred_element_type=jnp.float32).astype(jnp.bfloat16)
-    value_up = jnp.dot(piece, whole_value, preferred_element_type=jnp.float32).astype(jnp.bfloat16)
-    rim_gate, rim_value = from_behind((gate_up[-2:], value_up[-2:]), "sp", 1)
-
-    def depthwise(rim, upward, taps):
-        extended = jnp.concatenate([rim, upward], axis=0).astype(jnp.float32)
-        return taps[0] * extended[:-2] + taps[1] * extended[1:-1] + taps[2] * extended[2:]
-
-    hidden = (
-        jax.nn.silu(depthwise(rim_gate, gate_up, conv_gate))
-        * depthwise(rim_value, value_up, conv_value)
-    ).astype(jnp.bfloat16)
-    down = lax.dot_general(hidden, whole_down, NT, preferred_element_type=jnp.float32)
-    down_total = lax.psum_scatter(
-        down.astype(jnp.bfloat16), "tp", scatter_dimension=0, tiled=True
-    ).astype(jnp.float32)
-    return (middle_f + down_total).astype(jnp.bfloat16)
+    pieces, rim = gather_rows(normed)
+    parts = feed_forward(pieces, rim, whole, conv_gate, conv_value)
+    return reduce_rows(parts, middle)
 
 
 def solution(mesh):

time: 376 us -> 230 us (0.61)
  waiting for transfers between devices: 170 us -> 0.02 us
  Pallas kernels: 140 us -> 192 us
  matrix products: 25 us -> 3.03 us
  starting transfers between devices: 5.81 us -> 0.01 us
  local copies, waits for them, and re-layouts: 8.19 us -> 13.6 us
  other arithmetic: 9.21 us -> 4.92 us
    all_gather x2 -> x1, waiting for transfers between devices: 130 us -> 0.01 us  [local(): whole = lax.all_gather(weights, 'sp', axis=0, tiled=False)]
    pallas_call x0 -> x3, Pallas kernels: none -> 84.3 us  [the longest x1 31.8 us: gather_rows(): pl.pallas_call(gather_kernel, out_shape=(jax.ShapeDtypeStruct((2 * SIDE,...]
    reduce_scatter x1 -> x0, waiting for transfers between devices: 35.1 us -> none  [local(): lax.psum_scatter(down.astype(jnp.bfloat16), 'tp', scatter_dimension=0, ti...]
    dot_general x3 -> x0, matrix products: 22 us -> none  [the longest x1 10.6 us: local(): lax.dot_general(hidden, whole_down, NT, preferred_element_type=jnp.float32)]
    pallas_call x1, Pallas kernels: 51.1 us -> 32 us  [exchange(): pl.pallas_call(exchange_kernel, out_shape=(jax.ShapeDtypeStruct((count, r...]
    pallas_call x1, Pallas kernels: 44.9 us -> 31.1 us  [deliver(): pl.pallas_call(deliver_kernel, out_shape=(jax.ShapeDtypeStruct((heads, SI...]
    ppermute x2 -> x0, starting transfers between devices: 5.73 us -> none  [from_behind(): return lax.ppermute(block, axis, route)]
    unnamed x30 -> x29, local copies, waits for them, and re-layouts: 6.1 us -> 11.7 us
  transfers between devices with their start and end apart: 5 -> 1, of which waited for: 4 -> 0; matrix products, arithmetic and copies ran while one was open for 2% -> 3% of each run, Pallas kernels for 0% -> 47%
where the time goes in v3:
time: 230 us; the launch traced here: 227 us
  Pallas kernels  192 us (83%)
  local copies, waits for them, and re-layouts  13.6 us (6%)
  between operations  13.6 us (6%)
  other arithmetic  4.92 us (2%)
  matrix products  3.03 us (1%)
    pallas_call x1, Pallas kernels, attention(): pl.pallas_call(attention_kernel, out_shape=(jax.ShapeDtypeStruct((count,...  44.3 us
    pallas_call x1, Pallas kernels, exchange(): pl.pallas_call(exchange_kernel, out_shape=(jax.ShapeDtypeStruct((count, r...  32 us
    pallas_call x1, Pallas kernels, gather_rows(): pl.pallas_call(gather_kernel, out_shape=(jax.ShapeDtypeStruct((2 * SIDE,...  31.8 us
    pallas_call x1, Pallas kernels, reduce_rows(): pl.pallas_call(reduce_kernel, out_shape=jax.ShapeDtypeStruct((rows, depth...  31.2 us
    pallas_call x1, Pallas kernels, deliver(): pl.pallas_call(deliver_kernel, out_shape=(jax.ShapeDtypeStruct((heads, SI...  31.1 us
    pallas_call x1, Pallas kernels, feed_forward(): pl.pallas_call(feed_forward_kernel, out_shape=jax.ShapeDtypeStruct((block...  21.3 us
    unnamed x29, local copies, waits for them, and re-layouts  11.7 us
  transfers between devices with their start and end apart: 1, of which 0 were waited for; matrix products, arithmetic and copies ran while one was open for 3% of the time, Pallas kernels for 47%

profile of v3, /device:TPU:26, one launch (start us, length us, event | category | flops | bytes accessed | tf_op | source)
XLA Modules:
  0.0 226.9 jit_solution(7132648688430401018)
XLA Ops:
  6.5 0.0 all-gather.3.cloned.1.call-start
  6.5 0.7 reduce
  7.3 0.6 pad.4.b_ref
  7.9 2.0 pad_maximum_fusion
  9.8 32.0 %exchange.1 = (bf16[16,256,128]{2,1,0:T(8,128)(2,1)}, bf16[4,1024,128]{2,1,0:T(8,128)(2,1)}, bf16[4,1024,128]{2,1,0:T(8,128)(2,1)}, bf16[4,16,256]{2,1,0:T(8,128)(2,1)}) custom-call(bf16[1024,128]{1,0:T(8,128)(2,1)} %q_ref.1, bf16[1024,128]{1,0:T(8,128)(2,1)} %k_ref.3, bf16[1024,128]{1,0:T(8,128)(2,1)} %v_ref.3, bf16[16,256]{1,0:T(8,128)(2,1)} %pad.4.b_ref), custom_call_target="tpu_custom_call" | custom-call | flops 10000000000 | bytes 4194304 | tf_op jit(solution)/shard_map/exchange/pallas_call | solution.py:163
  41.8 0.0 all-gather.3.cloned.1.call-update
  41.9 1.2 copy-done.6
  43.1 1.2 copy-done.7
  44.4 1.2 copy-done.8
  45.6 0.8 copy-done.11
  46.3 44.3 %attention.1 = (bf16[16,256,128]{2,1,0:T(8,128)(2,1)S(1)}, f32[16,2,8,128]{3,2,1,0:T(8,128)S(1)}) custom-call(bf16[1024,128]{1,0:T(8,128)(2,1)S(1)} %copy-done.1, bf16[1024,128]{1,0:T(8,128)(2,1)S(1)} %copy-done.2, bf16[16,256]{1,0:T(8,128)(2,1)S(1)} %copy-done, bf16[16,256,128]{2,1,0:T(8,128)(2,1)S(1)} %copy-done.6, bf16[4,1024,128]{2,1,0:T(8,128)(2,1)S(1)} %copy-done.7, ...), custom_call_target="tpu_custom_call" | custom-call | flops 11274289152 | bytes 4194304 | tf_op jit(solution)/shard_map/attention/pallas_call | solution.py:287
  90.7 0.0 copy-start.5
  90.7 1.1 copy-done.5
  91.7 0.7 copy-done.9
  92.4 31.1 %deliver.1 = (bf16[8,4,128,128]{3,2,1,0:T(8,128)(2,1)}, f32[8,4,8,128]{3,2,1,0:T(8,128)}) custom-call(bf16[16,256,128]{2,1,0:T(8,128)(2,1)} %copy-done.5, f32[16,2,8,128]{3,2,1,0:T(8,128)} %copy-done.9), custom_call_target="tpu_custom_call" | custom-call | flops 5000000000 | bytes 4194304 | tf_op jit(solution)/shard_map/deliver/pallas_call | solution.py:383
  123.5 0.0 copy-start.12
  123.5 1.0 slice.3
  124.5 0.1 broadcast_select_fusion
  124.7 0.1 exponential_select_fusion
  124.8 1.8 multiply_reduce_fusion
  126.6 0.2 copy.13
  126.8 0.0 copy-start.13
  126.8 3.0 %fusion.1 = (f32[128]{0:T(128)S(1)}, bf16[128,2048]{1,0:T(8,128)(2,1)S(1)}) fusion(bf16[128,1024]{0,1:T(8,128)(2,1)S(1)} %bitcast.12, bf16[1024,2048]{1,0:T(8,128)(2,1)} %param.17, bf16[128,2048]{1,0:T(8,128)(2,1)S(1)} %copy-done.12), kind=kOutput, calls=%fused_computation.5 | convolution fusion | flops 538443648 | bytes 5505536 | tf_op jit(solution)/shard_map/dot_general | solution.py:721
  129.9 0.2 fusion.3.n_ref
  130.1 31.8 %gather_rows.1 = (bf16[8,128,2048]{2,1,0:T(8,128)(2,1)S(1)}, bf16[16,2048]{1,0:T(8,128)(2,1)S(1)}) custom-call(bf16[128,2048]{1,0:T(8,128)(2,1)S(1)} %fusion.3.n_ref), custom_call_target="tpu_custom_call" | custom-call | flops 5000000000 | bytes 4194304 | tf_op jit(solution)/shard_map/gather_rows/pallas_call | solution.py:501
  161.9 2.0 copy-done.4
  163.9 0.6 copy-done.10
  164.5 21.3 %feed_forward.1.p_ref = bf16[8,128,2048]{2,1,0:T(8,128)(2,1)} custom-call(bf16[8,128,2048]{2,1,0:T(8,128)(2,1)} %copy-done.4, bf16[16,2048]{1,0:T(8,128)(2,1)} %copy-done.10, bf16[16,2112,128]{2,1,0:T(8,128)(2,1)} %bitcast.18, f32[3,704]{1,0:T(4,128)} %cg_ref.1, f32[3,704]{1,0:T(4,128)} %cv_ref.1), custom_call_target="tpu_custom_call" | custom-call | flops 8999999488 | bytes 18874368 | tf_op jit(solution)/shard_map/feed_forward/pallas_call | solution.py:582
  185.8 0.0 copy-start.3
  185.9 2.2 copy-done.3
  188.0 31.2 %reduce_rows.1 = bf16[128,2048]{1,0:T(8,128)(2,1)S(1)} custom-call(bf16[8,128,2048]{2,1,0:T(8,128)(2,1)S(1)} %copy-done.3, bf16[128,2048]{1,0:T(8,128)(2,1)S(1)} %get-tuple-element.36.m_ref), custom_call_target="tpu_custom_call" | custom-call | flops 5000000000 | bytes 6291456 | tf_op jit(solution)/shard_map/reduce_rows/pallas_call | solution.py:680
  219.2 0.8 copy.15
  (22 shorter events, 0.2 us)
Async XLA Ops:
  6.5 158.0 %all-gather.3.cloned.1.call-start = ((), (), s32[]{:S(2)}) async-start(), calls=%async_computation | async-start | bytes 9191424 | tf_op jit(solution)/shard_map/all_gather | solution.py:718
  9.8 32.0 %copy-start = (bf16[16,256]{1,0:T(8,128)(2,1)S(1)}, bf16[16,256]{1,0:T(8,128)(2,1)}, u32[]{:S(2)}) copy-start(bf16[16,256]{1,0:T(8,128)(2,1)} %pad.4.b_ref) | copy-start | bytes 24580
  9.8 32.0 %copy-start.1 = (bf16[1024,128]{1,0:T(8,128)(2,1)S(1)}, bf16[1024,128]{1,0:T(8,128)(2,1)}, u32[]{:S(2)}) copy-start(bf16[1024,128]{1,0:T(8,128)(2,1)} %k_ref.3) | copy-start | bytes 786436
  9.8 32.1 %copy-start.2 = (bf16[1024,128]{1,0:T(8,128)(2,1)S(1)}, bf16[1024,128]{1,0:T(8,128)(2,1)}, u32[]{:S(2)}) copy-start(bf16[1024,128]{1,0:T(8,128)(2,1)} %v_ref.3) | copy-start | bytes 786436
  41.9 1.2 copy-start.6
  43.1 1.2 copy-start.7
  44.4 1.2 copy-start.8
  45.6 0.8 copy-start.11
  90.7 1.1 copy-start.5
  91.7 0.7 copy-start.9
  123.5 3.3 %copy-start.12 = (bf16[128,2048]{1,0:T(8,128)(2,1)S(1)}, bf16[128,2048]{1,0:T(8,128)(2,1)}, u32[]{:S(2)}) copy-start(bf16[128,2048]{1,0:T(8,128)(2,1)} %param.16) | copy-start | bytes 1572868
  126.8 3.1 %copy-start.13 = (f32[2048]{0:T(1024)S(1)}, f32[2048]{0:T(1024)}, u32[]{:S(2)}) copy-start(f32[2048]{0:T(1024)} %param.18) | copy-start | bytes 24580
  161.9 2.0 copy-start.4
  163.9 0.6 copy-start.10
  185.8 2.2 copy-start.3
Sparse Core Ops, SparseCore 0:
  42.0 84.7 all-gather.2

commit v4 on v3

--- a/solution.py
+++ b/solution.py
@@ -12,6 +12,7 @@
 PAD = 16
 SIDE = 4
 RIM = 16
+VMEM = 67_000_000
 
 
 def tri_matrix():
@@ -58,6 +59,13 @@
     pltpu.make_async_copy(dst, dst, sem).wait()
 
 
+def meet(peers, extra=0):
+    barrier = pltpu.get_barrier_semaphore()
+    for where in peers:
+        pl.semaphore_signal(barrier, inc=1, device_id=where, device_id_type=pl.DeviceIdType.MESH)
+    pl.semaphore_wait(barrier, len(peers) + extra)
+
+
 def exchange_kernel(
     q_ref, k_ref, v_ref, b_ref, qs_ref, ks_ref, vs_ref, bs_ref,
     send_sem, recv_sem, bias_send, bias_recv, q_send, q_recv, own_sem, z_send, z_recv,
@@ -68,6 +76,10 @@
     left = (y + 3) % SIDE
     across = (y + 2) % SIDE
     row = z * SIDE
+    meet(
+        [{"sp": row + (y + d) % SIDE} for d in (1, 2, 3)]
+        + [{"sp": (z + d) % SIDE * SIDE + y} for d in (1, 2, 3)]
+    )
 
     def hop(part, src_slot, to, lane):
         src = (k_ref, v_ref)[part] if src_slot is None else (ks_ref, vs_ref)[part].at[src_slot]
@@ -174,7 +186,7 @@
             dma((2, 3)), dma((2, SIDE)), dma((SIDE,)), dma((SIDE,)), dma((SIDE, 2)),
             dma((SIDE, 2)), dma((2,)), dma((SIDE,)), dma((SIDE,)),
         ],
-        compiler_params=pltpu.CompilerParams(has_side_effects=True),
+        compiler_params=pltpu.CompilerParams(has_side_effects=True, collective_id=0, vmem_limit_bytes=VMEM),
         cost_estimate=pl.CostEstimate(flops=10**10, bytes_accessed=4 * 2**20, transcendentals=0),
         name="exchange",
     )(queries, keys, values, bias_rows)
@@ -281,7 +293,6 @@
 
 def attention(keys, values, bias_rows, q_parts, k_parts, v_parts, b_parts):
     rows, head = keys.shape
-    anywhere = pl.BlockSpec(memory_space=pl.ANY)
     vmem = pl.BlockSpec(memory_space=pltpu.VMEM)
     count = SIDE * SIDE
     return pl.pallas_call(
@@ -290,7 +301,7 @@
             jax.ShapeDtypeStruct((count, rows // SIDE, head), jnp.bfloat16),
             jax.ShapeDtypeStruct((count, 2, 8, 128), jnp.float32),
         ),
-        in_specs=[anywhere] * 7,
+        in_specs=[pl.BlockSpec(memory_space=pltpu.HBM)] * 7,
         out_specs=[vmem, vmem],
         scratch_shapes=[
             pltpu.VMEM((SIDE * rows, head), jnp.bfloat16),
@@ -302,7 +313,7 @@
             pltpu.SemaphoreType.DMA((3, SIDE)),
             pltpu.SemaphoreType.DMA((count,)),
         ],
-        compiler_params=pltpu.CompilerParams(vmem_limit_bytes=48 * 2**20),
+        compiler_params=pltpu.CompilerParams(vmem_limit_bytes=VMEM),
         cost_estimate=pl.CostEstimate(
             flops=14 * 6 * rows * rows * head, bytes_accessed=4 * 2**20, transcendentals=0
         ),
@@ -315,6 +326,22 @@
     head = lax.axis_index("tp")
     owner_rows = os_ref.shape[2]
     owners = owners_of(y)
+    x, core = place_of()
+    barrier = pltpu.get_barrier_semaphore()
+
+    def greet(group, carry):
+        for source in range(os_ref.shape[0]):
+            row = (x - source % 2 - 2 * core + 2 * SIDE) % SIDE
+            pl.semaphore_signal(
+                barrier,
+                inc=1,
+                device_id={"sp": group * SIDE + row, "tp": source},
+                device_id_type=pl.DeviceIdType.MESH,
+            )
+        return carry
+
+    lax.fori_loop(0, z + 1, greet, 0)
+    pl.semaphore_wait(barrier, 2 * (SIDE * SIDE - z * SIDE))
 
     def pieces(block, half):
         src = o_ref.at[block, pl.ds(half * owner_rows, owner_rows)]
@@ -392,7 +419,7 @@
             pltpu.SemaphoreType.DMA((2, count, 2)),
             pltpu.SemaphoreType.DMA((2, heads, SIDE)),
         ],
-        compiler_params=pltpu.CompilerParams(has_side_effects=True),
+        compiler_params=pltpu.CompilerParams(has_side_effects=True, collective_id=1, vmem_limit_bytes=VMEM),
         cost_estimate=pl.CostEstimate(flops=5 * 10**9, bytes_accessed=4 * 2**20, transcendentals=0),
         name="deliver",
     )(outs, logs)
@@ -414,116 +441,25 @@
     return me // 2, me % 2
 
 
-def gather_kernel(n_ref, all_ref, rim_ref, ring_send, ring_recv, twin_send, twin_recv, rim_send, rim_recv, own_sem):
+def feed_forward_kernel(
+    n_ref, m_ref, w_ref, cg_ref, cv_ref, out_ref,
+    all_ref, rim_ref, up_ref, down_ref, gate_ref, value_ref, p_ref, twin_buf, sum_buf, relay_buf,
+    ring_buf, w_sem, ring_send, ring_recv, twin_send, twin_recv, rim_send, rim_recv, own_sem,
+    pair_send, pair_recv, relay_send, relay_recv, back_send, back_recv,
+):
     x, core = place_of()
     block = lax.axis_index("sp")
-    rows = n_ref.shape[0]
+    rows, depth = n_ref.shape
     part = rows // 2
+    tile = 2 * rows
+    units = down_ref.shape[0]
+    shards = w_ref.shape[0]
+    deep = depth // shards
     right = (x + 1) % SIDE
     left = (x + 3) % SIDE
     across = (x + 2) % SIDE
-
-    def spot(chip, half, of_core=None):
-        of_core = core if of_core is None else of_core
-        return all_ref.at[2 * chip + of_core, pl.ds(half * part, part)]
-
-    def ring(chip, half, to, lane):
-        src = n_ref.at[pl.ds(half * part, part)] if chip is None else spot(chip, half)
-        chip = x if chip is None else chip
-        return remote_copy(
-            src, spot(chip, half), ring_send.at[lane, half], ring_recv.at[chip, half], tp=2 * to + core
-        )
-
-    def twin(chip, half):
-        src = n_ref.at[pl.ds(half * part, part)] if chip is None else spot(chip, half)
-        chip = x if chip is None else chip
-        return remote_copy(
-            src, spot(chip, half), twin_send.at[chip, half], twin_recv.at[chip, half], tp=2 * x + 1 - core
-        )
-
-    def rim(to):
-        return remote_copy(
-            n_ref.at[pl.ds(rows - RIM, RIM)], rim_ref, rim_send.at[to], rim_recv, sp=block + 1, tp=to
-        )
-
-    last = (x == SIDE - 1) & (core == 1) & (block < SIDE * SIDE - 1)
-    own = pltpu.make_async_copy(n_ref, all_ref.at[2 * x + core], own_sem)
-    ring(None, 0, right, 0).start()
-    ring(None, 1, left, 1).start()
-    ring(None, 1, right, 0).start()
-    ring(None, 0, left, 1).start()
-    own.start()
-    for half in range(2):
-        twin(None, half).start()
-
-    @pl.when(last)
-    def _():
-        for to in range(2 * SIDE):
-            rim(to).start()
-
-    arrived(spot(left, 0), ring_recv.at[left, 0])
-    ring(left, 0, right, 2).start()
-    twin(left, 0).start()
-    arrived(spot(right, 1), ring_recv.at[right, 1])
-    ring(right, 1, left, 2).start()
-    twin(right, 1).start()
-    for chip, half in ((left, 1), (right, 0), (across, 0), (across, 1)):
-        arrived(spot(chip, half), ring_recv.at[chip, half])
-        twin(chip, half).start()
-    own.wait()
-    for chip in range(SIDE):
-        for half in range(2):
-            arrived(spot(chip, half, 1 - core), twin_recv.at[chip, half])
-
-    @pl.when(block > 0)
-    def _():
-        arrived(rim_ref, rim_recv)
-
-    for half in range(2):
-        ring(None, half, right, 0).wait_send()
-        ring(None, half, left, 1).wait_send()
-        twin(None, half).wait_send()
-        for chip in (left, right, across):
-            twin(chip, half).wait_send()
-    ring(left, 0, right, 2).wait_send()
-    ring(right, 1, left, 2).wait_send()
-
-    @pl.when(last)
-    def _():
-        for to in range(2 * SIDE):
-            rim(to).wait_send()
-
-
-def gather_rows(normed):
-    rows, width = normed.shape
-    vmem = pl.BlockSpec(memory_space=pltpu.VMEM)
-    dma = pltpu.SemaphoreType.DMA
-    return pl.pallas_call(
-        gather_kernel,
-        out_shape=(
-            jax.ShapeDtypeStruct((2 * SIDE, rows, width), jnp.bfloat16),
-            jax.ShapeDtypeStruct((RIM, width), jnp.bfloat16),
-        ),
-        in_specs=[vmem],
-        out_specs=[vmem, vmem],
-        scratch_shapes=[
-            dma((3, 2)), dma((SIDE, 2)), dma((SIDE, 2)), dma((SIDE, 2)), dma((2 * SIDE,)), dma(()), dma(()),
-        ],
-        compiler_params=pltpu.CompilerParams(has_side_effects=True, vmem_limit_bytes=24 * 2**20),
-        cost_estimate=pl.CostEstimate(flops=5 * 10**9, bytes_accessed=4 * 2**20, transcendentals=0),
-        name="gather_rows",
-    )(normed)
-
-
-def feed_forward_kernel(
-    x_ref, rim_ref, w_ref, cg_ref, cv_ref, out_ref, up_ref, down_ref, gate_ref, value_ref, w_sem
-):
-    blocks, rows, depth = x_ref.shape
-    units = down_ref.shape[0]
-    shards = w_ref.shape[0]
-    deep = depth // shards
-    tile = 2 * rows
-    first = lax.axis_index("sp") == 0
+    other = 2 * x + 1 - core
+    halves = (slice(0, part), slice(part, rows))
 
     def weight_copies(k):
         at = slice(k * deep, (k + 1) * deep)
@@ -539,160 +475,253 @@
     for k in range(shards):
         for copy in weight_copies(k):
             copy.start()
-    for k in range(shards):
-        weight_copies(k)[0].wait()
-
-    def up(x, which):
+
+    def spot(chip, half, of_core):
+        return all_ref.at[2 * chip + of_core, pl.ds(half * part, part)]
+
+    def ring(chip, half, to, lane):
+        src = n_ref.at[pl.ds(half * part, part)] if chip is None else spot(chip, half, core)
+        chip = x if chip is None else chip
+        return remote_copy(
+            src,
+            spot(chip, half, core),
+            ring_send.at[lane, half],
+            ring_recv.at[chip, half],
+            tp=2 * to + core,
+        )
+
+    def twin(chip, half):
+        src = n_ref.at[pl.ds(half * part, part)] if chip is None else spot(chip, half, core)
+        chip = x if chip is None else chip
+        return remote_copy(
+            src, spot(chip, half, core), twin_send.at[chip, half], twin_recv.at[chip, half], tp=other
+        )
+
+    def rim(to):
+        return remote_copy(
+            n_ref.at[pl.ds(rows - RIM, RIM)], rim_ref, rim_send.at[to], rim_recv, sp=block + 1, tp=to
+        )
+
+    last = (x == SIDE - 1) & (core == 1) & (block < SIDE * SIDE - 1)
+    barrier = pltpu.get_barrier_semaphore()
+
+    @pl.when(block > 0)
+    def _():
+        pl.semaphore_signal(
+            barrier,
+            inc=1,
+            device_id={"sp": block - 1, "tp": 2 * SIDE - 1},
+            device_id_type=pl.DeviceIdType.MESH,
+        )
+
+    meet(
+        [{"tp": 2 * right + core}, {"tp": 2 * left + core}, {"tp": other}],
+        jnp.where(last, 2 * SIDE, 0),
+    )
+    own = pltpu.make_async_copy(n_ref, all_ref.at[2 * x + core], own_sem)
+    ring(None, 0, right, 0).start()
+    ring(None, 1, left, 1).start()
+    ring(None, 1, right, 0).start()
+    ring(None, 0, left, 1).start()
+    own.start()
+    for half in range(2):
+        twin(None, half).start()
+
+    @pl.when(last)
+    def _():
+        for to in range(2 * SIDE):
+            rim(to).start()
+
+    def up(rows_in, which):
         w = up_ref[which * units : (which + 1) * units, :]
-        return lax.dot_general(x, w, NT, preferred_element_type=jnp.float32)
-
-    for which, ref in enumerate((gate_ref, value_ref)):
-        rim = up(rim_ref[...], which)
-        ref[0:RIM, :] = jnp.where(first, 0.0, rim)
-
-    def conv(ref, taps, start):
-        at = pl.multiple_of(start, tile)
-        window = ref[pl.ds(at, tile + RIM), :]
+        return lax.dot_general(rows_in, w, NT, preferred_element_type=jnp.float32)
+
+    def project_up(chip):
+        rows_in = all_ref[pl.ds(2 * chip, 2)].reshape(tile, depth)
+        for which, ref in enumerate((gate_ref, value_ref)):
+            ref[pl.ds(pl.multiple_of(chip * tile + RIM, RIM), tile), :] = up(rows_in, which)
+
+    def conv(ref, taps, chip):
+        window = ref[pl.ds(pl.multiple_of(chip * tile, tile), tile + RIM), :]
         return (
             taps[0:1, :] * window[RIM - 2 : RIM - 2 + tile]
             + taps[1:2, :] * window[RIM - 1 : RIM - 1 + tile]
             + taps[2:3, :] * window[RIM : RIM + tile]
         )
 
+    def project_down(chip):
+        gate = conv(gate_ref, cg_ref, chip)
+        value = conv(value_ref, cv_ref, chip)
+        hidden = (gate / (1.0 + jnp.exp(-gate)) * value).astype(jnp.bfloat16)
+        down = jnp.dot(hidden, down_ref[...], preferred_element_type=jnp.float32)
+        p_ref[pl.ds(2 * chip, 2)] = down.astype(p_ref.dtype).reshape(2, rows, depth)
+
+    def twin_arrived(chip):
+        for half in range(2):
+            arrived(spot(chip, half, 1 - core), twin_recv.at[chip, half])
+
+    for k in range(shards):
+        weight_copies(k)[0].wait()
+    own.wait()
+    twin_arrived(x)
+    project_up(x)
+    arrived(spot(left, 0, core), ring_recv.at[left, 0])
+    ring(left, 0, right, 2).start()
+    twin(left, 0).start()
+    arrived(spot(right, 1, core), ring_recv.at[right, 1])
+    ring(right, 1, left, 2).start()
+    twin(right, 1).start()
+
+    @pl.when(block > 0)
+    def _():
+        arrived(rim_ref, rim_recv)
+        for which, ref in enumerate((gate_ref, value_ref)):
+            ref[0:RIM, :] = up(rim_ref[...], which)
+
+    @pl.when(block == 0)
+    def _():
+        for ref in (gate_ref, value_ref):
+            ref[0:RIM, :] = jnp.zeros((RIM, units), jnp.float32)
+
+    for chip, half in ((left, 1), (right, 0)):
+        arrived(spot(chip, half, core), ring_recv.at[chip, half])
+        twin(chip, half).start()
+    twin_arrived(right)
+    project_up(right)
+    twin_arrived(left)
+    project_up(left)
+    for half in range(2):
+        arrived(spot(across, half, core), ring_recv.at[across, half])
+        twin(across, half).start()
     for k in range(shards):
         weight_copies(k)[1].wait()
 
-    @pl.loop(0, blocks // 2)
-    def _(t):
-        x = x_ref[pl.ds(t * 2, 2)].reshape(tile, depth)
-        start = t * tile
-        for which, ref in enumerate((gate_ref, value_ref)):
-            ref[pl.ds(pl.multiple_of(start + RIM, RIM), tile), :] = up(x, which)
-        gate = conv(gate_ref, cg_ref, start)
-        value = conv(value_ref, cv_ref, start)
-        hidden = (gate / (1.0 + jnp.exp(-gate)) * value).astype(jnp.bfloat16)
-        down = jnp.dot(hidden, down_ref[...], preferred_element_type=jnp.float32)
-        out_ref[pl.ds(t * 2, 2)] = down.astype(out_ref.dtype).reshape(2, rows, depth)
-
-
-def feed_forward(pieces, rim, whole, conv_gate, conv_value):
-    blocks, rows, depth = pieces.shape
-    units = conv_gate.shape[1]
-    vmem = pl.BlockSpec(memory_space=pltpu.VMEM)
-    return pl.pallas_call(
-        feed_forward_kernel,
-        out_shape=jax.ShapeDtypeStruct((blocks, rows, depth), jnp.bfloat16),
-        in_specs=[vmem, vmem, pl.BlockSpec(memory_space=pl.ANY), vmem, vmem],
-        out_specs=vmem,
-        scratch_shapes=[
-            pltpu.VMEM((2 * units, depth), jnp.bfloat16),
-            pltpu.VMEM((units, depth), jnp.bfloat16),
-            pltpu.VMEM((RIM + blocks * rows, units), jnp.float32),
-            pltpu.VMEM((RIM + blocks * rows, units), jnp.float32),
-            pltpu.SemaphoreType.DMA((2, whole.shape[0])),
-        ],
-        compiler_params=pltpu.CompilerParams(vmem_limit_bytes=56 * 2**20),
-        cost_estimate=pl.CostEstimate(flops=9 * 10**9, bytes_accessed=18 * 2**20, transcendentals=0),
-        name="feed_forward",
-    )(pieces, rim, whole, conv_gate, conv_value)
-
-
-def reduce_kernel(p_ref, m_ref, out_ref, twin_buf, sum_buf, relay_buf, ring_buf, twin_send, twin_recv, relay_send, relay_recv, ring_send, ring_recv):
-    x, core = place_of()
-    rows = p_ref.shape[1]
-    part = rows // 2
-    right = (x + 1) % SIDE
-    left = (x + 3) % SIDE
-    across = (x + 2) % SIDE
-    halves = (slice(0, part), slice(part, rows))
-
-    def twin(chip):
+    def pair(chip):
         return remote_copy(
             p_ref.at[2 * chip + 1 - core],
             twin_buf.at[chip],
-            twin_send.at[chip],
-            twin_recv.at[chip],
-            tp=2 * x + 1 - core,
-        )
-
-    for chip in (across, right, left, x):
-        twin(chip).start()
+            pair_send.at[chip],
+            pair_recv.at[chip],
+            tp=other,
+        )
 
     def pair_sum(chip, half):
         mine = p_ref[2 * chip + core, halves[half], :].astype(jnp.float32)
         return mine + twin_buf[chip, halves[half], :].astype(jnp.float32)
 
     def relay(side):
-        to = (right, left)[side]
         return remote_copy(
             sum_buf.at[0, halves[side]],
             relay_buf.at[side],
             relay_send.at[side],
             relay_recv.at[side],
-            tp=2 * to + core,
-        )
-
-    def ring(side, half):
-        to = (right, left)[side]
+            tp=2 * (right, left)[side] + core,
+        )
+
+    def back(side, half):
         return remote_copy(
             sum_buf.at[1 + side, halves[half]],
             ring_buf.at[side, halves[half]],
-            ring_send.at[side, half],
-            ring_recv.at[side, half],
-            tp=2 * to + core,
-        )
-
-    arrived(twin_buf.at[across], twin_recv.at[across])
+            back_send.at[side, half],
+            back_recv.at[side, half],
+            tp=2 * (right, left)[side] + core,
+        )
+
+    def direct(side):
+        to = (right, left)[side]
+        half = 1 - side
+        arrived(twin_buf.at[to], pair_recv.at[to])
+        sum_buf[1 + side, halves[half], :] = pair_sum(to, half).astype(jnp.bfloat16)
+        back(side, half).start()
+
+    project_down(right)
+    pair(right).start()
+    project_down(x)
+    pair(x).start()
+    direct(0)
+    twin_arrived(across)
+    project_up(across)
+    project_down(across)
+    pair(across).start()
+    arrived(twin_buf.at[across], pair_recv.at[across])
     for side in range(2):
         sum_buf[0, halves[side], :] = pair_sum(across, side).astype(jnp.bfloat16)
         relay(side).start()
-    for side in range(2):
-        to = (right, left)[side]
-        arrived(twin_buf.at[to], twin_recv.at[to])
-        half = 1 - side
-        sum_buf[1 + side, halves[half], :] = pair_sum(to, half).astype(jnp.bfloat16)
-        ring(side, half).start()
-    arrived(twin_buf.at[x], twin_recv.at[x])
+    project_down(left)
+    pair(left).start()
+    direct(1)
+    arrived(twin_buf.at[x], pair_recv.at[x])
     for side in range(2):
         to = (right, left)[side]
         arrived(relay_buf.at[side], relay_recv.at[side])
         total = pair_sum(to, side) + relay_buf[side].astype(jnp.float32)
         sum_buf[1 + side, halves[side], :] = total.astype(jnp.bfloat16)
-        ring(side, side).start()
+        back(side, side).start()
     for half in range(2):
         total = m_ref[halves[half], :].astype(jnp.float32) + pair_sum(x, half)
         for side in (1 - half, half):
-            arrived(ring_buf.at[side, halves[half]], ring_recv.at[side, half])
+            arrived(ring_buf.at[side, halves[half]], back_recv.at[side, half])
             total = total + ring_buf[side, halves[half], :].astype(jnp.float32)
         out_ref[halves[half], :] = total.astype(out_ref.dtype)
+
+    for half in range(2):
+        ring(None, half, right, 0).wait_send()
+        ring(None, half, left, 1).wait_send()
+        twin(None, half).wait_send()
+        for chip in (left, right, across):
+            twin(chip, half).wait_send()
+    ring(left, 0, right, 2).wait_send()
+    ring(right, 1, left, 2).wait_send()
+
+    @pl.when(last)
+    def _():
+        for to in range(2 * SIDE):
+            rim(to).wait_send()
+
     for chip in range(SIDE):
-        twin(chip).wait_send()
+        pair(chip).wait_send()
     for side in range(2):
         relay(side).wait_send()
         for half in range(2):
-            ring(side, half).wait_send()
-
-
-def reduce_rows(parts, middle):
-    _, rows, depth = parts.shape
+            back(side, half).wait_send()
+
+
+def feed_forward(normed, middle, whole, conv_gate, conv_value):
+    rows, depth = normed.shape
+    units = conv_gate.shape[1]
+    total = 2 * SIDE * rows
     vmem = pl.BlockSpec(memory_space=pltpu.VMEM)
     dma = pltpu.SemaphoreType.DMA
+    bf16 = jnp.bfloat16
     return pl.pallas_call(
-        reduce_kernel,
-        out_shape=jax.ShapeDtypeStruct((rows, depth), jnp.bfloat16),
-        in_specs=[vmem, vmem],
+        feed_forward_kernel,
+        out_shape=jax.ShapeDtypeStruct((rows, depth), bf16),
+        in_specs=[vmem, vmem, pl.BlockSpec(memory_space=pl.ANY), vmem, vmem],
         out_specs=vmem,
         scratch_shapes=[
-            pltpu.VMEM((SIDE, rows, depth), jnp.bfloat16),
-            pltpu.VMEM((3, rows, depth), jnp.bfloat16),
-            pltpu.VMEM((2, rows // 2, depth), jnp.bfloat16),
-            pltpu.VMEM((2, rows, depth), jnp.bfloat16),
+            pltpu.VMEM((2 * SIDE, rows, depth), bf16),
+            pltpu.VMEM((RIM, depth), bf16),
+            pltpu.VMEM((2 * units, depth), bf16),
+            pltpu.VMEM((units, depth), bf16),
+            pltpu.VMEM((RIM + total, units), jnp.float32),
+            pltpu.VMEM((RIM + total, units), jnp.float32),
+            pltpu.VMEM((2 * SIDE, rows, depth), bf16),
+            pltpu.VMEM((SIDE, rows, depth), bf16),
+            pltpu.VMEM((3, rows, depth), bf16),
+            pltpu.VMEM((2, rows // 2, depth), bf16),
+            pltpu.VMEM((2, rows, depth), bf16),
+            dma((2, whole.shape[0])),
+            dma((3, 2)), dma((SIDE, 2)), dma((SIDE, 2)), dma((SIDE, 2)), dma((2 * SIDE,)), dma(()), dma(()),
             dma((SIDE,)), dma((SIDE,)), dma((2,)), dma((2,)), dma((2, 2)), dma((2, 2)),
         ],
-        compiler_params=pltpu.CompilerParams(has_side_effects=True, vmem_limit_bytes=32 * 2**20),
-        cost_estimate=pl.CostEstimate(flops=5 * 10**9, bytes_accessed=6 * 2**20, transcendentals=0),
-        name="reduce_rows",
-    )(parts, middle)
+        compiler_params=pltpu.CompilerParams(
+            has_side_effects=True, collective_id=2, vmem_limit_bytes=VMEM
+        ),
+        cost_estimate=pl.CostEstimate(
+            flops=9 * 10**9, bytes_accessed=12 * 2**20, transcendentals=0
+        ),
+        name="feed_forward",
+    )(normed, middle, whole, conv_gate, conv_value)
 
 
 def local(
@@ -726,9 +755,7 @@
         * lax.rsqrt(jnp.mean(middle_f * middle_f, axis=-1, keepdims=True) + EPS)
         * norm_gain
     ).astype(jnp.bfloat16)
-    pieces, rim = gather_rows(normed)
-    parts = feed_forward(pieces, rim, whole, conv_gate, conv_value)
-    return reduce_rows(parts, middle)
+    return feed_forward(normed, middle, whole, conv_gate, conv_value)
 
 
 def solution(mesh):

time: 230 us -> 191 us (0.83)
  Pallas kernels: 192 us -> 157 us
  local copies, waits for them, and re-layouts: 13.6 us -> 4.58 us
  waiting for transfers between devices: 0.02 us -> 5.02 us
    pallas_call x3 -> x1, Pallas kernels: 84.3 us -> 57.8 us  [feed_forward(): pl.pallas_call(feed_forward_kernel, out_shape=jax.ShapeDtypeStruct((rows,...]
    unnamed x29 -> x7, local copies, waits for them, and re-layouts: 11.7 us -> 2.72 us
    pallas_call x1, Pallas kernels: 32 us -> 26 us  [exchange(): pl.pallas_call(exchange_kernel, out_shape=(jax.ShapeDtypeStruct((count, r...]
    all_gather x1, waiting for transfers between devices: 0.01 us -> 5 us  [local(): whole = lax.all_gather(weights, 'sp', axis=0, tiled=False)]
    pallas_call x1, Pallas kernels: 31.1 us -> 27.7 us  [deliver(): pl.pallas_call(deliver_kernel, out_shape=(jax.ShapeDtypeStruct((heads, SI...]
  transfers between devices with their start and end apart: 1 -> 1, of which waited for: 0 -> 1; matrix products, arithmetic and copies ran while one was open for 3% -> 4% of each run, Pallas kernels for 47% -> 39%
where the time goes in v4:
time: 191 us; the launch traced here: 189 us
  Pallas kernels  157 us (82%)
  between operations  13.5 us (7%)
  other arithmetic  5.7 us (3%)
  waiting for transfers between devices  5.02 us (3%)
  local copies, waits for them, and re-layouts  4.58 us (2%)
  matrix products  3.04 us (2%)
    pallas_call x1, Pallas kernels, feed_forward(): pl.pallas_call(feed_forward_kernel, out_shape=jax.ShapeDtypeStruct((rows,...  57.8 us
    pallas_call x1, Pallas kernels, attention(): pl.pallas_call(attention_kernel, out_shape=(jax.ShapeDtypeStruct((count,...  45.5 us
    pallas_call x1, Pallas kernels, deliver(): pl.pallas_call(deliver_kernel, out_shape=(jax.ShapeDtypeStruct((heads, SI...  27.7 us
    pallas_call x1, Pallas kernels, exchange(): pl.pallas_call(exchange_kernel, out_shape=(jax.ShapeDtypeStruct((count, r...  26 us
    all_gather x1, waiting for transfers between devices, local(): whole = lax.all_gather(weights, 'sp', axis=0, tiled=False)  5 us
  transfers between devices with their start and end apart: 1, of which 1 were waited for; matrix products, arithmetic and copies ran while one was open for 4% of the time, Pallas kernels for 39%

profile of v4, /device:TPU:26, one launch (start us, length us, event | category | flops | bytes accessed | tf_op | source)
XLA Modules:
  0.0 188.9 jit_solution(12856168921971787350)
XLA Ops:
  6.5 0.0 all-gather.3.cloned.1.call-start
  6.5 0.7 reduce
  7.3 0.6 pad.4.b_ref
  7.9 2.0 %pad_maximum_fusion = bf16[2112,128]{1,0:T(8,128)(2,1)} fusion(bf16[704,128]{1,0:T(8,128)(2,1)} %bitcast.13, bf16[704,128]{1,0:T(8,128)(2,1)} %bitcast.14, bf16[704,128]{1,0:T(8,128)(2,1)} %bitcast.15), kind=kLoop, calls=%fused_computation.8 | loop fusion | flops 1622016 | bytes 1081344 | tf_op jit(solution)/shard_map/concatenate | solution.py:745
  9.8 26.0 %exchange.1 = (bf16[16,256,128]{2,1,0:T(8,128)(2,1)}, bf16[4,1024,128]{2,1,0:T(8,128)(2,1)}, bf16[4,1024,128]{2,1,0:T(8,128)(2,1)}, bf16[4,16,256]{2,1,0:T(8,128)(2,1)}) custom-call(bf16[1024,128]{1,0:T(8,128)(2,1)} %q_ref.1, bf16[1024,128]{1,0:T(8,128)(2,1)} %k_ref.3, bf16[1024,128]{1,0:T(8,128)(2,1)} %v_ref.3, bf16[16,256]{1,0:T(8,128)(2,1)} %pad.4.b_ref), custom_call_target="tpu_custom_call" | custom-call | flops 10000000000 | bytes 4194304 | tf_op jit(solution)/shard_map/exchange/pallas_call | solution.py:175
  35.8 0.0 all-gather.3.cloned.1.call-update
  35.9 45.5 %attention.1 = (bf16[16,256,128]{2,1,0:T(8,128)(2,1)}, f32[16,2,8,128]{3,2,1,0:T(8,128)}) custom-call(bf16[1024,128]{1,0:T(8,128)(2,1)} %k_ref.3, bf16[1024,128]{1,0:T(8,128)(2,1)} %v_ref.3, bf16[16,256]{1,0:T(8,128)(2,1)} %pad.4.b_ref, bf16[16,256,128]{2,1,0:T(8,128)(2,1)} %get-tuple-element.22.qs_ref, bf16[4,1024,128]{2,1,0:T(8,128)(2,1)} %get-tuple-element.23.ks_ref, ...), custom_call_target="tpu_custom_call" | custom-call | flops 11274289152 | bytes 4194304 | tf_op jit(solution)/shard_map/attention/pallas_call | solution.py:298
  81.4 27.7 %deliver.1 = (bf16[8,4,128,128]{3,2,1,0:T(8,128)(2,1)}, f32[8,4,8,128]{3,2,1,0:T(8,128)}) custom-call(bf16[16,256,128]{2,1,0:T(8,128)(2,1)} %get-tuple-element.26.o_ref, f32[16,2,8,128]{3,2,1,0:T(8,128)} %get-tuple-element.27.g_ref), custom_call_target="tpu_custom_call" | custom-call | flops 5000000000 | bytes 4194304 | tf_op jit(solution)/shard_map/deliver/pallas_call | solution.py:410
  109.1 0.0 copy-start.1
  109.1 1.0 slice.3
  110.1 0.1 broadcast_select_fusion
  110.3 0.1 exponential_select_fusion
  110.4 1.8 multiply_reduce_fusion
  112.2 0.2 copy.13
  112.4 0.0 copy-done.1
  112.4 0.0 copy-start.2
  112.5 3.0 %fusion.1 = (f32[128]{0:T(128)S(1)}, bf16[128,2048]{1,0:T(8,128)(2,1)S(1)}) fusion(bf16[128,1024]{0,1:T(8,128)(2,1)S(1)} %bitcast.12, bf16[1024,2048]{1,0:T(8,128)(2,1)} %param.17, bf16[128,2048]{1,0:T(8,128)(2,1)S(1)} %copy-done.1), kind=kOutput, calls=%fused_computation.5 | convolution fusion | flops 538443648 | bytes 5505536 | tf_op jit(solution)/shard_map/dot_general | solution.py:750
  115.5 0.0 copy-start
  115.5 0.8 copy-done
  116.3 0.0 copy-done.2
  116.3 1.0 fusion.3.n_ref
  117.3 5.0 %all-gather.3.cloned.1.call-done = bf16[33792,128]{1,0:T(8,128)(2,1)} async-done(((bf16[2112,128]{1,0:T(8,128)(2,1)}), bf16[33792,128]{1,0:T(8,128)(2,1)}) %all-gather.3.cloned.1.call-update) | async-done | bytes 8650768 | tf_op jit(solution)/shard_map/all_gather | solution.py:747
  122.3 57.8 %feed_forward.1 = bf16[128,2048]{1,0:T(8,128)(2,1)} custom-call(bf16[128,2048]{1,0:T(8,128)(2,1)} %fusion.3.n_ref, bf16[128,2048]{1,0:T(8,128)(2,1)} %copy-done, bf16[16,2112,128]{2,1,0:T(8,128)(2,1)} %bitcast.18, f32[3,704]{1,0:T(4,128)} %cg_ref.1, f32[3,704]{1,0:T(4,128)} %cv_ref.1), custom_call_target="tpu_custom_call" | custom-call | flops 8999999488 | bytes 12582912 | tf_op jit(solution)/shard_map/feed_forward/pallas_call | solution.py:696
  180.2 1.9 copy.15
  (6 shorter events, 0.1 us)
Async XLA Ops:
  6.5 115.8 %all-gather.3.cloned.1.call-start = ((), (), s32[]{:S(2)}) async-start(), calls=%async_computation | async-start | bytes 9191424 | tf_op jit(solution)/shard_map/all_gather | solution.py:747
  109.1 3.3 %copy-start.1 = (bf16[128,2048]{1,0:T(8,128)(2,1)S(1)}, bf16[128,2048]{1,0:T(8,128)(2,1)}, u32[]{:S(2)}) copy-start(bf16[128,2048]{1,0:T(8,128)(2,1)} %param.16) | copy-start | bytes 1572868
  112.4 3.9 %copy-start.2 = (f32[2048]{0:T(1024)S(1)}, f32[2048]{0:T(1024)}, u32[]{:S(2)}) copy-start(f32[2048]{0:T(1024)} %param.18) | copy-start | bytes 24580
  115.5 0.8 copy-start
Sparse Core Ops, SparseCore 0:
  36.0 86.3 all-gather.2

commit v5 on v4

v5 whole, which is shorter than its diff:
```python
import jax
import jax.numpy as jnp
from jax import lax
from jax.experimental import pallas as pl
from jax.experimental.pallas import tpu as pltpu
from jax.sharding import PartitionSpec as P

EPS = 1e-06
LOG2E = 1.4426950408889634
NT = (((1,), (1,)), ((), ()))
CHUNK = 256
PAD = 16
SIDE = 4
RIM = 16
VMEM = 67_000_000


def tri_matrix():
    rows = lax.broadcasted_iota(jnp.int32, (CHUNK, CHUNK), 0)
    cols = lax.broadcasted_iota(jnp.int32, (CHUNK, CHUNK), 1)
    return (rows > cols).astype(jnp.bfloat16), rows > cols


def visit_chunk(q, k, v, bias, tri, gone, acc, mask=None):
    scale = 128 ** (-0.5) * LOG2E
    s = lax.dot_general(q, k, NT, preferred_element_type=jnp.float32) * scale + bias
    if mask is not None:
        s = jnp.where(mask, s, -1e30)
    soft = jnp.maximum(jnp.log(1.0 + jnp.exp2(jnp.minimum(s, 126.0))) * LOG2E, s)
    behind = jnp.dot(soft.astype(jnp.bfloat16), tri, preferred_element_type=jnp.float32)
    stick = jnp.exp2((s - soft) - (behind + gone)).astype(jnp.bfloat16)
    acc = acc + jnp.dot(stick, v, preferred_element_type=jnp.float32)
    gone = gone + (behind[:, 0:1] + soft[:, 0:1])
    return gone, acc


def position():
    me = lax.axis_index("sp")
    return me, me // SIDE, me % SIDE


def owners_of(y):
    core = lax.axis_index("tp") % 2
    return 2 * ((y + core) % SIDE), 2 * ((y + core + 2) % SIDE) + 1


def place_of():
    me = lax.axis_index("tp")
    return me // 2, me % 2


def remote_copy(src, dst, send_sem, recv_sem, **where):
    return pltpu.make_async_remote_copy(
        src_ref=src,
        dst_ref=dst,
        send_sem=send_sem,
        recv_sem=recv_sem,
        device_id=where,
        device_id_type=pl.DeviceIdType.MESH,
    )


def arrived(dst, sem):
    pltpu.make_async_copy(dst, dst, sem).wait()


def meet(peers, extra=0):
    barrier = pltpu.get_barrier_semaphore()
    for where in peers:
        pl.semaphore_signal(barrier, inc=1, device_id=where, device_id_type=pl.DeviceIdType.MESH)
    pl.semaphore_wait(barrier, len(peers) + extra)


def attend_kernel(
    q_ref, k_ref, v_ref, b_ref, w_ref, os_ref, gs_ref, whole_ref,
    q_all, k_all, v_all, b_all, o_buf, g_buf, acc_ref, gone_ref,
    kv_send, kv_recv, kv_own, bias_send, bias_recv, bias_own, q_send, q_recv, q_own, z_send, z_recv,
    w1_send, w1_relay, w2_send, w2_relay, w_recv, w_own, o_send, o_recv,
):
    me, z, y = position()
    x, core = place_of()
    head = lax.axis_index("tp")
    rows, width = k_ref.shape
    quarter = rows // SIDE
    share = quarter // 2
    chunks = rows // CHUNK
    right = (y + 1) % SIDE
    left = (y + 3) % SIDE
    across = (y + 2) % SIDE
    row = z * SIDE
    owners = owners_of(y)
    tri, _ = tri_matrix()

    barrier = pltpu.get_barrier_semaphore()

    def greet(group, carry):
        for source in range(os_ref.shape[0]):
            of = (x - source % 2 - 2 * core + 2 * SIDE) % SIDE
            pl.semaphore_signal(
                barrier,
                inc=1,
                device_id={"sp": group * SIDE + of, "tp": source},
                device_id_type=pl.DeviceIdType.MESH,
            )
        return carry

    lax.fori_loop(0, z + 1, greet, 0)
    meet(
        [{"sp": row + (y + d) % SIDE} for d in (1, 2, 3)]
        + [{"sp": (z + d) % SIDE * SIDE + y} for d in (1, 2, 3)],
        2 * (SIDE * SIDE - row),
    )

    def hop(part, src_slot, to, lane):
        src = (k_ref, v_ref)[part] if src_slot is None else (k_all, v_all)[part].at[src_slot]
        slot = y if src_slot is None else src_slot
        return remote_copy(
            src,
            (k_all, v_all)[part].at[slot],
            kv_send.at[part, lane],
            kv_recv.at[part, slot],
            sp=row + to,
        )

    def kv_mine(part):
        return pltpu.make_async_copy(
            (k_ref, v_ref)[part], (k_all, v_all)[part].at[y], kv_own.at[part]
        )

    def bias_hop(d):
        return remote_copy(
            b_ref, b_all.at[y], bias_send.at[d], bias_recv.at[y], sp=row + (y + d) % SIDE
        )

    def q_source(of, half):
        return q_ref.at[pl.ds(pl.multiple_of(owners_of(of)[half] * share, share), share)]

    def q_mine(half):
        return pltpu.make_async_copy(
            q_source(y, half), q_all.at[me, pl.ds(half * share, share)], q_own.at[half]
        )

    def q_piece(d, half):
        of = (y + d) % SIDE
        return remote_copy(
            q_source(of, half),
            q_all.at[me, pl.ds(half * share, share)],
            q_send.at[d, half],
            q_recv.at[y, half],
            sp=row + of,
        )

    def q_down(dz):
        ours = q_all.at[pl.ds(pl.multiple_of(row, SIDE), SIDE)]
        return remote_copy(ours, ours, z_send.at[dz], z_recv.at[z], sp=row - dz * SIDE + y)

    bulk = w_ref.shape[0] // 2
    piece = bulk // 2
    steps = (0, 3, 1, 2)

    def w_axes(part):
        return (y, z) if part == 0 else (z, y)

    def w_index(part, c1, c2):
        return c2 * SIDE + c1 if part == 0 else c1 * SIDE + c2

    def w_rows(part, half):
        return pl.ds(part * bulk + half * piece, piece)

    def w_copy(part, half, c1, c2, own, to1, to2, send):
        slot = w_index(part, c1, c2)
        spot = whole_ref.at[slot, w_rows(part, half)]
        src = w_ref.at[w_rows(part, half)] if own else spot
        return remote_copy(
            src, spot, send, w_recv.at[part, slot, half], sp=w_index(part, to1, to2)
        )

    def w_first(part, way, half):
        c1, c2 = w_axes(part)
        to = (c1 + (1, 3)[way]) % SIDE
        return w_copy(part, half, c1, c2, True, to, c2, w1_send.at[part, way, half])

    def w_first_relay(part, way):
        c1, c2 = w_axes(part)
        source = (c1 + (3, 1)[way]) % SIDE
        to = (c1 + (1, 3)[way]) % SIDE
        return w_copy(part, way, source, c2, False, to, c2, w1_relay.at[part, way])

    def w_second(part, k, way, half):
        c1, c2 = w_axes(part)
        to = (c2 + (1, 3)[way]) % SIDE
        source = (c1 + steps[k]) % SIDE
        return w_copy(part, half, source, c2, k == 0, c1, to, w2_send.at[part, k, way, half])

    def w_second_relay(part, k, way):
        c1, c2 = w_axes(part)
        source = (c2 + (3, 1)[way]) % SIDE
        to = (c2 + (1, 3)[way]) % SIDE
        return w_copy(
            part, way, (c1 + steps[k]) % SIDE, source, False, c1, to, w2_relay.at[part, k, way]
        )

    def w_take(part, half, c1, c2):
        slot = w_index(part, c1, c2)
        arrived(whole_ref.at[slot, w_rows(part, half)], w_recv.at[part, slot, half])

    def w_mine():
        return pltpu.make_async_copy(w_ref, whole_ref.at[me], w_own)

    def w_stage(stage):
        for part in range(2):
            c1, c2 = w_axes(part)
            low, high, far = ((c1 + d) % SIDE for d in (3, 1, 2))
            if stage == 0:
                for half in range(2):
                    w_first(part, 0, half).start()
                    w_first(part, 1, 1 - half).start()
            elif stage == 1:
                for half in range(2):
                    w_second(part, 0, 0, half).start()
                    w_second(part, 0, 1, 1 - half).start()
            elif stage == 2:
                w_take(part, 0, low, c2)
                w_first_relay(part, 0).start()
                w_take(part, 1, high, c2)
                w_first_relay(part, 1).start()
            elif stage == 3:
                w_take(part, 1, low, c2)
                w_take(part, 0, high, c2)
                for k in (1, 2):
                    for half in range(2):
                        w_second(part, k, 0, half).start()
                        w_second(part, k, 1, 1 - half).start()
            elif stage == 4:
                for half in range(2):
                    w_take(part, half, far, c2)
                for half in range(2):
                    w_second(part, 3, 0, half).start()
                    w_second(part, 3, 1, 1 - half).start()
            elif stage < 9:
                k = stage - 5
                for way in range(2):
                    w_take(part, way, (c1 + steps[k]) % SIDE, (c2 + (3, 1)[way]) % SIDE)
                    w_second_relay(part, k, way).start()
            else:
                for k in range(SIDE):
                    source = (c1 + steps[k]) % SIDE
                    w_take(part, 1, source, (c2 + 3) % SIDE)
                    w_take(part, 0, source, (c2 + 1) % SIDE)
                    for half in range(2):
                        w_take(part, half, source, (c2 + 2) % SIDE)

    def w_sent():
        for part in range(2):
            for way in range(2):
                w_first_relay(part, way).wait_send()
                for half in range(2):
                    w_first(part, way, half).wait_send()
                for k in range(SIDE):
                    w_second_relay(part, k, way).wait_send()
                    for half in range(2):
                        w_second(part, k, way, half).wait_send()

    def out_pieces(block, half):
        src = o_buf.at[block, pl.ds(half * share, share)]
        return ((src, os_ref), (g_buf.at[block, half], gs_ref))

    def out_remote(block, half, part):
        src, dst = out_pieces(block, half)[part]
        return remote_copy(
            src,
            dst.at[head, z],
            o_send.at[part, block, half],
            o_recv.at[part, head, z],
            sp=block,
            tp=owners[half],
        )

    def out_local(block, half, part):
        src, dst = out_pieces(block, half)[part]
        return pltpu.make_async_copy(src, dst.at[head, z], o_recv.at[part, head, z])

    def for_outs(group, act, act_local):
        for m in range(SIDE):
            block = group * SIDE + m
            for half in range(2):
                mine = (block == me) & (owners[half] == head)
                if act_local is not None:

                    @pl.when(mine)
                    def _():
                        for part in range(2):
                            act_local(out_local(block, half, part))

                @pl.when(jnp.logical_not(mine))
                def _():
                    for part in range(2):
                        act(out_remote(block, half, part))

    def finish(group):
        acc = acc_ref[...]
        gone = gone_ref[...]
        for m in range(SIDE):
            here = slice(m * quarter, (m + 1) * quarter)
            o_buf[group * SIDE + m] = acc[here].astype(o_buf.dtype)
            turned = gone[here].T
            for half in range(2):
                g_buf[group * SIDE + m, half] = turned[0:8, half * 128 : (half + 1) * 128]
        for_outs(group, lambda copy: copy.start(), lambda copy: copy.start())

    for half in range(2):
        q_mine(half).start()
    for d in (2, 1, 3):
        for half in range(2):
            q_piece(d, half).start()
        bias_hop(d).start()
    hop(0, None, right, 0).start()
    hop(1, None, left, 0).start()
    hop(1, None, right, 1).start()
    hop(0, None, left, 1).start()
    for part in range(2):
        kv_mine(part).start()
    bias_mine = pltpu.make_async_copy(b_ref, b_all.at[y], bias_own)
    bias_mine.start()
    for half in range(2):
        q_mine(half).wait()
        for d in (1, 2, 3):
            slot = (y + d) % SIDE
            arrived(q_all.at[row + slot, pl.ds(half * share, share)], q_recv.at[slot, half])
    for dz in (2, 3, 1):

        @pl.when(z >= dz)
        def _():
            q_down(dz).start()

    arrived(k_all.at[left], kv_recv.at[0, left])
    hop(0, left, right, 2).start()
    arrived(v_all.at[right], kv_recv.at[1, right])
    hop(1, right, left, 2).start()
    w_stage(0)
    w_stage(1)
    w_mine().start()
    arrived(v_all.at[left], kv_recv.at[1, left])
    arrived(k_all.at[right], kv_recv.at[0, right])
    arrived(k_all.at[across], kv_recv.at[0, across])
    arrived(v_all.at[across], kv_recv.at[1, across])
    for part in range(2):
        kv_mine(part).wait()
    bias_mine.wait()
    for d in (1, 2, 3):
        slot = (y + d) % SIDE
        arrived(b_all.at[slot], bias_recv.at[slot])

    first, second = (owner * share for owner in owners)
    acc_ref[...] = jnp.zeros_like(acc_ref)
    gone_ref[...] = jnp.zeros_like(gone_ref)
    for j in range(SIDE - 1, -1, -1):
        low = j * quarter
        size = rows - low
        q = q_all[pl.ds(row + j, SIDE - j)].reshape(size, width)
        bias = b_all[j].astype(jnp.float32) * LOG2E
        acc = acc_ref[low:, :]
        gone = gone_ref[low:, 0:1]
        at_row = lax.broadcasted_iota(jnp.int32, (size, CHUNK), 0)
        col = lax.broadcasted_iota(jnp.int32, (size, CHUNK), 1)
        place = at_row + jnp.where(at_row < share, first, second - share)
        for c in range(chunks - 1, -1, -1):
            at = slice(c * CHUNK, (c + 1) * CHUNK)
            mask = (at_row >= quarter) | (col + c * CHUNK < place)
            gone, acc = visit_chunk(
                q, k_all[j, at, :], v_all[j, at, :], bias[c : c + 1, :], tri, gone, acc, mask
            )
        acc_ref[low:, :] = acc
        gone_ref[low:, :] = jnp.broadcast_to(gone, (size, 128))
    finish(z)
    w_stage(2)
    for other in range(1, SIDE):

        @pl.when(z < other)
        def _():
            arrived(q_all.at[pl.ds(other * SIDE, SIDE)], z_recv.at[other])

    def step(s, carry):
        group = z + 1 + s // SIDE
        j = SIDE - 1 - s % SIDE

        @pl.when(group < SIDE)
        def _():
            @pl.when(j == SIDE - 1)
            def _():
                acc_ref[...] = jnp.zeros_like(acc_ref)
                gone_ref[...] = jnp.zeros_like(gone_ref)

            q = q_all[pl.ds(group * SIDE, SIDE)].reshape(rows, width)
            bias = b_all[j].astype(jnp.float32) * LOG2E
            gone = gone_ref[:, 0:1]
            acc = acc_ref[...]
            for c in range(chunks - 1, -1, -1):
                at = slice(c * CHUNK, (c + 1) * CHUNK)
                gone, acc = visit_chunk(
                    q, k_all[j, at, :], v_all[j, at, :], bias[c : c + 1, :], tri, gone, acc
                )
            acc_ref[...] = acc
            gone_ref[...] = jnp.broadcast_to(gone, (rows, 128))

            @pl.when(j == 0)
            def _():
                finish(group)

        for stage, after in ((3, 0), (4, 1), (5, 2), (6, 4), (7, 6), (8, 8)):

            @pl.when(s == after)
            def _():
                w_stage(stage)

        return carry

    lax.fori_loop(0, (SIDE - 1) * SIDE, step, 0)

    def take(group, carry):
        for h in range(os_ref.shape[0]):
            for part in range(2):
                arrived((os_ref, gs_ref)[part].at[h, group], o_recv.at[part, h, group])
        return carry

    lax.fori_loop(0, z + 1, take, 0)
    w_stage(9)
    w_mine().wait()

    def sent(group, carry):
        for_outs(group, lambda copy: copy.wait_send(), None)
        return carry

    lax.fori_loop(z, SIDE, sent, 0)
    w_sent()
    hop(0, None, right, 0).wait_send()
    hop(1, None, left, 0).wait_send()
    hop(1, None, right, 1).wait_send()
    hop(0, None, left, 1).wait_send()
    hop(0, left, right, 2).wait_send()
    hop(1, right, left, 2).wait_send()
    for d in (1, 2, 3):
        bias_hop(d).wait_send()
        for half in range(2):
            q_piece(d, half).wait_send()
    for dz in (1, 2, 3):

        @pl.when(z >= dz)
        def _():
            q_down(dz).wait_send()


def attend(queries, keys, values, bias_rows, weights, heads):
    rows, width = queries.shape
    anywhere = pl.BlockSpec(memory_space=pl.ANY)
    vmem = pl.BlockSpec(memory_space=pltpu.VMEM)
    count = SIDE * SIDE
    quarter = rows // SIDE
    dma = pltpu.SemaphoreType.DMA
    bf16 = jnp.bfloat16
    return pl.pallas_call(
        attend_kernel,
        out_shape=(
            jax.ShapeDtypeStruct((heads, SIDE, quarter // 2, width), bf16),
            jax.ShapeDtypeStruct((heads, SIDE, 8, 128), jnp.float32),
            jax.ShapeDtypeStruct((count,) + weights.shape, bf16),
        ),
        in_specs=[anywhere, anywhere, anywhere, vmem, anywhere],
        out_specs=[vmem, vmem, anywhere],
        scratch_shapes=[
            pltpu.VMEM((count, quarter, width), bf16),
            pltpu.VMEM((SIDE, rows, width), bf16),
            pltpu.VMEM((SIDE, rows, width), bf16),
            pltpu.VMEM((SIDE,) + bias_rows.shape, bf16),
            pltpu.VMEM((count, quarter, width), bf16),
            pltpu.VMEM((count, 2, 8, 128), jnp.float32),
            pltpu.VMEM((rows, width), jnp.float32),
            pltpu.VMEM((rows, 128), jnp.float32),
            dma((2, 3)), dma((2, SIDE)), dma((2,)), dma((SIDE,)), dma((SIDE,)), dma(()),
            dma((SIDE, 2)), dma((SIDE, 2)), dma((2,)), dma((SIDE,)), dma((SIDE,)),
            dma((2, 2, 2)), dma((2, 2)), dma((2, SIDE, 2, 2)), dma((2, SIDE, 2)),
            dma((2, count, 2)), dma(()), dma((2, count, 2)), dma((2, heads, SIDE)),
        ],
        compiler_params=pltpu.CompilerParams(
            has_side_effects=True, collective_id=0, vmem_limit_bytes=VMEM
        ),
        cost_estimate=pl.CostEstimate(
            flops=14 * 6 * rows * rows * width, bytes_accessed=12 * 2**20, transcendentals=0
        ),
        name="attend",
    )(queries, keys, values, bias_rows, weights)


def combine(parts, logs):
    group = lax.axis_index("sp") // SIDE
    valid = jnp.arange(SIDE) <= group
    left = jnp.where(valid[None, :, None], logs[:, :, 0, :], 0.0)
    later = jnp.flip(jnp.cumsum(jnp.flip(left, 1), axis=1), 1) - left
    weight = jnp.where(valid[None, :, None], jnp.exp2(-later), 0.0)
    terms = jnp.where(valid[None, :, None, None], parts.astype(jnp.float32), 0.0)
    total = jnp.sum(terms * weight[..., None], axis=1)
    return total.transpose(1, 0, 2).reshape(total.shape[1], -1).astype(jnp.bfloat16)


def feed_forward_kernel(
    n_ref, m_ref, w_ref, cg_ref, cv_ref, out_ref,
    all_ref, rim_ref, up_ref, down_ref, gate_ref, value_ref, p_ref, twin_buf, sum_buf, relay_buf,
    ring_buf, w_sem, ring_send, ring_recv, twin_send, twin_recv, rim_send, rim_recv, own_sem,
    pair_send, pair_recv, relay_send, relay_recv, back_send, back_recv,
):
    x, core = place_of()
    block = lax.axis_index("sp")
    rows, depth = n_ref.shape
    part = rows // 2
    tile = 2 * rows
    units = down_ref.shape[0]
    shards = w_ref.shape[0]
    deep = depth // shards
    right = (x + 1) % SIDE
    left = (x + 3) % SIDE
    across = (x + 2) % SIDE
    other = 2 * x + 1 - core
    halves = (slice(0, part), slice(part, rows))

    def weight_copies(k):
        at = slice(k * deep, (k + 1) * deep)
        return (
            pltpu.make_async_copy(
                w_ref.at[k, pl.ds(0, 2 * units)], up_ref.at[:, at], w_sem.at[0, k]
            ),
            pltpu.make_async_copy(
                w_ref.at[k, pl.ds(2 * units, units)], down_ref.at[:, at], w_sem.at[1, k]
            ),
        )

    for k in range(shards):
        for copy in weight_copies(k):
            copy.start()

    def spot(chip, half, of_core):
        return all_ref.at[2 * chip + of_core, pl.ds(half * part, part)]

    def ring(chip, half, to, lane):
        src = n_ref.at[pl.ds(half * part, part)] if chip is None else spot(chip, half, core)
        chip = x if chip is None else chip
        return remote_copy(
            src,
            spot(chip, half, core),
            ring_send.at[lane, half],
            ring_recv.at[chip, half],
            tp=2 * to + core,
        )

    def twin(chip, half):
        src = n_ref.at[pl.ds(half * part, part)] if chip is None else spot(chip, half, core)
        chip = x if chip is None else chip
        return remote_copy(
            src, spot(chip, half, core), twin_send.at[chip, half], twin_recv.at[chip, half], tp=other
        )

    def rim(to):
        return remote_copy(
            n_ref.at[pl.ds(rows - RIM, RIM)], rim_ref, rim_send.at[to], rim_recv, sp=block + 1, tp=to
        )

    last = (x == SIDE - 1) & (core == 1) & (block < SIDE * SIDE - 1)
    barrier = pltpu.get_barrier_semaphore()

    @pl.when(block > 0)
    def _():
        pl.semaphore_signal(
            barrier,
            inc=1,
            device_id={"sp": block - 1, "tp": 2 * SIDE - 1},
            device_id_type=pl.DeviceIdType.MESH,
        )

    meet(
        [{"tp": 2 * right + core}, {"tp": 2 * left + core}, {"tp": other}],
        jnp.where(last, 2 * SIDE, 0),
    )
    own = pltpu.make_async_copy(n_ref, all_ref.at[2 * x + core], own_sem)
    ring(None, 0, right, 0).start()
    ring(None, 1, left, 1).start()
    ring(None, 1, right, 0).start()
    ring(None, 0, left, 1).start()
    own.start()
    for half in range(2):
        twin(None, half).start()

    @pl.when(last)
    def _():
        for to in range(2 * SIDE):
            rim(to).start()

    def up(rows_in, which):
        w = up_ref[which * units : (which + 1) * units, :]
        return lax.dot_general(rows_in, w, NT, preferred_element_type=jnp.float32)

    def project_up(chip):
        rows_in = all_ref[pl.ds(2 * chip, 2)].reshape(tile, depth)
        for which, ref in enumerate((gate_ref, value_ref)):
            ref[pl.ds(pl.multiple_of(chip * tile + RIM, RIM), tile), :] = up(rows_in, which)

    def conv(ref, taps, chip):
        window = ref[pl.ds(pl.multiple_of(chip * tile, tile), tile + RIM), :]
        return (
            taps[0:1, :] * window[RIM - 2 : RIM - 2 + tile]
            + taps[1:2, :] * window[RIM - 1 : RIM - 1 + tile]
            + taps[2:3, :] * window[RIM : RIM + tile]
        )

    def project_down(chip):
        gate = conv(gate_ref, cg_ref, chip)
        value = conv(value_ref, cv_ref, chip)
        hidden = (gate / (1.0 + jnp.exp(-gate)) * value).astype(jnp.bfloat16)
        down = jnp.dot(hidden, down_ref[...], preferred_element_type=jnp.float32)
        p_ref[pl.ds(2 * chip, 2)] = down.astype(p_ref.dtype).reshape(2, rows, depth)

    def twin_arrived(chip):
        for half in range(2):
            arrived(spot(chip, half, 1 - core), twin_recv.at[chip, half])

    for k in range(shards):
        weight_copies(k)[0].wait()
    own.wait()
    twin_arrived(x)
    project_up(x)
    arrived(spot(left, 0, core), ring_recv.at[left, 0])
    ring(left, 0, right, 2).start()
    twin(left, 0).start()
    arrived(spot(right, 1, core), ring_recv.at[right, 1])
    ring(right, 1, left, 2).start()
    twin(right, 1).start()

    @pl.when(block > 0)
    def _():
        arrived(rim_ref, rim_recv)
        for which, ref in enumerate((gate_ref, value_ref)):
            ref[0:RIM, :] = up(rim_ref[...], which)

    @pl.when(block == 0)
    def _():
        for ref in (gate_ref, value_ref):
            ref[0:RIM, :] = jnp.zeros((RIM, units), jnp.float32)

    for chip, half in ((left, 1), (right, 0)):
        arrived(spot(chip, half, core), ring_recv.at[chip, half])
        twin(chip, half).start()
    twin_arrived(right)
    project_up(right)
    twin_arrived(left)
    project_up(left)
    for half in range(2):
        arrived(spot(across, half, core), ring_recv.at[across, half])
        twin(across, half).start()
    for k in range(shards):
        weight_copies(k)[1].wait()

    def pair(chip):
        return remote_copy(
            p_ref.at[2 * chip + 1 - core],
            twin_buf.at[chip],
            pair_send.at[chip],
            pair_recv.at[chip],
            tp=other,
        )

    def pair_sum(chip, half):
        mine = p_ref[2 * chip + core, halves[half], :].astype(jnp.float32)
        return mine + twin_buf[chip, halves[half], :].astype(jnp.float32)

    def relay(side):
        return remote_copy(
            sum_buf.at[0, halves[side]],
            relay_buf.at[side],
            relay_send.at[side],
            relay_recv.at[side],
            tp=2 * (right, left)[side] + core,
        )

    def back(side, half):
        return remote_copy(
            sum_buf.at[1 + side, halves[half]],
            ring_buf.at[side, halves[half]],
            back_send.at[side, half],
            back_recv.at[side, half],
            tp=2 * (right, left)[side] + core,
        )

    def direct(side):
        to = (right, left)[side]
        half = 1 - side
        arrived(twin_buf.at[to], pair_recv.at[to])
        sum_buf[1 + side, halves[half], :] = pair_sum(to, half).astype(jnp.bfloat16)
        back(side, half).start()

    project_down(right)
    pair(right).start()
    project_down(x)
    pair(x).start()
    direct(0)
    twin_arrived(across)
    project_up(across)
    project_down(across)
    pair(across).start()
    arrived(twin_buf.at[across], pair_recv.at[across])
    for side in range(2):
        sum_buf[0, halves[side], :] = pair_sum(across, side).astype(jnp.bfloat16)
        relay(side).start()
    project_down(left)
    pair(left).start()
    direct(1)
    arrived(twin_buf.at[x], pair_recv.at[x])
    for side in range(2):
        to = (right, left)[side]
        arrived(relay_buf.at[side], relay_recv.at[side])
        total = pair_sum(to, side) + relay_buf[side].astype(jnp.float32)
        sum_buf[1 + side, halves[side], :] = total.astype(jnp.bfloat16)
        back(side, side).start()
    for half in range(2):
        total = m_ref[halves[half], :].astype(jnp.float32) + pair_sum(x, half)
        for side in (1 - half, half):
            arrived(ring_buf.at[side, halves[half]], back_recv.at[side, half])
            total = total + ring_buf[side, halves[half], :].astype(jnp.float32)
        out_ref[halves[half], :] = total.astype(out_ref.dtype)

    for half in range(2):
        ring(None, half, right, 0).wait_send()
        ring(None, half, left, 1).wait_send()
        twin(None, half).wait_send()
        for chip in (left, right, across):
            twin(chip, half).wait_send()
    ring(left, 0, right, 2).wait_send()
    ring(right, 1, left, 2).wait_send()

    @pl.when(last)
    def _():
        for to in range(2 * SIDE):
            rim(to).wait_send()

    for chip in range(SIDE):
        pair(chip).wait_send()
    for side in range(2):
        relay(side).wait_send()
        for half in range(2):
            back(side, half).wait_send()


def feed_forward(normed, middle, whole, conv_gate, conv_value):
    rows, depth = normed.shape
    units = conv_gate.shape[1]
    total = 2 * SIDE * rows
    vmem = pl.BlockSpec(memory_space=pltpu.VMEM)
    dma = pltpu.SemaphoreType.DMA
    bf16 = jnp.bfloat16
    return pl.pallas_call(
        feed_forward_kernel,
        out_shape=jax.ShapeDtypeStruct((rows, depth), bf16),
        in_specs=[vmem, vmem, pl.BlockSpec(memory_space=pl.ANY), vmem, vmem],
        out_specs=vmem,
        scratch_shapes=[
            pltpu.VMEM((2 * SIDE, rows, depth), bf16),
            pltpu.VMEM((RIM, depth), bf16),
            pltpu.VMEM((2 * units, depth), bf16),
            pltpu.VMEM((units, depth), bf16),
            pltpu.VMEM((RIM + total, units), jnp.float32),
            pltpu.VMEM((RIM + total, units), jnp.float32),
            pltpu.VMEM((2 * SIDE, rows, depth), bf16),
            pltpu.VMEM((SIDE, rows, depth), bf16),
            pltpu.VMEM((3, rows, depth), bf16),
            pltpu.VMEM((2, rows // 2, depth), bf16),
            pltpu.VMEM((2, rows, depth), bf16),
            dma((2, whole.shape[0])),
            dma((3, 2)), dma((SIDE, 2)), dma((SIDE, 2)), dma((SIDE, 2)), dma((2 * SIDE,)), dma(()), dma(()),
            dma((SIDE,)), dma((SIDE,)), dma((2,)), dma((2,)), dma((2, 2)), dma((2, 2)),
        ],
        compiler_params=pltpu.CompilerParams(
            has_side_effects=True, collective_id=1, vmem_limit_bytes=VMEM
        ),
        cost_estimate=pl.CostEstimate(
            flops=9 * 10**9, bytes_accessed=12 * 2**20, transcendentals=0
        ),
        name="feed_forward",
    )(normed, middle, whole, conv_gate, conv_value)


def local(
    queries,
    keys,
    values,
    stick_bias,
    residual,
    out_weight,
    norm_gain,
    gate_weight,
    value_weight,
    down_weight,
    conv_gate,
    conv_value,
):
    rows_here = queries.shape[0]
    model_width = residual.shape[1]
    bias_rows = stick_bias.reshape(rows_here // CHUNK, CHUNK)
    bias_rows = jnp.pad(bias_rows, ((0, PAD - bias_rows.shape[0]), (0, 0)))
    weights = jnp.concatenate([gate_weight.T, value_weight.T, down_weight.T], axis=0)
    parts, logs, whole = attend(
        queries, keys, values, bias_rows, weights, lax.axis_size("tp")
    )
    row_heads = combine(parts, logs)
    projected = jnp.dot(row_heads, out_weight, preferred_element_type=jnp.float32)
    middle = (residual.astype(jnp.float32) + projected).astype(jnp.bfloat16)
    middle_f = middle.astype(jnp.float32)
    normed = (
        middle_f
        * lax.rsqrt(jnp.mean(middle_f * middle_f, axis=-1, keepdims=True) + EPS)
        * norm_gain
    ).astype(jnp.bfloat16)
    return feed_forward(normed, middle, whole, conv_gate, conv_value)


def solution(mesh):
    in_specs = (
        P("sp", "tp"),
        P("sp", "tp"),
        P("sp", "tp"),
        P("sp", "tp"),
        P(("sp", "tp"), None),
        P(),
        P(),
        P("sp", "tp"),
        P("sp", "tp"),
        P("sp", "tp"),
        P(None, "tp"),
        P(None, "tp"),
    )
    out_specs = P(("sp", "tp"), None)
    return jax.shard_map(local, mesh=mesh, in_specs=in_specs, out_specs=out_specs, check_vma=False)
```

time: 191 us -> 162 us (0.85)
  between operations: 13.5 us -> 0.11 us
  Pallas kernels: 157 us -> 146 us
  waiting for transfers between devices: 5.02 us -> 0 us
    pallas_call x3 -> x1, Pallas kernels: 99.2 us -> 86.9 us  [attend(): pl.pallas_call(attend_kernel, out_shape=(jax.ShapeDtypeStruct((heads, SID...]
    all_gather x1 -> x0, waiting for transfers between devices: 5 us -> none  [local(): whole = lax.all_gather(weights, 'sp', axis=0, tiled=False)]
  transfers between devices with their start and end apart: 1 -> 0, of which waited for: 1 -> 0; matrix products, arithmetic and copies ran while one was open for 4% -> 0% of each run, Pallas kernels for 39% -> 0%
where the time goes in v5:
time: 162 us; the launch traced here: 159 us
  Pallas kernels  146 us (90%)
  other arithmetic  5.67 us (4%)
  local copies, waits for them, and re-layouts  4.57 us (3%)
  matrix products  3.04 us (2%)
    pallas_call x1, Pallas kernels, attend(): pl.pallas_call(attend_kernel, out_shape=(jax.ShapeDtypeStruct((heads, SID...  86.9 us
    pallas_call x1, Pallas kernels, feed_forward(): pl.pallas_call(feed_forward_kernel, out_shape=jax.ShapeDtypeStruct((rows,...  58.7 us

profile of v5, /device:TPU:26, one launch (start us, length us, event | category | flops | bytes accessed | tf_op | source)
XLA Modules:
  0.0 159.0 jit_solution(6147265056038081343)
XLA Ops:
  0.0 0.7 reduce
  0.7 0.6 pad.4.b_ref
  1.3 1.9 %pad_maximum_fusion.w_ref = bf16[2112,128]{1,0:T(8,128)(2,1)} fusion(bf16[704,128]{1,0:T(8,128)(2,1)} %bitcast.12, bf16[704,128]{1,0:T(8,128)(2,1)} %bitcast.13, bf16[704,128]{1,0:T(8,128)(2,1)} %bitcast.14), kind=kLoop, calls=%fused_computation.8 | loop fusion | flops 1622016 | bytes 1081344 | tf_op jit(solution)/shard_map/concatenate | solution.py:806
  3.3 86.9 %attend.1 = (bf16[8,4,128,128]{3,2,1,0:T(8,128)(2,1)}, f32[8,4,8,128]{3,2,1,0:T(8,128)}, bf16[16,2112,128]{2,1,0:T(8,128)(2,1)}) custom-call(bf16[1024,128]{1,0:T(8,128)(2,1)} %q_ref.1, bf16[1024,128]{1,0:T(8,128)(2,1)} %k_ref.1, bf16[1024,128]{1,0:T(8,128)(2,1)} %v_ref.1, bf16[16,256]{1,0:T(8,128)(2,1)} %pad.4.b_ref, bf16[2112,128]{1,0:T(8,128)(2,1)} %pad_maximum_fusion.w_ref), custom_call_target="tpu_custom_call" | custom-call | flops 11274289152 | bytes 12582912 | tf_op jit(solution)/shard_map/attend/pallas_call | solution.py:461
  90.2 0.0 copy-start.1
  90.2 1.0 slice.3
  91.2 0.1 broadcast_select_fusion
  91.4 0.1 exponential_select_fusion
  91.5 1.8 %multiply_reduce_fusion = bf16[8,128,128]{2,1,0:T(8,128)(2,1)S(1)} fusion(bf16[8,4,128,128]{3,2,1,0:T(8,128)(2,1)} %get-tuple-element.8, f32[8,4,128]{2,1,0:T(4,128)S(1)} %exponential_select_fusion, pred[4]{0:T(512)(128)(4,1)S(1)} %iota_compare_fusion), kind=kLoop, calls=%fused_computation.2 | loop fusion | flops 1966080 | bytes 1327108 | tf_op jit(solution)/shard_map/reduce_sum | solution.py:501
  93.3 0.2 copy.13
  93.5 0.0 copy-done.1
  93.5 0.0 copy-start.2
  93.5 3.0 %fusion.1 = (f32[128]{0:T(128)S(1)}, bf16[128,2048]{1,0:T(8,128)(2,1)S(1)}) fusion(bf16[128,1024]{0,1:T(8,128)(2,1)S(1)} %bitcast.11, bf16[1024,2048]{1,0:T(8,128)(2,1)} %param.17, bf16[128,2048]{1,0:T(8,128)(2,1)S(1)} %copy-done.1), kind=kOutput, calls=%fused_computation.5 | convolution fusion | flops 538443648 | bytes 5505536 | tf_op jit(solution)/shard_map/dot_general | solution.py:811
  96.6 0.0 copy-start
  96.6 0.8 copy-done
  97.4 0.0 copy-done.2
  97.4 1.0 fusion.3.n_ref
  98.4 58.7 %feed_forward.1 = bf16[128,2048]{1,0:T(8,128)(2,1)} custom-call(bf16[128,2048]{1,0:T(8,128)(2,1)} %fusion.3.n_ref, bf16[128,2048]{1,0:T(8,128)(2,1)} %copy-done, bf16[16,2112,128]{2,1,0:T(8,128)(2,1)} %get-tuple-element.10.w_ref, f32[3,704]{1,0:T(4,128)} %cg_ref.1, f32[3,704]{1,0:T(4,128)} %cv_ref.1), custom_call_target="tpu_custom_call" | custom-call | flops 8999999488 | bytes 12582912 | tf_op jit(solution)/shard_map/feed_forward/pallas_call | solution.py:757
  157.1 1.9 %copy.15 = bf16[128,2048]{1,0:T(8,128)(2,1)} copy(bf16[128,2048]{1,0:T(8,128)(2,1)} %feed_forward.1) | data formatting | bytes 1048576
  (6 shorter events, 0.1 us)
Async XLA Ops:
  90.2 3.3 %copy-start.1 = (bf16[128,2048]{1,0:T(8,128)(2,1)S(1)}, bf16[128,2048]{1,0:T(8,128)(2,1)}, u32[]{:S(2)}) copy-start(bf16[128,2048]{1,0:T(8,128)(2,1)} %param.16) | copy-start | bytes 1572868
  93.5 3.9 %copy-start.2 = (f32[2048]{0:T(1024)S(1)}, f32[2048]{0:T(1024)}, u32[]{:S(2)}) copy-start(f32[2048]{0:T(1024)} %param.18) | copy-start | bytes 24580
  96.6 0.8 copy-start

commit v6 on v5

--- a/solution.py
+++ b/solution.py
@@ -13,6 +13,10 @@
 SIDE = 4
 RIM = 16
 VMEM = 67_000_000
+ATTEND = 28
+STAGES = (
+    (0, 0, 3), (1, 0, 4), (2, 0, 5), (3, 0, 6), (4, 0, 7), (6, 0, 8), (11, 1, 0), (11, 1, 1),
+)
 
 
 def tri_matrix():
@@ -71,11 +75,11 @@
     pl.semaphore_wait(barrier, len(peers) + extra)
 
 
-def attend_kernel(
+def attend_part(
     q_ref, k_ref, v_ref, b_ref, w_ref, os_ref, gs_ref, whole_ref,
-    q_all, k_all, v_all, b_all, o_buf, g_buf, acc_ref, gone_ref,
+    q_all, k_all, v_all, b_all, o_buf, g_buf, acc_ref, gone_ref, block_out, block_gone,
     kv_send, kv_recv, kv_own, bias_send, bias_recv, bias_own, q_send, q_recv, q_own, z_send, z_recv,
-    w1_send, w1_relay, w2_send, w2_relay, w_recv, w_own, o_send, o_recv,
+    w1_send, w1_relay, w2_send, w2_relay, w_recv, o_send, o_recv,
 ):
     me, z, y = position()
     x, core = place_of()
@@ -105,10 +109,23 @@
         return carry
 
     lax.fori_loop(0, z + 1, greet, 0)
+
+    @pl.when(me > 0)
+    def _():
+        pl.semaphore_signal(
+            barrier,
+            inc=1,
+            device_id={"sp": me - 1, "tp": 2 * SIDE - 1},
+            device_id_type=pl.DeviceIdType.MESH,
+        )
+
     meet(
         [{"sp": row + (y + d) % SIDE} for d in (1, 2, 3)]
-        + [{"sp": (z + d) % SIDE * SIDE + y} for d in (1, 2, 3)],
-        2 * (SIDE * SIDE - row),
+        + [{"sp": (z + d) % SIDE * SIDE + y} for d in (1, 2, 3)]
+        + [{"tp": 2 * ((x + d) % SIDE) + core} for d in (1, 3)]
+        + [{"tp": 2 * x + 1 - core}],
+        2 * (SIDE * SIDE - row)
+        + jnp.where((head == 2 * SIDE - 1) & (me < SIDE * SIDE - 1), 2 * SIDE, 0),
     )
 
     def hop(part, src_slot, to, lane):
@@ -154,8 +171,9 @@
         ours = q_all.at[pl.ds(pl.multiple_of(row, SIDE), SIDE)]
         return remote_copy(ours, ours, z_send.at[dz], z_recv.at[z], sp=row - dz * SIDE + y)
 
-    bulk = w_ref.shape[0] // 2
-    piece = bulk // 2
+    third = w_ref.shape[0] // 3
+    starts = (0, 2 * third)
+    bulks = (third, third // 2)
     steps = (0, 3, 1, 2)
 
     def w_axes(part):
@@ -164,102 +182,116 @@
     def w_index(part, c1, c2):
         return c2 * SIDE + c1 if part == 0 else c1 * SIDE + c2
 
-    def w_rows(part, half):
-        return pl.ds(part * bulk + half * piece, piece)
-
-    def w_copy(part, half, c1, c2, own, to1, to2, send):
+    def w_rows(batch, part, half):
+        piece = bulks[batch] // 2
+        return pl.ds(starts[batch] + (2 * part + half) * piece, piece)
+
+    def w_copy(batch, part, half, c1, c2, own, to1, to2, send):
         slot = w_index(part, c1, c2)
-        spot = whole_ref.at[slot, w_rows(part, half)]
-        src = w_ref.at[w_rows(part, half)] if own else spot
-        return remote_copy(
-            src, spot, send, w_recv.at[part, slot, half], sp=w_index(part, to1, to2)
-        )
-
-    def w_first(part, way, half):
+        spot = whole_ref.at[slot, w_rows(batch, part, half)]
+        src = w_ref.at[w_rows(batch, part, half)] if own else spot
+        return remote_copy(
+            src, spot, send, w_recv.at[batch, part, slot, half], sp=w_index(part, to1, to2)
+        )
+
+    def w_first(batch, part, way, half):
         c1, c2 = w_axes(part)
         to = (c1 + (1, 3)[way]) % SIDE
-        return w_copy(part, half, c1, c2, True, to, c2, w1_send.at[part, way, half])
-
-    def w_first_relay(part, way):
+        return w_copy(batch, part, half, c1, c2, True, to, c2, w1_send.at[batch, part, way, half])
+
+    def w_first_relay(batch, part, way):
         c1, c2 = w_axes(part)
         source = (c1 + (3, 1)[way]) % SIDE
         to = (c1 + (1, 3)[way]) % SIDE
-        return w_copy(part, way, source, c2, False, to, c2, w1_relay.at[part, way])
-
-    def w_second(part, k, way, half):
+        return w_copy(batch, part, way, source, c2, False, to, c2, w1_relay.at[batch, part, way])
+
+    def w_second(batch, part, k, way, half):
         c1, c2 = w_axes(part)
         to = (c2 + (1, 3)[way]) % SIDE
         source = (c1 + steps[k]) % SIDE
-        return w_copy(part, half, source, c2, k == 0, c1, to, w2_send.at[part, k, way, half])
-
-    def w_second_relay(part, k, way):
+        return w_copy(batch, part, half, source, c2, k == 0, c1, to, w2_send.at[batch, part, k, way, half])
+
+    def w_second_relay(batch, part, k, way):
         c1, c2 = w_axes(part)
         source = (c2 + (3, 1)[way]) % SIDE
         to = (c2 + (1, 3)[way]) % SIDE
         return w_copy(
-            part, way, (c1 + steps[k]) % SIDE, source, False, c1, to, w2_relay.at[part, k, way]
-        )
-
-    def w_take(part, half, c1, c2):
+            batch, part, way, (c1 + steps[k]) % SIDE, source, False, c1, to, w2_relay.at[batch, part, k, way]
+        )
+
+    def w_take(batch, part, half, c1, c2):
         slot = w_index(part, c1, c2)
-        arrived(whole_ref.at[slot, w_rows(part, half)], w_recv.at[part, slot, half])
-
-    def w_mine():
-        return pltpu.make_async_copy(w_ref, whole_ref.at[me], w_own)
-
-    def w_stage(stage):
-        for part in range(2):
-            c1, c2 = w_axes(part)
-            low, high, far = ((c1 + d) % SIDE for d in (3, 1, 2))
-            if stage == 0:
+        arrived(whole_ref.at[slot, w_rows(batch, part, half)], w_recv.at[batch, part, slot, half])
+
+    def w_near(part):
+        c1, c2 = w_axes(part)
+        return (c1 + 3) % SIDE, (c1 + 1) % SIDE, (c1 + 2) % SIDE, c2
+
+    def w_own(batch, first_part):
+        for half in range(2):
+            for way in range(2):
+                of = (half + way) % 2
+                w_first(batch, first_part, way, of).start()
+                w_second(batch, 1 - first_part, 0, way, of).start()
+
+    def w_stage(batch, stage):
+        if stage == 0:
+            w_own(batch, 0)
+        elif stage == 1:
+            w_own(batch, 1)
+        elif stage == 2:
+            for way in range(2):
+                for part in (1, 0):
+                    near = w_near(part)
+                    w_take(batch, part, way, near[way], near[3])
+                    w_first_relay(batch, part, way).start()
+        elif stage == 3:
+            for part in (1, 0):
+                near = w_near(part)
+                for way in range(2):
+                    w_take(batch, part, 1 - way, near[way], near[3])
+            for half in range(2):
+                for k in (1, 2):
+                    for way in range(2):
+                        for part in (1, 0):
+                            w_second(batch, part, k, way, (half + way) % 2).start()
+        elif stage == 4:
+            for part in (1, 0):
+                near = w_near(part)
                 for half in range(2):
-                    w_first(part, 0, half).start()
-                    w_first(part, 1, 1 - half).start()
-            elif stage == 1:
-                for half in range(2):
-                    w_second(part, 0, 0, half).start()
-                    w_second(part, 0, 1, 1 - half).start()
-            elif stage == 2:
-                w_take(part, 0, low, c2)
-                w_first_relay(part, 0).start()
-                w_take(part, 1, high, c2)
-                w_first_relay(part, 1).start()
-            elif stage == 3:
-                w_take(part, 1, low, c2)
-                w_take(part, 0, high, c2)
-                for k in (1, 2):
-                    for half in range(2):
-                        w_second(part, k, 0, half).start()
-                        w_second(part, k, 1, 1 - half).start()
-            elif stage == 4:
-                for half in range(2):
-                    w_take(part, half, far, c2)
-                for half in range(2):
-                    w_second(part, 3, 0, half).start()
-                    w_second(part, 3, 1, 1 - half).start()
-            elif stage < 9:
-                k = stage - 5
+                    w_take(batch, part, half, near[2], near[3])
+            for half in range(2):
                 for way in range(2):
-                    w_take(part, way, (c1 + steps[k]) % SIDE, (c2 + (3, 1)[way]) % SIDE)
-                    w_second_relay(part, k, way).start()
-            else:
+                    for part in (1, 0):
+                        w_second(batch, part, 3, way, (half + way) % 2).start()
+        elif stage < 9:
+            k = stage - 5
+            for way in range(2):
+                for part in (1, 0):
+                    c1, c2 = w_axes(part)
+                    w_take(batch, part, way, (c1 + steps[k]) % SIDE, (c2 + (3, 1)[way]) % SIDE)
+                    w_second_relay(batch, part, k, way).start()
+        else:
+            for part in range(2):
+                c1, c2 = w_axes(part)
                 for k in range(SIDE):
                     source = (c1 + steps[k]) % SIDE
-                    w_take(part, 1, source, (c2 + 3) % SIDE)
-                    w_take(part, 0, source, (c2 + 1) % SIDE)
+                    w_take(batch, part, 1, source, (c2 + 3) % SIDE)
+                    w_take(batch, part, 0, source, (c2 + 1) % SIDE)
                     for half in range(2):
-                        w_take(part, half, source, (c2 + 2) % SIDE)
+                        w_take(batch, part, half, source, (c2 + 2) % SIDE)
 
     def w_sent():
-        for part in range(2):
-            for way in range(2):
-                w_first_relay(part, way).wait_send()
-                for half in range(2):
-                    w_first(part, way, half).wait_send()
-                for k in range(SIDE):
-                    w_second_relay(part, k, way).wait_send()
+        for batch in range(2):
+            for part in range(2):
+                for way in range(2):
+                    w_first_relay(batch, part, way).wait_send()
                     for half in range(2):
-                        w_second(part, k, way, half).wait_send()
+                        w_first(batch, part, way, half).wait_send()
+                    for k in range(SIDE):
+                        w_second_relay(batch, part, k, way).wait_send()
+                        for half in range(2):
+                            w_second(batch, part, k, way, half).wait_send()
 
     def out_pieces(block, half):
         src = o_buf.at[block, pl.ds(half * share, share)]
@@ -308,6 +340,7 @@
                 g_buf[group * SIDE + m, half] = turned[0:8, half * 128 : (half + 1) * 128]
         for_outs(group, lambda copy: copy.start(), lambda copy: copy.start())
 
+    w_stage(0, 1)
     for half in range(2):
         q_mine(half).start()
     for d in (2, 1, 3):
@@ -322,58 +355,83 @@
         kv_mine(part).start()
     bias_mine = pltpu.make_async_copy(b_ref, b_all.at[y], bias_own)
     bias_mine.start()
-    for half in range(2):
-        q_mine(half).wait()
-        for d in (1, 2, 3):
-            slot = (y + d) % SIDE
-            arrived(q_all.at[row + slot, pl.ds(half * share, share)], q_recv.at[slot, half])
-    for dz in (2, 3, 1):
-
-        @pl.when(z >= dz)
+
+    first, second = (owner * share for owner in owners)
+    at_row = lax.broadcasted_iota(jnp.int32, (rows, CHUNK), 0)
+    col = lax.broadcasted_iota(jnp.int32, (rows, CHUNK), 1)
+    inside = at_row % quarter
+    place = (
+        at_row // quarter * rows
+        + inside
+        + jnp.where(inside < share, first, second - share)
+        - col
+    )
+
+    def diagonal(i, carry):
+        j = (y + jnp.where(i == 0, 0, jnp.where(i == 1, 3, i - 1))) % SIDE
+
+        @pl.when(i == 0)
         def _():
-            q_down(dz).start()
-
-    arrived(k_all.at[left], kv_recv.at[0, left])
-    hop(0, left, right, 2).start()
-    arrived(v_all.at[right], kv_recv.at[1, right])
-    hop(1, right, left, 2).start()
-    w_stage(0)
-    w_stage(1)
-    w_mine().start()
-    arrived(v_all.at[left], kv_recv.at[1, left])
-    arrived(k_all.at[right], kv_recv.at[0, right])
-    arrived(k_all.at[across], kv_recv.at[0, across])
-    arrived(v_all.at[across], kv_recv.at[1, across])
-    for part in range(2):
-        kv_mine(part).wait()
-    bias_mine.wait()
-    for d in (1, 2, 3):
-        slot = (y + d) % SIDE
-        arrived(b_all.at[slot], bias_recv.at[slot])
-
-    first, second = (owner * share for owner in owners)
-    acc_ref[...] = jnp.zeros_like(acc_ref)
-    gone_ref[...] = jnp.zeros_like(gone_ref)
-    for j in range(SIDE - 1, -1, -1):
-        low = j * quarter
-        size = rows - low
-        q = q_all[pl.ds(row + j, SIDE - j)].reshape(size, width)
+            for half in range(2):
+                q_mine(half).wait()
+                for d in (1, 2, 3):
+                    slot = (y + d) % SIDE
+                    arrived(q_all.at[row + slot, pl.ds(half * share, share)], q_recv.at[slot, half])
+            for dz in (2, 3, 1):
+
+                @pl.when(z >= dz)
+                def _():
+                    q_down(dz).start()
+
+            for part in range(2):
+                kv_mine(part).wait()
+            bias_mine.wait()
+
+        @pl.when(i == 1)
+        def _():
+            arrived(k_all.at[left], kv_recv.at[0, left])
+            hop(0, left, right, 2).start()
+            arrived(v_all.at[right], kv_recv.at[1, right])
+            hop(1, right, left, 2).start()
+            w_stage(0, 0)
+            arrived(v_all.at[left], kv_recv.at[1, left])
+            arrived(b_all.at[left], bias_recv.at[left])
+
+        @pl.when(i == 2)
+        def _():
+            arrived(k_all.at[right], kv_recv.at[0, right])
+            arrived(b_all.at[right], bias_recv.at[right])
+
+        @pl.when(i == 3)
+        def _():
+            arrived(k_all.at[across], kv_recv.at[0, across])
+            arrived(v_all.at[across], kv_recv.at[1, across])
+            arrived(b_all.at[across], bias_recv.at[across])
+
+        q = q_all[pl.ds(row, SIDE)].reshape(rows, width)
         bias = b_all[j].astype(jnp.float32) * LOG2E
-        acc = acc_ref[low:, :]
-        gone = gone_ref[low:, 0:1]
-        at_row = lax.broadcasted_iota(jnp.int32, (size, CHUNK), 0)
-        col = lax.broadcasted_iota(jnp.int32, (size, CHUNK), 1)
-        place = at_row + jnp.where(at_row < share, first, second - share)
+        gone = jnp.zeros((rows, 1), jnp.float32)
+        acc = jnp.zeros((rows, width), jnp.float32)
         for c in range(chunks - 1, -1, -1):
             at = slice(c * CHUNK, (c + 1) * CHUNK)
-            mask = (at_row >= quarter) | (col + c * CHUNK < place)
+            mask = place > j * rows + c * CHUNK
             gone, acc = visit_chunk(
                 q, k_all[j, at, :], v_all[j, at, :], bias[c : c + 1, :], tri, gone, acc, mask
             )
-        acc_ref[low:, :] = acc
-        gone_ref[low:, :] = jnp.broadcast_to(gone, (size, 128))
+        block_out[j] = acc
+        block_gone[j] = jnp.broadcast_to(gone, (rows, 128))
+        return carry
+
+    lax.fori_loop(0, SIDE, diagonal, 0)
+    gone = block_gone[SIDE - 1]
+    acc = block_out[SIDE - 1]
+    for j in range(SIDE - 2, -1, -1):
+        acc = acc + jnp.exp2(-gone) * block_out[j]
+        gone = gone + block_gone[j]
+    acc_ref[...] = acc
+    gone_ref[...] = gone
     finish(z)
-    w_stage(2)
+    w_stage(0, 2)
     for other in range(1, SIDE):
 
         @pl.when(z < other)
@@ -407,11 +465,11 @@
             def _():
                 finish(group)
 
-        for stage, after in ((3, 0), (4, 1), (5, 2), (6, 4), (7, 6), (8, 8)):
+        for after, batch, stage in STAGES:
 
             @pl.when(s == after)
             def _():
-                w_stage(stage)
+                w_stage(batch, stage)
 
         return carry
 
@@ -424,86 +482,40 @@
         return carry
 
     lax.fori_loop(0, z + 1, take, 0)
-    w_stage(9)
-    w_mine().wait()
-
-    def sent(group, carry):
-        for_outs(group, lambda copy: copy.wait_send(), None)
-        return carry
-
-    lax.fori_loop(z, SIDE, sent, 0)
-    w_sent()
-    hop(0, None, right, 0).wait_send()
-    hop(1, None, left, 0).wait_send()
-    hop(1, None, right, 1).wait_send()
-    hop(0, None, left, 1).wait_send()
-    hop(0, left, right, 2).wait_send()
-    hop(1, right, left, 2).wait_send()
-    for d in (1, 2, 3):
-        bias_hop(d).wait_send()
-        for half in range(2):
-            q_piece(d, half).wait_send()
-    for dz in (1, 2, 3):
-
-        @pl.when(z >= dz)
-        def _():
-            q_down(dz).wait_send()
-
-
-def attend(queries, keys, values, bias_rows, weights, heads):
-    rows, width = queries.shape
-    anywhere = pl.BlockSpec(memory_space=pl.ANY)
-    vmem = pl.BlockSpec(memory_space=pltpu.VMEM)
-    count = SIDE * SIDE
-    quarter = rows // SIDE
-    dma = pltpu.SemaphoreType.DMA
-    bf16 = jnp.bfloat16
-    return pl.pallas_call(
-        attend_kernel,
-        out_shape=(
-            jax.ShapeDtypeStruct((heads, SIDE, quarter // 2, width), bf16),
-            jax.ShapeDtypeStruct((heads, SIDE, 8, 128), jnp.float32),
-            jax.ShapeDtypeStruct((count,) + weights.shape, bf16),
-        ),
-        in_specs=[anywhere, anywhere, anywhere, vmem, anywhere],
-        out_specs=[vmem, vmem, anywhere],
-        scratch_shapes=[
-            pltpu.VMEM((count, quarter, width), bf16),
-            pltpu.VMEM((SIDE, rows, width), bf16),
-            pltpu.VMEM((SIDE, rows, width), bf16),
-            pltpu.VMEM((SIDE,) + bias_rows.shape, bf16),
-            pltpu.VMEM((count, quarter, width), bf16),
-            pltpu.VMEM((count, 2, 8, 128), jnp.float32),
-            pltpu.VMEM((rows, width), jnp.float32),
-            pltpu.VMEM((rows, 128), jnp.float32),
-            dma((2, 3)), dma((2, SIDE)), dma((2,)), dma((SIDE,)), dma((SIDE,)), dma(()),
-            dma((SIDE, 2)), dma((SIDE, 2)), dma((2,)), dma((SIDE,)), dma((SIDE,)),
-            dma((2, 2, 2)), dma((2, 2)), dma((2, SIDE, 2, 2)), dma((2, SIDE, 2)),
-            dma((2, count, 2)), dma(()), dma((2, count, 2)), dma((2, heads, SIDE)),
-        ],
-        compiler_params=pltpu.CompilerParams(
-            has_side_effects=True, collective_id=0, vmem_limit_bytes=VMEM
-        ),
-        cost_estimate=pl.CostEstimate(
-            flops=14 * 6 * rows * rows * width, bytes_accessed=12 * 2**20, transcendentals=0
-        ),
-        name="attend",
-    )(queries, keys, values, bias_rows, weights)
-
-
-def combine(parts, logs):
-    group = lax.axis_index("sp") // SIDE
-    valid = jnp.arange(SIDE) <= group
-    left = jnp.where(valid[None, :, None], logs[:, :, 0, :], 0.0)
-    later = jnp.flip(jnp.cumsum(jnp.flip(left, 1), axis=1), 1) - left
-    weight = jnp.where(valid[None, :, None], jnp.exp2(-later), 0.0)
-    terms = jnp.where(valid[None, :, None, None], parts.astype(jnp.float32), 0.0)
-    total = jnp.sum(terms * weight[..., None], axis=1)
-    return total.transpose(1, 0, 2).reshape(total.shape[1], -1).astype(jnp.bfloat16)
-
-
-def feed_forward_kernel(
-    n_ref, m_ref, w_ref, cg_ref, cv_ref, out_ref,
+    def up_weights():
+        w_stage(0, 9)
+
+    def down_weights(stage):
+        w_stage(1, stage)
+
+    def all_sent():
+        def sent(group, carry):
+            for_outs(group, lambda copy: copy.wait_send(), None)
+            return carry
+
+        lax.fori_loop(z, SIDE, sent, 0)
+        w_sent()
+        hop(0, None, right, 0).wait_send()
+        hop(1, None, left, 0).wait_send()
+        hop(1, None, right, 1).wait_send()
+        hop(0, None, left, 1).wait_send()
+        hop(0, left, right, 2).wait_send()
+        hop(1, right, left, 2).wait_send()
+        for d in (1, 2, 3):
+            bias_hop(d).wait_send()
+            for half in range(2):
+                q_piece(d, half).wait_send()
+        for dz in (1, 2, 3):
+
+            @pl.when(z >= dz)
+            def _():
+                q_down(dz).wait_send()
+
+    return up_weights, down_weights, all_sent
+
+
+def feed_forward_part(
+    up_weights, down_weights, n_ref, m_ref, mine_ref, w_ref, cg_ref, cv_ref, out_ref,
     all_ref, rim_ref, up_ref, down_ref, gate_ref, value_ref, p_ref, twin_buf, sum_buf, relay_buf,
     ring_buf, w_sem, ring_send, ring_recv, twin_send, twin_recv, rim_send, rim_recv, own_sem,
     pair_send, pair_recv, relay_send, relay_recv, back_send, back_recv,
@@ -522,20 +534,26 @@
     other = 2 * x + 1 - core
     halves = (slice(0, part), slice(part, rows))
 
-    def weight_copies(k):
+    def up_copy(k, src):
         at = slice(k * deep, (k + 1) * deep)
-        return (
-            pltpu.make_async_copy(
-                w_ref.at[k, pl.ds(0, 2 * units)], up_ref.at[:, at], w_sem.at[0, k]
-            ),
-            pltpu.make_async_copy(
-                w_ref.at[k, pl.ds(2 * units, units)], down_ref.at[:, at], w_sem.at[1, k]
-            ),
-        )
-
-    for k in range(shards):
-        for copy in weight_copies(k):
-            copy.start()
+        return pltpu.make_async_copy(src.at[pl.ds(0, 2 * units)], up_ref.at[:, at], w_sem.at[0, k])
+
+    def down_copy(k, src):
+        at = slice(k * deep, (k + 1) * deep)
+        return pltpu.make_async_copy(
+            src.at[pl.ds(2 * units, units)], down_ref.at[:, at], w_sem.at[1, k]
+        )
+
+    def load(copy):
+        for k in range(shards):
+
+            @pl.when(block == k)
+            def _():
+                copy(k, mine_ref).start()
+
+            @pl.when(block != k)
+            def _():
+                copy(k, w_ref.at[k]).start()
 
     def spot(chip, half, of_core):
         return all_ref.at[2 * chip + of_core, pl.ds(half * part, part)]
@@ -564,21 +582,6 @@
         )
 
     last = (x == SIDE - 1) & (core == 1) & (block < SIDE * SIDE - 1)
-    barrier = pltpu.get_barrier_semaphore()
-
-    @pl.when(block > 0)
-    def _():
-        pl.semaphore_signal(
-            barrier,
-            inc=1,
-            device_id={"sp": block - 1, "tp": 2 * SIDE - 1},
-            device_id_type=pl.DeviceIdType.MESH,
-        )
-
-    meet(
-        [{"tp": 2 * right + core}, {"tp": 2 * left + core}, {"tp": other}],
-        jnp.where(last, 2 * SIDE, 0),
-    )
     own = pltpu.make_async_copy(n_ref, all_ref.at[2 * x + core], own_sem)
     ring(None, 0, right, 0).start()
     ring(None, 1, left, 1).start()
@@ -621,11 +624,15 @@
         for half in range(2):
             arrived(spot(chip, half, 1 - core), twin_recv.at[chip, half])
 
+    up_weights()
+    load(up_copy)
+    down_weights(2)
     for k in range(shards):
-        weight_copies(k)[0].wait()
+        up_copy(k, mine_ref).wait()
     own.wait()
     twin_arrived(x)
     project_up(x)
+    down_weights(3)
     arrived(spot(left, 0, core), ring_recv.at[left, 0])
     ring(left, 0, right, 2).start()
     twin(left, 0).start()
@@ -633,6 +640,8 @@
     ring(right, 1, left, 2).start()
     twin(right, 1).start()
 
+    down_weights(4)
+
     @pl.when(block > 0)
     def _():
         arrived(rim_ref, rim_recv)
@@ -647,15 +656,21 @@
     for chip, half in ((left, 1), (right, 0)):
         arrived(spot(chip, half, core), ring_recv.at[chip, half])
         twin(chip, half).start()
+    down_weights(5)
+    down_weights(6)
     twin_arrived(right)
     project_up(right)
+    down_weights(7)
+    down_weights(8)
     twin_arrived(left)
     project_up(left)
+    down_weights(9)
+    load(down_copy)
     for half in range(2):
         arrived(spot(across, half, core), ring_recv.at[across, half])
         twin(across, half).start()
     for k in range(shards):
-        weight_copies(k)[1].wait()
+        down_copy(k, mine_ref).wait()
 
     def pair(chip):
         return remote_copy(
@@ -747,42 +762,112 @@
             back(side, half).wait_send()
 
 
-def feed_forward(normed, middle, whole, conv_gate, conv_value):
-    rows, depth = normed.shape
+def middle_part(os_ref, gs_ref, res_ref, ow_ref, gain_ref, m_ref, n_ref):
+    z = position()[1]
+    heads, groups, rows, width = os_ref.shape
+    outs = [jnp.zeros((rows, width), jnp.float32) for _ in range(heads)]
+    later = jnp.zeros((rows, 128), jnp.float32)
+    for group in range(groups - 1, -1, -1):
+        valid = group <= z
+        weight = jnp.exp2(-later)
+        for h in range(heads):
+            term = jnp.where(valid, os_ref[h, group].astype(jnp.float32), 0.0)
+            outs[h] = outs[h] + term * weight[:, h : h + 1]
+        if group:
+            left = jnp.concatenate([gs_ref[h, group, 0:1, :] for h in range(heads)], axis=0)
+            left = jnp.where(valid, left, 0.0)
+            later = later + jnp.concatenate([left] * (128 // heads), axis=0).T
+    attended = jnp.concatenate(outs, axis=1).astype(jnp.bfloat16)
+    projected = jnp.dot(attended, ow_ref[...], preferred_element_type=jnp.float32)
+    middle = (res_ref[...].astype(jnp.float32) + projected).astype(jnp.bfloat16)
+    m_ref[...] = middle
+    wide = middle.astype(jnp.float32)
+    scale = lax.rsqrt(jnp.mean(wide * wide, axis=-1, keepdims=True) + EPS)
+    n_ref[...] = (wide * scale * gain_ref[...]).astype(jnp.bfloat16)
+
+
+def layer_kernel(*refs):
+    q, k, v, b, w, res, ow, gain, cg, cv, out, whole = refs[:12]
+    os_ref, gs_ref, ow_ref, m_ref, n_ref, ow_sem = refs[12:18]
+    attend_refs = refs[18 : 18 + ATTEND]
+    ff_refs = refs[18 + ATTEND :]
+    ow_copy = pltpu.make_async_copy(ow, ow_ref, ow_sem)
+    ow_copy.start()
+    up_weights, down_weights, all_sent = attend_part(q, k, v, b, w, os_ref, gs_ref, whole, *attend_refs)
+    ow_copy.wait()
+    middle_part(os_ref, gs_ref, res, ow_ref, gain, m_ref, n_ref)
+    feed_forward_part(up_weights, down_weights, n_ref, m_ref, w, whole, cg, cv, out, *ff_refs)
+    all_sent()
+
+
+def layer(queries, keys, values, bias_rows, weights, residual, out_weight, gain, conv_gate, conv_value):
+    rows, width = queries.shape
+    share, depth = residual.shape
     units = conv_gate.shape[1]
-    total = 2 * SIDE * rows
+    heads = lax.axis_size("tp")
+    count = SIDE * SIDE
+    quarter = rows // SIDE
+    anywhere = pl.BlockSpec(memory_space=pl.ANY)
     vmem = pl.BlockSpec(memory_space=pltpu.VMEM)
     dma = pltpu.SemaphoreType.DMA
     bf16 = jnp.bfloat16
+    f32 = jnp.float32
+    attend_scratch = [
+        pltpu.VMEM((count, quarter, width), bf16),
+        pltpu.VMEM((SIDE, rows, width), bf16),
+        pltpu.VMEM((SIDE, rows, width), bf16),
+        pltpu.VMEM((SIDE,) + bias_rows.shape, bf16),
+        pltpu.VMEM((count, quarter, width), bf16),
+        pltpu.VMEM((count, 2, 8, 128), f32),
+        pltpu.VMEM((rows, width), f32),
+        pltpu.VMEM((rows, 128), f32),
+        pltpu.VMEM((SIDE, rows, width), f32),
+        pltpu.VMEM((SIDE, rows, 128), f32),
+        dma((2, 3)), dma((2, SIDE)), dma((2,)), dma((SIDE,)), dma((SIDE,)), dma(()),
+        dma((SIDE, 2)), dma((SIDE, 2)), dma((2,)), dma((SIDE,)), dma((SIDE,)),
+        dma((2, 2, 2, 2)), dma((2, 2, 2)), dma((2, 2, SIDE, 2, 2)), dma((2, 2, SIDE, 2)),
+        dma((2, 2, count, 2)), dma((2, count, 2)), dma((2, heads, SIDE)),
+    ]
+    ff_scratch = [
+        pltpu.VMEM((2 * SIDE, share, depth), bf16),
+        pltpu.VMEM((RIM, depth), bf16),
+        pltpu.VMEM((2 * units, depth), bf16),
+        pltpu.VMEM((units, depth), bf16),
+        pltpu.VMEM((RIM + rows, units), f32),
+        pltpu.VMEM((RIM + rows, units), f32),
+        pltpu.VMEM((2 * SIDE, share, depth), bf16),
+        pltpu.VMEM((SIDE, share, depth), bf16),
+        pltpu.VMEM((3, share, depth), bf16),
+        pltpu.VMEM((2, share // 2, depth), bf16),
+        pltpu.VMEM((2, share, depth), bf16),
+        dma((2, count)),
+        dma((3, 2)), dma((SIDE, 2)), dma((SIDE, 2)), dma((SIDE, 2)), dma((2 * SIDE,)), dma(()), dma(()),
+        dma((SIDE,)), dma((SIDE,)), dma((2,)), dma((2,)), dma((2, 2)), dma((2, 2)),
+    ]
+    assert len(attend_scratch) == ATTEND
     return pl.pallas_call(
-        feed_forward_kernel,
-        out_shape=jax.ShapeDtypeStruct((rows, depth), bf16),
-        in_specs=[vmem, vmem, pl.BlockSpec(memory_space=pl.ANY), vmem, vmem],
-        out_specs=vmem,
+        layer_kernel,
+        out_shape=(
+            jax.ShapeDtypeStruct((share, depth), bf16),
+            jax.ShapeDtypeStruct((count,) + weights.shape, bf16),
+        ),
+        in_specs=[anywhere, anywhere, anywhere, vmem, anywhere, vmem, anywhere, vmem, vmem, vmem],
+        out_specs=[vmem, anywhere],
         scratch_shapes=[
-            pltpu.VMEM((2 * SIDE, rows, depth), bf16),
-            pltpu.VMEM((RIM, depth), bf16),
-            pltpu.VMEM((2 * units, depth), bf16),
-            pltpu.VMEM((units, depth), bf16),
-            pltpu.VMEM((RIM + total, units), jnp.float32),
-            pltpu.VMEM((RIM + total, units), jnp.float32),
-            pltpu.VMEM((2 * SIDE, rows, depth), bf16),
-            pltpu.VMEM((SIDE, rows, depth), bf16),
-            pltpu.VMEM((3, rows, depth), bf16),
-            pltpu.VMEM((2, rows // 2, depth), bf16),
-            pltpu.VMEM((2, rows, depth), bf16),
-            dma((2, whole.shape[0])),
-            dma((3, 2)), dma((SIDE, 2)), dma((SIDE, 2)), dma((SIDE, 2)), dma((2 * SIDE,)), dma(()), dma(()),
-            dma((SIDE,)), dma((SIDE,)), dma((2,)), dma((2,)), dma((2, 2)), dma((2, 2)),
+            pltpu.VMEM((heads, SIDE, share, width), bf16),
+            pltpu.VMEM((heads, SIDE, 8, 128), f32),
+            pltpu.VMEM(out_weight.shape, bf16),
+            pltpu.VMEM((share, depth), bf16),
+            pltpu.VMEM((share, depth), bf16),
+            dma(()),
+            *attend_scratch,
+            *ff_scratch,
         ],
         compiler_params=pltpu.CompilerParams(
-            has_side_effects=True, collective_id=1, vmem_limit_bytes=VMEM
+            has_side_effects=True, collective_id=0, vmem_limit_bytes=VMEM
         ),
-        cost_estimate=pl.CostEstimate(
-            flops=9 * 10**9, bytes_accessed=12 * 2**20, transcendentals=0
-        ),
-        name="feed_forward",
-    )(normed, middle, whole, conv_gate, conv_value)
+        name="layer",
+    )(queries, keys, values, bias_rows, weights, residual, out_weight, gain, conv_gate, conv_value)[0]
 
 
 def local(
@@ -800,23 +885,21 @@
     conv_value,
 ):
     rows_here = queries.shape[0]
-    model_width = residual.shape[1]
     bias_rows = stick_bias.reshape(rows_here // CHUNK, CHUNK)
     bias_rows = jnp.pad(bias_rows, ((0, PAD - bias_rows.shape[0]), (0, 0)))
     weights = jnp.concatenate([gate_weight.T, value_weight.T, down_weight.T], axis=0)
-    parts, logs, whole = attend(
-        queries, keys, values, bias_rows, weights, lax.axis_size("tp")
+    return layer(
+        queries,
+        keys,
+        values,
+        bias_rows,
+        weights,
+        residual,
+        out_weight,
+        norm_gain.reshape(1, -1),
+        conv_gate,
+        conv_value,
     )
-    row_heads = combine(parts, logs)
-    projected = jnp.dot(row_heads, out_weight, preferred_element_type=jnp.float32)
-    middle = (residual.astype(jnp.float32) + projected).astype(jnp.bfloat16)
-    middle_f = middle.astype(jnp.float32)
-    normed = (
-        middle_f
-        * lax.rsqrt(jnp.mean(middle_f * middle_f, axis=-1, keepdims=True) + EPS)
-        * norm_gain
-    ).astype(jnp.bfloat16)
-    return feed_forward(normed, middle, whole, conv_gate, conv_value)
 
 
 def solution(mesh):

time: 162 us -> 150 us (0.926); the launches traced: 159 us -> 150 us
  matrix products: 3.04 us -> 0 us
  other arithmetic: 5.67 us -> 2.67 us
  local copies, waits for them, and re-layouts: 4.57 us -> 2.5 us
    dot_general x1 -> x0, matrix products: 3.04 us -> none  [local(): jnp.dot(row_heads, out_weight, preferred_element_type=jnp.float32)]
    reduce_sum x1 -> x0, other arithmetic: 1.82 us -> none  [combine(): total = jnp.sum(terms * weight[..., None], axis=1)]
    pallas_call x2 -> x1, Pallas kernels: 146 us -> 145 us  [layer(): pl.pallas_call(layer_kernel, out_shape=(jax.ShapeDtypeStruct((share, dept...]
where the time goes in v6:
time: 150 us
  Pallas kernels  145 us (97%)
  other arithmetic  2.67 us (2%)
  local copies, waits for them, and re-layouts  2.5 us (2%)
    pallas_call x1, Pallas kernels, layer(): pl.pallas_call(layer_kernel, out_shape=(jax.ShapeDtypeStruct((share, dept...  145 us

profile of v6, /device:TPU:26, one launch (start us, length us, event | category | flops | bytes accessed | tf_op | source)
XLA Modules:
  0.0 149.9 jit_solution(47564713612177320)
XLA Ops:
  0.0 0.7 reduce
  0.7 0.6 pad.4.refs_3_
  1.3 2.0 %pad_maximum_fusion.refs_4_ = bf16[2112,128]{1,0:T(8,128)(2,1)} fusion(bf16[704,128]{1,0:T(8,128)(2,1)} %bitcast.4, bf16[704,128]{1,0:T(8,128)(2,1)} %bitcast.5, bf16[704,128]{1,0:T(8,128)(2,1)} %bitcast.6), kind=kLoop, calls=%fused_computation | loop fusion | flops 1622016 | bytes 1081344 | tf_op jit(solution)/shard_map/concatenate | solution.py:890
  3.3 144.8 %layer.1 = (bf16[128,2048]{1,0:T(8,128)(2,1)}, bf16[16,2112,128]{2,1,0:T(8,128)(2,1)}) custom-call(bf16[1024,128]{1,0:T(8,128)(2,1)} %refs_0_.1, bf16[1024,128]{1,0:T(8,128)(2,1)} %refs_1_.1, bf16[1024,128]{1,0:T(8,128)(2,1)} %refs_2_.1, bf16[16,256]{1,0:T(8,128)(2,1)} %pad.4.refs_3_, bf16[2112,128]{1,0:T(8,128)(2,1)} %pad_maximum_fusion.refs_4_, ...), custom_call_target="tpu_custom_call" | custom-call | tf_op jit(solution)/shard_map/layer/pallas_call | solution.py:848
  148.1 1.9 %copy.14 = bf16[128,2048]{1,0:T(8,128)(2,1)} copy(bf16[128,2048]{1,0:T(8,128)(2,1)} %get-tuple-element.6) | data formatting | bytes 1048576
  (1 shorter events, 0.0 us)

commit v7 on v6

--- a/solution.py
+++ b/solution.py
@@ -15,7 +15,7 @@
 VMEM = 67_000_000
 ATTEND = 28
 STAGES = (
-    (0, 0, 3), (1, 0, 4), (2, 0, 5), (3, 0, 6), (4, 0, 7), (6, 0, 8), (11, 1, 0), (11, 1, 1),
+    (0, 0, 3), (2, 0, 4), (4, 0, 5), (5, 0, 6), (7, 0, 7), (9, 0, 8), (11, 1, 0), (11, 1, 1),
 )
 
 
@@ -712,10 +712,8 @@
 
     project_down(right)
     pair(right).start()
-    project_down(x)
-    pair(x).start()
+    twin_arrived(across)
     direct(0)
-    twin_arrived(across)
     project_up(across)
     project_down(across)
     pair(across).start()
@@ -726,13 +724,15 @@
     project_down(left)
     pair(left).start()
     direct(1)
-    arrived(twin_buf.at[x], pair_recv.at[x])
+    project_down(x)
+    pair(x).start()
     for side in range(2):
         to = (right, left)[side]
         arrived(relay_buf.at[side], relay_recv.at[side])
         total = pair_sum(to, side) + relay_buf[side].astype(jnp.float32)
         sum_buf[1 + side, halves[side], :] = total.astype(jnp.bfloat16)
         back(side, side).start()
+    arrived(twin_buf.at[x], pair_recv.at[x])
     for half in range(2):
         total = m_ref[halves[half], :].astype(jnp.float32) + pair_sum(x, half)
         for side in (1 - half, half):

time: 150 us -> 148 us (0.987)
  Pallas kernels: 145 us -> 142 us
    pallas_call x1, Pallas kernels: 145 us -> 142 us  [layer(): pl.pallas_call(layer_kernel, out_shape=(jax.ShapeDtypeStruct((share, dept...]
where the time goes in v7:
time: 148 us
  Pallas kernels  142 us (96%)
  other arithmetic  2.67 us (2%)
  local copies, waits for them, and re-layouts  2.5 us (2%)
    pallas_call x1, Pallas kernels, layer(): pl.pallas_call(layer_kernel, out_shape=(jax.ShapeDtypeStruct((share, dept...  142 us

profile of v7, /device:TPU:26, one launch (start us, length us, event | category | flops | bytes accessed | tf_op | source)
XLA Modules:
  0.0 147.6 jit_solution(384945984513677417)
XLA Ops:
  0.0 0.7 reduce
  0.7 0.6 pad.4.refs_3_
  1.3 2.0 %pad_maximum_fusion.refs_4_ = bf16[2112,128]{1,0:T(8,128)(2,1)} fusion(bf16[704,128]{1,0:T(8,128)(2,1)} %bitcast.4, bf16[704,128]{1,0:T(8,128)(2,1)} %bitcast.5, bf16[704,128]{1,0:T(8,128)(2,1)} %bitcast.6), kind=kLoop, calls=%fused_computation | loop fusion | flops 1622016 | bytes 1081344 | tf_op jit(solution)/shard_map/concatenate | solution.py:890
  3.3 142.4 %layer.1 = (bf16[128,2048]{1,0:T(8,128)(2,1)}, bf16[16,2112,128]{2,1,0:T(8,128)(2,1)}) custom-call(bf16[1024,128]{1,0:T(8,128)(2,1)} %refs_0_.1, bf16[1024,128]{1,0:T(8,128)(2,1)} %refs_1_.1, bf16[1024,128]{1,0:T(8,128)(2,1)} %refs_2_.1, bf16[16,256]{1,0:T(8,128)(2,1)} %pad.4.refs_3_, bf16[2112,128]{1,0:T(8,128)(2,1)} %pad_maximum_fusion.refs_4_, ...), custom_call_target="tpu_custom_call" | custom-call | tf_op jit(solution)/shard_map/layer/pallas_call | solution.py:848
  145.7 1.9 %copy.14 = bf16[128,2048]{1,0:T(8,128)(2,1)} copy(bf16[128,2048]{1,0:T(8,128)(2,1)} %get-tuple-element.6) | data formatting | bytes 1048576
  (1 shorter events, 0.0 us)
